TPU v7x, 256 devices: a whole 4x4x8 slice. The times are simulated.
256 devices in a mesh: sp: 32 (over z, x), tp: 8 (over y, core).
Axes of the slice: x: 4, y: 4, z: 8, core: 2. Of those that a mesh axis runs over, the one named last changes fastest.
Arguments:
- sequence_embeddings: bfloat16 [12288, 2048], P('sp'), may hold values from -6 to 6
- entry_rescale_vector: bfloat16 [2048], replicated, may hold values from 0.099609375 to 1.8984375
- probe_matrix: bfloat16 [2048, 1024], P('sp', 'tp'), may hold values from -0.125 to 0.125
- onward_retain_matrix: bfloat16 [2048, 1024], P('sp', 'tp'), may hold values from -0.125 to 0.125
- reverse_retain_matrix: bfloat16 [2048, 1024], P('sp', 'tp'), may hold values from -0.125 to 0.125
- content_matrix: bfloat16 [2048, 1024], P('sp', 'tp'), may hold values from -0.125 to 0.125
- emission_switch_matrix: bfloat16 [2048, 1024], P('sp', 'tp'), may hold values from -0.125 to 0.125
- pointwise_content_matrix: bfloat16 [2048, 1024], P('sp', 'tp'), may hold values from -0.125 to 0.125
- pointwise_switch_matrix: bfloat16 [2048, 1024], P('sp', 'tp'), may hold values from -0.125 to 0.125
- retain_lower_slack: float32 [2, 1024], P(None, 'tp'), may hold values from 0 to 0.034, as said below
- extra_log_shrink: float32 [2, 12288, 8], P(None, 'sp', 'tp'), may hold values from -1 to 0
- subspace_rescale: bfloat16 [128], replicated, may hold values from 0.099609375 to 1.8984375
- filter_kernel_coefs: bfloat16 [31, 1024], P(None, 'tp'), may hold values from -1 to 1
- channel_cluster_scale: bfloat16 [1024], P('tp'), may hold values from 0.099609375 to 1.8984375
- scan_readout_matrix: bfloat16 [1024, 2048], P('tp', 'sp'), may hold values from -0.125 to 0.125
- filter_readout_matrix: bfloat16 [1024, 2048], P('tp', 'sp'), may hold values from -0.125 to 0.125
Outputs:
- mixed: bfloat16 [12288, 2048], P(('sp', 'tp'))
Inputs may be any that keep to these rules, and one draw needn't show every extreme that they name: `retain_lower_slack`: every entry is positive.
All inputs are finite; a program needn't handle non-finite values.
Results may differ from a plain program's by a relative error of at most 0.015.
Values may be sent and summed in bfloat16 or wider, within the bound.
No kernel may reach another device: no remote copies, remote signals or barrier semaphores. Data moves between devices by JAX's collectives and lax.ppermute only.
A program may use at most 64 MiB of HBM per device.

v0:
```python
import jax
import jax.numpy as jnp
from jax import lax
from jax.experimental import pallas as pl
from jax.experimental.pallas import tpu as pltpu
from jax.sharding import Mesh
from jax.sharding import PartitionSpec as P


CONV_KW = 31
BLOCK = 64
HEAD = 128
PACK = 144
BF = jnp.bfloat16
F32 = jnp.float32
ROOM = pltpu.CompilerParams(vmem_limit_bytes=24 * 2**20)
SMEM = pl.BlockSpec(memory_space=pltpu.SMEM)
VMEM = pl.BlockSpec(memory_space=pltpu.VMEM)
ANY = pl.BlockSpec(memory_space=pl.ANY)


def ring(count, step):
    return [(i, (i + step) % count) for i in range(count)]


def shift(array, axis, step):
    return lax.ppermute(array, axis, ring(lax.axis_size(axis), step))


def line(array, axes, step):
    count = lax.axis_size(axes)
    pairs = [(i, i + step) for i in range(count) if 0 <= i + step < count]
    return lax.ppermute(array, axes, pairs)


def ordered(first, *arrays):
    return lax.optimization_barrier((first, *arrays))


def keep(array):
    return pltpu.with_memory_space_constraint(array, pltpu.VMEM)


def far_off(array):
    return pltpu.with_memory_space_constraint(array, pltpu.HBM)


def kernel_call(body, micros, outs, *operands, scratch=(), left=()):
    return pl.pallas_call(
        body,
        out_shape=tuple(outs),
        in_specs=[
            SMEM if o.dtype == jnp.int32 else ANY if k in left else VMEM
            for k, o in enumerate(operands)
        ],
        scratch_shapes=list(scratch),
        compiler_params=ROOM,
        cost_estimate=pl.CostEstimate(
            flops=int(micros * 4e6), transcendentals=0, bytes_accessed=0
        ),
    )(*operands)


def nt(a, b):
    return lax.dot_general(a, b, (((1,), (1,)), ((), ())), preferred_element_type=F32)


def tn(a, b):
    return lax.dot_general(a, b, (((0,), (0,)), ((), ())), preferred_element_type=F32)


def dot(a, b):
    return jnp.dot(a, b, preferred_element_type=F32)


def collect_kernel(x, *refs):
    first, later, top, bottom, done = refs[-5:]
    edge = top.shape[0]
    rows = (x.at[:edge], x.at[x.shape[0] - edge :])
    copies = [
        pltpu.make_async_copy(source, into, done.at[k])
        for k, (source, into) in enumerate(zip(rows, (top, bottom)))
    ]
    for copy in copies:
        copy.start()
    for k, ref in enumerate(refs[:3]):
        for z in range(8):
            first[z, :, k * HEAD : (k + 1) * HEAD] = ref[...]
    for k, ref in enumerate(refs[3:-5]):
        later[:, k * HEAD : (k + 1) * HEAD] = ref[...]
    for copy in copies:
        copy.wait()


def stack_kernel(own, ahead, far, behind, later):
    for k, ref in enumerate((own, ahead, far, behind)):
        later[k * 64 : (k + 1) * 64] = ref[...]


def normalize_kernel(place, x, gain, out, *other):
    turn = place[1]
    floats = x[...].astype(F32)
    factor = lax.rsqrt(jnp.mean(floats * floats, axis=-1, keepdims=True) + 1e-06)
    low = lax.broadcasted_iota(jnp.int32, (x.shape[0], HEAD), 1) < 64
    for pair in range(4):
        pieces = []
        for k in (2 * pair, 2 * pair + 1):
            at = slice(k * 256, (k + 1) * 256)
            scaled = x[:, at].astype(F32) * factor * gain[:, at].astype(F32)
            turned = pltpu.roll(scaled, turn, 1)
            out[:, at] = turned.astype(BF)
            pieces.append((turned[:, :HEAD], turned[:, HEAD:]))
        if other:
            for half in range(2):
                one, two = pieces[0][half], pieces[1][half]
                even = jnp.where(low, one, pltpu.roll(two, 64, 1))
                odd = jnp.where(low, pltpu.roll(one, 64, 1), two)
                for piece, value in ((2 * half, even), (2 * half + 1, odd)):
                    at = piece * 512 + pair * HEAD
                    other[0][:, at : at + HEAD] = value.astype(BF)


def normalized(place, x, gain, count):
    outs = [pltpu.VMEM(x.shape, BF)] * count
    return kernel_call(normalize_kernel, 3, outs, place, x, gain)


def near_scores_kernel(normed, own, ahead, behind, out):
    total = dot(normed[:, :512], own[...])
    total = total + dot(normed[:, 512:1024], ahead[...])
    out[...] = total + dot(normed[:, 1536:], behind[...])


def pack(state, log):
    high = log.astype(BF).astype(F32)
    pad = jnp.zeros((PACK - HEAD - 8, HEAD), F32)
    rows = lax.broadcasted_iota(jnp.int32, (8, HEAD), 0)
    logs = jnp.where(rows == 0, high, jnp.where(rows == 1, log - high, 0.0))
    return jnp.concatenate([state, logs, pad], axis=0).astype(BF)


def unpack(message):
    state = message[:HEAD].astype(F32)
    logs = message[HEAD:PACK].astype(F32)
    return state, logs[0:1] + logs[1:2]


def gates_kernel(near, normed, far_low, far_high, slack, extra, values_o, gap_o, cum_o, start_o, passed_o, send):
    length = near.shape[0]
    blocks = length // BLOCK
    scores = near[...] + dot(normed[:, 1024:1280], far_low[...])
    scores = scores + dot(normed[:, 1280:1536], far_high[...])
    inside = lax.rem(lax.broadcasted_iota(jnp.int32, (length, HEAD), 0), BLOCK)
    v = scores[:, 256:].astype(BF)
    values_o[...] = v
    for d in range(2):
        gap = slack[d : d + 1, :] * jax.nn.sigmoid(-scores[:, d * HEAD : (d + 1) * HEAD])
        cum = jnp.log1p(-gap) + extra[d]
        step = 1
        while step < BLOCK:
            if d == 0:
                moved = jnp.where(inside >= step, pltpu.roll(cum, step, 0), 0.0)
            else:
                moved = jnp.where(inside < BLOCK - step, pltpu.roll(cum, length - step, 0), 0.0)
            cum = cum + moved
            step *= 2
        gap_o[d] = gap
        cum_o[d] = cum
        state = jnp.zeros((HEAD, HEAD), F32)
        passed = jnp.zeros((1, HEAD), F32)
        for n in range(blocks) if d == 0 else reversed(range(blocks)):
            rows = slice(n * BLOCK, (n + 1) * BLOCK)
            last = n * BLOCK + (BLOCK - 1 if d == 0 else 0)
            total = cum[last : last + 1]
            fade = gap[rows] * jnp.exp(total - cum[rows])
            start_o[d, n] = state.astype(BF)
            passed_o[d, n : n + 1] = passed
            state = jnp.exp(total) * state + tn(v[rows], fade.astype(BF))
            passed = passed + total
        send[d] = pack(state, passed)


def row_kernel(place, own, ahead, far, behind, before_o, send, got):
    x, z = place[2], place[0]
    for k, ref in enumerate((own, ahead, far, behind)):
        got[lax.rem(x + k, 4)] = ref[...]
    messages = []
    for d in range(2):
        state = jnp.zeros((HEAD, HEAD), F32)
        log = jnp.zeros((1, HEAD), F32)
        before, passed = state, log
        for k in range(4) if d == 0 else reversed(range(4)):
            before = jnp.where(k == x, state, before)
            passed = jnp.where(k == x, log, passed)
            new, step = unpack(got[k, d])
            state = jnp.exp(step) * state + new
            log = log + step
        before_o[d, :HEAD] = before
        before_o[d, HEAD : HEAD + 8] = jnp.broadcast_to(passed, (8, HEAD))
        messages.append(pack(state, log))
    for k in range(8):
        send[k] = jnp.where(k > z, messages[0], messages[1])


def later_kernel(place, normed, edges, *refs):
    pieces = refs[:9]
    values, gap, cum, start, passed, taps, scale = refs[9:16]
    local_o, lifted_o, gate_o, conv_o, columns_o, query, glu, weights, done = refs[16:]
    x, z_here = place[2], place[0]
    copies = []
    for k, piece in enumerate(pieces):
        step, inside = (k, 0) if k < 5 else (k - 1, 128 if k == 5 else 0)
        to = pl.multiple_of(lax.rem(z_here + step, 8) * 256 + inside, 128)
        into = weights.at[pl.ds(to, piece.shape[0])]
        copies.append(pltpu.make_async_copy(piece, into, done.at[k]))
        copies[-1].start()
    for copy in copies:
        copy.wait()
    length = normed.shape[0]
    blocks = length // BLOCK
    pre = dot(normed[...], weights[:, :256])
    query[...] = pre[:, :HEAD] * jax.nn.sigmoid(pre[:, :HEAD])
    gate_o[...] = pre[:, HEAD:] * jax.nn.sigmoid(pre[:, HEAD:])

    def gated(rows):
        pair = dot(rows, weights[:, 256:512])
        return (pair[:, :HEAD] * jax.nn.sigmoid(pair[:, HEAD:])).astype(BF).astype(F32)

    glu[16 : 16 + length] = gated(normed[...])
    edge = gated(edges[...])
    glu[:16] = edge[:16]
    glu[16 + length :] = edge[16:]
    framed = glu[...]
    kernel = taps[...].astype(F32)
    total = None
    for r in range(8):
        turned = framed if r == 0 else pltpu.roll(framed, length + 32 - r, 0)
        for j in range(CONV_KW):
            if (1 + j) % 8 == r:
                at = (1 + j) - r
                part = turned[at : at + length] * kernel[j : j + 1]
                total = part if total is None else total + part
    centred = total - jnp.mean(total, axis=-1, keepdims=True)
    variance = jnp.mean(centred * centred, axis=-1, keepdims=True)
    standard = centred * lax.rsqrt(variance + 1e-05) * scale[...].astype(F32)
    conv_o[...] = (standard * jax.nn.sigmoid(standard)).astype(BF)

    for k in range(4):
        turn = lax.rem(x + k, 4)
        for z in range(8):
            to = pl.multiple_of((z * 4 + turn) * 64, 64)
            at = (z * 4 + k) * 64
            columns_o[pl.ds(to, 64)] = weights[at : at + 64, 512:768]

    t = lax.broadcasted_iota(jnp.int32, (BLOCK, BLOCK), 0)
    s = lax.broadcasted_iota(jnp.int32, (BLOCK, BLOCK), 1)
    for n in range(blocks):
        rows = slice(n * BLOCK, (n + 1) * BLOCK)
        q = query[rows]
        v = values[rows]
        total = jnp.zeros((BLOCK, HEAD), F32)
        for d in range(2):
            c = cum[d, rows]
            lifted = q * jnp.exp(c)
            lowered = gap[d, rows] * jnp.exp(-c)
            scores = nt(lifted.astype(BF), lowered.astype(BF))
            scores = jnp.where(s <= t if d == 0 else s >= t, scores, 0.0)
            total = total + dot(scores.astype(BF), v)
            total = total + nt(lifted.astype(BF), start[d, n])
            lifted_o[d, rows] = (lifted * jnp.exp(passed[d, n : n + 1])).astype(BF)
        local_o[rows] = total


def readout_kernel(place, local, lifted, every, before, rescale, gate, out):
    z = place[0]
    summed = local[...]
    for d in range(2):
        state = jnp.zeros((HEAD, HEAD), F32)
        for k in range(8) if d == 0 else reversed(range(8)):
            new, step = unpack(every[k])
            state = jnp.where(k < z if d == 0 else k > z, jnp.exp(step) * state + new, state)
        incoming = before[d, :HEAD] + jnp.exp(before[d, HEAD : HEAD + 1]) * state
        summed = summed + nt(lifted[d], incoming.astype(BF))
    factor = lax.rsqrt(jnp.mean(summed * summed, axis=-1, keepdims=True) + 1e-06)
    out[...] = (summed * factor * rescale[...].astype(F32) * gate[...]).astype(BF)


def project_out_kernel(place, rec, conv, columns, out):
    core = place[0]
    at = [pl.multiple_of(k * 96 + core * 48, 16) for k in range(4)]
    left = jnp.concatenate([rec[pl.ds(k, 48)] for k in at], axis=0)
    right = jnp.concatenate([conv[pl.ds(k, 48)] for k in at], axis=0)
    rows = jnp.concatenate([left, right], axis=1)
    for c in range(0, 2048, 512):
        part = nt(rows, columns[c : c + 512])
        for k in range(4):
            out[k, :, c : c + 512] = part[k * 48 : (k + 1) * 48].astype(out.dtype)


def meet_kernel(place, mine, got, far_low, far_high, ahead, behind, own):
    y = place[3]

    def block(step):
        k = lax.rem(y + step, 4)
        return mine[k] + got[k].astype(F32)

    far = block(2)
    far_low[...] = far[:, :1024].astype(BF)
    far_high[...] = far[:, 1024:].astype(BF)
    ahead[...] = block(1)
    behind[...] = block(3)
    own[...] = block(0)


def relay_kernel(ahead, behind, low, high, ahead_o, behind_o):
    ahead_o[:, :1024] = (ahead[:, :1024] + low[...].astype(F32)).astype(BF)
    ahead_o[:, 1024:] = ahead[:, 1024:].astype(BF)
    behind_o[:, :1024] = behind[:, :1024].astype(BF)
    behind_o[:, 1024:] = (behind[:, 1024:] + high[...].astype(F32)).astype(BF)


def layer(
    sequence_embeddings,
    entry_rescale_vector,
    probe_matrix,
    onward_retain_matrix,
    reverse_retain_matrix,
    content_matrix,
    emission_switch_matrix,
    pointwise_content_matrix,
    pointwise_switch_matrix,
    retain_lower_slack,
    extra_log_shrink,
    subspace_rescale,
    filter_kernel_coefs,
    channel_cluster_scale,
    scan_readout_matrix,
    filter_readout_matrix,
):
    x, z, y = (lax.axis_index(axis) for axis in "xzy")
    core = lax.axis_index("core")
    length = sequence_embeddings.shape[0]
    gain = entry_rescale_vector[None]
    place = jnp.stack([z, lax.rem(4 - x, 4) * 64, x, y]).astype(jnp.int32)
    edge = pltpu.VMEM((16, sequence_embeddings.shape[1]), BF)
    first, shard, top, bottom = kernel_call(
        collect_kernel,
        2,
        [pltpu.VMEM((8, 64, 384), BF), pltpu.VMEM((64, 768), BF), edge, edge],
        far_off(sequence_embeddings),
        *(
            far_off(weight)
            for weight in (
                onward_retain_matrix,
                reverse_retain_matrix,
                content_matrix,
                probe_matrix,
                emission_switch_matrix,
                pointwise_content_matrix,
                pointwise_switch_matrix,
                scan_readout_matrix.T,
                filter_readout_matrix.T,
            )
        ),
        scratch=(pltpu.SemaphoreType.DMA((2,)),),
        left=(0,),
    )
    first = lax.all_to_all(first, "z", 0, 0, tiled=True).reshape(512, 384)
    ahead, far, behind = shift(shard, "x", -1), shift(shard, "x", 2), shift(shard, "x", 1)
    normed, normed_first = normalized(place, far_off(sequence_embeddings), gain, 2)
    low, high = line(bottom, ("z", "x"), 1), line(top, ("z", "x"), -1)
    normed, normed_first, shard, ahead, far, behind, low, high = lax.optimization_barrier(
        (normed, normed_first, shard, ahead, far, behind, low, high)
    )
    (edges,) = normalized(place, jnp.concatenate([low, high], axis=0), gain, 1)
    (later,) = kernel_call(
        stack_kernel,
        1,
        [pltpu.HBM((256, 768), BF)],
        keep(shard),
        keep(ahead),
        keep(far),
        keep(behind),
    )
    _, later = ordered(first, later)
    ahead, behind = shift(first, "x", -1), shift(first, "x", 1)
    up1, down1 = shift(later, "z", 1), shift(later, "z", -1)
    far_low, far_high = shift(behind[:256], "x", 1), shift(ahead[256:], "x", -1)
    normed_first = keep(normed_first)
    (near,) = kernel_call(
        near_scores_kernel,
        2,
        [pltpu.VMEM((length, 384), F32)],
        normed_first,
        keep(first),
        keep(ahead),
        keep(behind),
    )
    _, up1, down1 = ordered(near, up1, down1)
    up2, down2 = shift(up1, "z", 1), shift(down1, "z", -1)
    blocks = length // BLOCK
    values, gap, cum, start, passed, send = kernel_call(
        gates_kernel,
        3,
        [
            pltpu.HBM((length, HEAD), BF),
            pltpu.HBM((2, length, HEAD), F32),
            pltpu.HBM((2, length, HEAD), F32),
            pltpu.HBM((2, blocks, HEAD, HEAD), BF),
            pltpu.HBM((2, 8, HEAD), F32),
            pltpu.VMEM((2, PACK, HEAD), BF),
        ],
        keep(near),
        normed_first,
        keep(far_low),
        keep(far_high),
        retain_lower_slack,
        extra_log_shrink,
    )
    row = [send, shift(send, "x", -1), shift(send, "x", 2), shift(send, "x", 1)]
    _, up2, down2 = ordered(send, up2, down2)
    up3, down3 = shift(up2, "z", 1), shift(down2, "z", -1)
    before, send = kernel_call(
        row_kernel,
        1,
        [pltpu.HBM((2, HEAD + 8, HEAD), F32), pltpu.VMEM((8, PACK, HEAD), BF)],
        place,
        *(keep(piece) for piece in row),
        scratch=(pltpu.VMEM((4, 2, PACK, HEAD), BF),),
    )
    _, up3, down3 = ordered(send, up3, down3)
    low4, high4 = shift(up3[:128], "z", 1), shift(down3[128:], "z", -1)
    every = lax.all_to_all(send, "z", 0, 0, tiled=True)

    local, lifted, gate, conv_out, columns = kernel_call(
        later_kernel,
        0.5,
        [
            pltpu.HBM((length, HEAD), F32),
            pltpu.HBM((2, length, HEAD), BF),
            pltpu.HBM((length, HEAD), F32),
            pltpu.VMEM((length, HEAD), BF),
            pltpu.VMEM((2048, 256), BF),
        ],
        place,
        keep(normed),
        keep(edges),
        *(far_off(a) for a in (later, down1, down2, down3, low4, high4, up3, up2, up1)),
        *(far_off(a) for a in (values, gap, cum, start, passed)),
        filter_kernel_coefs,
        channel_cluster_scale[None],
        scratch=(
            pltpu.VMEM((length, HEAD), F32),
            pltpu.VMEM((length + 32, HEAD), F32),
            pltpu.VMEM((2048, 768), BF),
            pltpu.SemaphoreType.DMA((9,)),
        ),
        left=range(3, 12),
    )
    (rec_out,) = kernel_call(
        readout_kernel,
        1,
        [pltpu.VMEM((length, HEAD), BF)],
        place,
        far_off(local),
        far_off(lifted),
        keep(every),
        far_off(before),
        subspace_rescale[None],
        far_off(gate),
    )
    theirs, mine = (
        kernel_call(
            project_out_kernel,
            1,
            [pltpu.VMEM((4, 48, 2048), kind)],
            side[None].astype(jnp.int32),
            keep(rec_out),
            keep(conv_out),
            keep(columns),
        )[0]
        for side, kind in ((1 - core, BF), (core, F32))
    )
    half, whole, final = (
        pltpu.VMEM((48, 1024), BF),
        pltpu.VMEM((48, 2048), F32),
        pltpu.VMEM((48, 2048), BF),
    )
    far_low, far_high, ahead, behind, own = kernel_call(
        meet_kernel,
        1,
        [half, half, whole, whole, whole],
        place,
        keep(mine),
        keep(shift(theirs, "core", 1)),
    )
    ahead, behind = kernel_call(
        relay_kernel,
        0.5,
        [final, final],
        keep(ahead),
        keep(behind),
        keep(shift(far_low, "y", 1)),
        keep(shift(far_high, "y", -1)),
    )
    ahead, behind = shift(ahead, "y", 1), shift(behind, "y", -1)
    return (own + ahead.astype(F32) + behind.astype(F32)).astype(BF)


def solution(mesh):
    finer = Mesh(mesh.devices.reshape(8, 4, 4, 2), ("z", "x", "y", "core"))
    sp, tp = ("z", "x"), ("y", "core")
    in_specs = (
        P(sp, None),
        P(),
        *(P(sp, tp) for _ in range(7)),
        P(None, tp),
        P(None, sp, tp),
        P(),
        P(None, tp),
        P(tp),
        P(tp, sp),
        P(tp, sp),
    )
    return jax.shard_map(
        layer,
        mesh=finer,
        in_specs=in_specs,
        out_specs=P((*sp, *tp), None),
        check_vma=False,
    )
```

profile of v0, /device:TPU:1, one launch (start us, length us, event | category | flops | bytes accessed | tf_op | source)
XLA Modules:
  0.0 112.5 jit_solution(16207015742625894919)
XLA Ops:
  0.0 2.5 %shard_map.155 = (bf16[8,64,384]{2,1,0:T(8,128)(2,1)}, bf16[64,768]{1,0:T(8,128)(2,1)S(1)}, bf16[16,2048]{1,0:T(8,128)(2,1)S(1)}, bf16[16,2048]{1,0:T(8,128)(2,1)S(1)}) custom-call(bf16[384,2048]{1,0:T(8,128)(2,1)} %x.3, bf16[64,128]{1,0:T(8,128)(2,1)} %refs_0_.1, bf16[64,128]{1,0:T(8,128)(2,1)} %refs_1_.1, bf16[64,128]{1,0:T(8,128)(2,1)} %refs_2_.1, ...), custom_call_target="tpu_custom_call" | custom-call | flops 8000000 | tf_op jit(solution)/shard_map/pallas_call | solution.py:49
  2.5 9.0 %all-to-all-start = ((bf16[8,64,384]{2,1,0:T(8,128)(2,1)}), bf16[8,64,384]{2,1,0:T(8,128)(2,1)S(1)}, u32[]{:S(2)}, u32[]{:S(2)}) async-start(bf16[8,64,384]{2,1,0:T(8,128)(2,1)} %get-tuple-element.54), calls=%async_computation | async-start | bytes 786432 | tf_op jit(solution)/shard_map/all_to_all | solution.py:368
  11.5 2.5 %collective-permute-start = (bf16[64,768]{1,0:T(8,128)(2,1)S(1)}, bf16[64,768]{1,0:T(8,128)(2,1)S(1)}, u32[]{:S(2)}, u32[]{:S(2)}) collective-permute-start(bf16[64,768]{1,0:T(8,128)(2,1)S(1)} %get-tuple-element.55.own), channel_id=1, source_target_pairs={{0,24},{8,0},{16,8},{24,16},{1,25},{9,1},{17,9},{25,17},{2,26},{10... | collective-permute-start | bytes 294920 | tf_op jit(solution)/shard_map/ppermute | solution.py:27
  14.0 0.5 collective-permute-start.1
  14.5 0.6 collective-permute-start.2
  15.1 3.4 %collective-permute-start.3 = (bf16[16,2048]{1,0:T(8,128)(2,1)S(1)}, bf16[16,2048]{1,0:T(8,128)(2,1)S(1)}, u32[]{:S(2)}, u32[]{:S(2)}) collective-permute-start(bf16[16,2048]{1,0:T(8,128)(2,1)S(1)} %get-tuple-element.49), channel_id=1, source_target_pairs={{0,8},{8,16},{16,24},{24,32},{32,40},{40,48},{48,56},{56,64},{64,7... | collective-permute-start | bytes 196616 | tf_op jit(solution)/shard_map/ppermute | solution.py:33
  18.5 1.3 %collective-permute-start.4 = (bf16[16,2048]{1,0:T(8,128)(2,1)S(1)}, bf16[16,2048]{1,0:T(8,128)(2,1)S(1)}, u32[]{:S(2)}, u32[]{:S(2)}) collective-permute-start(bf16[16,2048]{1,0:T(8,128)(2,1)S(1)} %get-tuple-element.50), channel_id=1, source_target_pairs={{8,0},{16,8},{24,16},{32,24},{40,32},{48,40},{56,48},{64,56},{72,6... | collective-permute-start | bytes 196616 | tf_op jit(solution)/shard_map/ppermute | solution.py:33
  19.9 0.1 pad_add_fusion.place
  20.0 3.3 %shard_map.154 = (bf16[384,2048]{1,0:T(8,128)(2,1)S(1)}, bf16[384,2048]{1,0:T(8,128)(2,1)S(1)}) custom-call(s32[4]{0:T(128)S(1)} %pad_add_fusion.place, bf16[384,2048]{1,0:T(8,128)(2,1)} %x.3, bf16[1,2048]{1,0:T(2,128)(2,1)S(1)} %broadcast_in_dim.16.gain), custom_call_target="tpu_custom_call" | custom-call | flops 12000000 | tf_op jit(solution)/shard_map/pallas_call | solution.py:49
  23.2 1.2 %copy-done = bf16[384,2048]{1,0:T(8,128)(2,1)} copy-done((bf16[384,2048]{1,0:T(8,128)(2,1)}, bf16[384,2048]{1,0:T(8,128)(2,1)S(1)}, u32[]{:S(2)}) %copy-start) | copy-done | bytes 1572888
  24.4 0.0 collective-permute-done.3
  24.4 1.4 %all-to-all-done = bf16[8,64,384]{2,1,0:T(8,128)(2,1)S(1)} async-done(((bf16[8,64,384]{2,1,0:T(8,128)(2,1)}), bf16[8,64,384]{2,1,0:T(8,128)(2,1)S(1)}, u32[]{:S(2)}, u32[]{:S(2)}) %all-to-all-start) | async-done | bytes 393248 | tf_op jit(solution)/shard_map/all_to_all | solution.py:368
  25.8 2.5 %collective-permute-start.5 = (bf16[512,384]{1,0:T(8,128)(2,1)S(1)}, bf16[512,384]{1,0:T(8,128)(2,1)S(1)}, u32[]{:S(2)}, u32[]{:S(2)}) collective-permute-start(bf16[512,384]{1,0:T(8,128)(2,1)S(1)} %bitcast.11), channel_id=1, source_target_pairs={{0,24},{8,0},{16,8},{24,16},{1,25},{9,1},{17,9},{25,17},{2,26},{10... | collective-permute-start | bytes 1179656 | tf_op jit(solution)/shard_map/ppermute | solution.py:27
  28.3 0.0 collective-permute-done.ahead
  28.3 0.0 collective-permute-done.2.behind
  28.3 0.8 shard_map.157.refs_0_
  29.1 1.7 %collective-permute-start.7 = (bf16[256,768]{1,0:T(8,128)(2,1)}, bf16[256,768]{1,0:T(8,128)(2,1)S(1)}, u32[]{:S(2)}, u32[]{:S(2)}) collective-permute-start(bf16[256,768]{1,0:T(8,128)(2,1)} %shard_map.157.refs_0_), channel_id=1, source_target_pairs={{0,32},{32,64},{64,96},{96,128},{128,160},{160,192},{192,224},{224... | collective-permute-start | bytes 1179656 | tf_op jit(solution)/shard_map/ppermute | solution.py:27
  30.8 1.2 %collective-permute-start.8 = (bf16[256,768]{1,0:T(8,128)(2,1)}, bf16[256,768]{1,0:T(8,128)(2,1)}, u32[]{:S(2)}, u32[]{:S(2)}) collective-permute-start(bf16[256,768]{1,0:T(8,128)(2,1)} %shard_map.157.refs_0_), channel_id=1, source_target_pairs={{0,224},{32,0},{64,32},{96,64},{128,96},{160,128},{192,160},{224,1... | collective-permute-start | bytes 1179656 | tf_op jit(solution)/shard_map/ppermute | solution.py:27
  32.0 3.0 %collective-permute-done.5.ahead = bf16[512,384]{1,0:T(8,128)(2,1)S(1)} collective-permute-done((bf16[512,384]{1,0:T(8,128)(2,1)S(1)}, bf16[512,384]{1,0:T(8,128)(2,1)S(1)}, u32[]{:S(2)}, u32[]{:S(2)}) %collective-permute-start.5) | collective-permute-done | bytes 393248 | tf_op jit(solution)/shard_map/ppermute | solution.py:27
  35.1 3.1 %collective-permute-done.6.behind = bf16[512,384]{1,0:T(8,128)(2,1)S(1)} collective-permute-done((bf16[512,384]{1,0:T(8,128)(2,1)S(1)}, bf16[512,384]{1,0:T(8,128)(2,1)S(1)}, u32[]{:S(2)}, u32[]{:S(2)}) %collective-permute-start.6) | collective-permute-done | bytes 393248 | tf_op jit(solution)/shard_map/ppermute | solution.py:27
  38.1 0.8 shard_map.158.near
  38.9 0.0 collective-permute-done.7.refs_8_
  38.9 0.6 collective-permute-start.11
  39.5 2.2 %collective-permute-start.12 = (bf16[256,768]{1,0:T(8,128)(2,1)}, bf16[256,768]{1,0:T(8,128)(2,1)}, u32[]{:S(2)}, u32[]{:S(2)}) collective-permute-start(bf16[256,768]{1,0:T(8,128)(2,1)} %collective-permute-done.8.refs_1_), channel_id=1, source_target_pairs={{0,224},{32,0},{64,32},{96,64},{128,96},{160,128},{192,160},{224,1... | collective-permute-start | bytes 1179656 | tf_op jit(solution)/shard_map/ppermute | solution.py:27
  41.7 0.7 slice.17
  42.4 2.5 %collective-permute-start.10 = (bf16[256,384]{1,0:T(8,128)(2,1)}, bf16[256,384]{1,0:T(8,128)(2,1)S(1)}, u32[]{:S(2)}, u32[]{:S(2)}) collective-permute-start(bf16[256,384]{1,0:T(8,128)(2,1)} %slice.17), channel_id=1, source_target_pairs={{0,24},{8,0},{16,8},{24,16},{1,25},{9,1},{17,9},{25,17},{2,26},{10... | collective-permute-start | bytes 589832 | tf_op jit(solution)/shard_map/ppermute | solution.py:27
  44.9 0.7 slice.16
  45.6 0.2 copy.17.extra
  45.8 2.0 %collective-permute-done.10.far_high = bf16[256,384]{1,0:T(8,128)(2,1)S(1)} collective-permute-done((bf16[256,384]{1,0:T(8,128)(2,1)}, bf16[256,384]{1,0:T(8,128)(2,1)S(1)}, u32[]{:S(2)}, u32[]{:S(2)}) %collective-permute-start.10) | collective-permute-done | bytes 196640 | tf_op jit(solution)/shard_map/ppermute | solution.py:27
  47.8 3.7 %collective-permute-done.9.far_low = bf16[256,384]{1,0:T(8,128)(2,1)S(1)} collective-permute-done((bf16[256,384]{1,0:T(8,128)(2,1)}, bf16[256,384]{1,0:T(8,128)(2,1)S(1)}, u32[]{:S(2)}, u32[]{:S(2)}) %collective-permute-start.9) | collective-permute-done | bytes 196640 | tf_op jit(solution)/shard_map/ppermute | solution.py:27
  51.6 1.7 %shard_map.159 = (bf16[384,128]{1,0:T(8,128)(2,1)}, f32[2,384,128]{2,1,0:T(8,128)}, f32[2,384,128]{2,1,0:T(8,128)}, bf16[2,6,128,128]{3,2,1,0:T(8,128)(2,1)}, f3...) custom-call(f32[384,384]{1,0:T(8,128)S(1)} %shard_map.158.near, bf16[384,2048]{1,0:T(8,128)(2,1)S(1)} %get-tuple-element.60.normed, ...), custom_call_target="tpu_custom_call" | custom-call | flops 12000000 | tf_op jit(solution)/shard_map/pallas_call | solution.py:49
  53.3 0.0 copy-start.5
  53.3 0.8 collective-permute-start.16
  54.1 2.1 %collective-permute-start.17 = (bf16[256,768]{1,0:T(8,128)(2,1)}, bf16[256,768]{1,0:T(8,128)(2,1)S(1)}, u32[]{:S(2)}, u32[]{:S(2)}) collective-permute-start(bf16[256,768]{1,0:T(8,128)(2,1)} %collective-permute-done.12.refs_2_), channel_id=1, source_target_pairs={{0,224},{32,0},{64,32},{96,64},{128,96},{160,128},{192,160},{224,1... | collective-permute-start | bytes 1179656 | tf_op jit(solution)/shard_map/ppermute | solution.py:27
  56.2 1.0 collective-permute-start.14
  57.2 0.5 collective-permute-start.15
  57.7 1.7 %collective-permute-done.13.ahead = bf16[2,144,128]{2,1,0:T(8,128)(2,1)S(1)} collective-permute-done((bf16[2,144,128]{2,1,0:T(8,128)(2,1)S(1)}, bf16[2,144,128]{2,1,0:T(8,128)(2,1)S(1)}, u32[]{:S(2)}, u32[]{:S(2)}) %collective-permute-start.13) | collective-permute-done | bytes 73760 | tf_op jit(solution)/shard_map/ppermute | solution.py:27
  59.4 1.5 %collective-permute-done.14.far = bf16[2,144,128]{2,1,0:T(8,128)(2,1)S(1)} collective-permute-done((bf16[2,144,128]{2,1,0:T(8,128)(2,1)S(1)}, bf16[2,144,128]{2,1,0:T(8,128)(2,1)S(1)}, u32[]{:S(2)}, u32[]{:S(2)}) %collective-permute-start.14) | collective-permute-done | bytes 73760 | tf_op jit(solution)/shard_map/ppermute | solution.py:27
  60.9 0.9 collective-permute-done.15.behind
  61.8 1.4 %shard_map.160 = (f32[2,136,128]{2,1,0:T(8,128)}, bf16[8,144,128]{2,1,0:T(8,128)(2,1)}) custom-call(s32[4]{0:T(128)S(1)} %pad_add_fusion.place, bf16[2,144,128]{2,1,0:T(8,128)(2,1)S(1)} %get-tuple-element.62.own, bf16[2,144,128]{2,1,0:T(8,128)(2,1)S(1)} %collective-permute-done.13.ahead, bf16[2,144,128]{2,1,0:T(8,128)(2,1)S(1)} %collective-permute-done.14.far, ...), custom_call_target="tpu_custom_call" | custom-call | flops 4000000 | tf_op jit(solution)/shard_map/pallas_call | solution.py:49
  63.2 6.6 %all-to-all-start.1 = ((bf16[8,144,128]{2,1,0:T(8,128)(2,1)}), bf16[8,144,128]{2,1,0:T(8,128)(2,1)S(1)}, u32[]{:S(2)}, u32[]{:S(2)}) async-start(bf16[8,144,128]{2,1,0:T(8,128)(2,1)} %get-tuple-element.65), calls=%async_computation.1 | async-start | bytes 589824 | tf_op jit(solution)/shard_map/all_to_all | solution.py:433
  69.8 0.0 collective-permute-done.17.refs_3_
  69.9 1.5 %collective-permute-start.18 = (bf16[128,768]{1,0:T(8,128)(2,1)S(1)}, bf16[128,768]{1,0:T(8,128)(2,1)S(1)}, u32[]{:S(2)}, u32[]{:S(2)}) collective-permute-start(bf16[128,768]{1,0:T(8,128)(2,1)S(1)} %slice.14), channel_id=1, source_target_pairs={{0,32},{32,64},{64,96},{96,128},{128,160},{160,192},{192,224},{224... | collective-permute-start | bytes 589832 | tf_op jit(solution)/shard_map/ppermute | solution.py:27
  71.4 1.3 %collective-permute-start.19 = (bf16[128,768]{1,0:T(8,128)(2,1)S(1)}, bf16[128,768]{1,0:T(8,128)(2,1)S(1)}, u32[]{:S(2)}, u32[]{:S(2)}) collective-permute-start(bf16[128,768]{1,0:T(8,128)(2,1)S(1)} %slice.15), channel_id=1, source_target_pairs={{0,224},{32,0},{64,32},{96,64},{128,96},{160,128},{192,160},{224,1... | collective-permute-start | bytes 589832 | tf_op jit(solution)/shard_map/ppermute | solution.py:27
  72.7 0.8 shard_map.156.edges
  73.5 5.0 %collective-permute-done.18.refs_4_ = bf16[128,768]{1,0:T(8,128)(2,1)S(1)} collective-permute-done((bf16[128,768]{1,0:T(8,128)(2,1)S(1)}, bf16[128,768]{1,0:T(8,128)(2,1)S(1)}, u32[]{:S(2)}, u32[]{:S(2)}) %collective-permute-start.18) | collective-permute-done | bytes 196640 | tf_op jit(solution)/shard_map/ppermute | solution.py:27
  78.5 0.7 copy-done.9
  79.2 0.1 copy-done.10
  79.3 7.0 %shard_map.161 = (f32[384,128]{1,0:T(8,128)}, bf16[2,384,128]{2,1,0:T(8,128)(2,1)}, f32[384,128]{1,0:T(8,128)}, bf16[384,128]{1,0:T(8,128)(2,1)S(1)}, bf16[2048,256]{1,0:T(8,128)(2,1)S(1)}) custom-call(s32[4]{0:T(128)S(1)} %pad_add_fusion.place, bf16[384,2048]{1,0:T(8,128)(2,1)S(1)} %copy-done.1, bf16[32,2048]{1,0:T(8,128)(2,1)S(1)} %shard_map.156.edges, ...), custom_call_target="tpu_custom_call" | custom-call | flops 2000000 | tf_op jit(solution)/shard_map/pallas_call | solution.py:49
  86.3 1.6 %shard_map.162.rec = bf16[384,128]{1,0:T(8,128)(2,1)S(1)} custom-call(s32[4]{0:T(128)S(1)} %pad_add_fusion.place, f32[384,128]{1,0:T(8,128)} %get-tuple-element.74.local, bf16[2,384,128]{2,1,0:T(8,128)(2,1)} %get-tuple-element.75.lifted, bf16[8,144,128]{2,1,0:T(8,128)(2,1)S(1)} %all-to-all-done.1.every, f32[2,136,128]{2,1,0:T(8,128)} %get-tuple-element.76.before, ...), custom_call_target="tpu_custom_call" | custom-call | flops 4000000 | tf_op jit(solution)/shard_map/pallas_call | solution.py:49
  87.9 0.5 shard_map.164
  88.4 8.9 %collective-permute-start.20 = (bf16[4,48,2048]{2,1,0:T(8,128)(2,1)S(1)}, bf16[4,48,2048]{2,1,0:T(8,128)(2,1)S(1)}, u32[]{:S(2)}, u32[]{:S(2)}) collective-permute-start(bf16[4,48,2048]{2,1,0:T(8,128)(2,1)S(1)} %shard_map.164), channel_id=1, source_target_pairs={{0,1},{1,0},{2,3},{3,2},{4,5},{5,4},{6,7},{7,6},{8,9},{9,8},{10,11... | collective-permute-start | bytes 2359304 | tf_op jit(solution)/shard_map/ppermute | solution.py:27
  97.3 0.5 shard_map.163.mine
  97.8 1.4 %collective-permute-done.20.got = bf16[4,48,2048]{2,1,0:T(8,128)(2,1)S(1)} collective-permute-done((bf16[4,48,2048]{2,1,0:T(8,128)(2,1)S(1)}, bf16[4,48,2048]{2,1,0:T(8,128)(2,1)S(1)}, u32[]{:S(2)}, u32[]{:S(2)}) %collective-permute-start.20) | collective-permute-done | bytes 786464 | tf_op jit(solution)/shard_map/ppermute | solution.py:27
  99.2 0.7 shard_map.165
  99.9 1.4 %collective-permute-start.21 = (bf16[48,1024]{1,0:T(8,128)(2,1)S(1)}, bf16[48,1024]{1,0:T(8,128)(2,1)S(1)}, u32[]{:S(2)}, u32[]{:S(2)}) collective-permute-start(bf16[48,1024]{1,0:T(8,128)(2,1)S(1)} %get-tuple-element.83), channel_id=1, source_target_pairs={{0,2},{2,4},{4,6},{6,0},{1,3},{3,5},{5,7},{7,1},{8,10},{10,12},{12... | collective-permute-start | bytes 294920 | tf_op jit(solution)/shard_map/ppermute | solution.py:27
  101.3 1.5 %collective-permute-start.22 = (bf16[48,1024]{1,0:T(8,128)(2,1)S(1)}, bf16[48,1024]{1,0:T(8,128)(2,1)S(1)}, u32[]{:S(2)}, u32[]{:S(2)}) collective-permute-start(bf16[48,1024]{1,0:T(8,128)(2,1)S(1)} %get-tuple-element.84), channel_id=1, source_target_pairs={{0,6},{2,0},{4,2},{6,4},{1,7},{3,1},{5,3},{7,5},{8,14},{10,8},{12,... | collective-permute-start | bytes 294920 | tf_op jit(solution)/shard_map/ppermute | solution.py:27
  102.8 2.5 %collective-permute-done.21.low = bf16[48,1024]{1,0:T(8,128)(2,1)S(1)} collective-permute-done((bf16[48,1024]{1,0:T(8,128)(2,1)S(1)}, bf16[48,1024]{1,0:T(8,128)(2,1)S(1)}, u32[]{:S(2)}, u32[]{:S(2)}) %collective-permute-start.21) | collective-permute-done | bytes 98336 | tf_op jit(solution)/shard_map/ppermute | solution.py:27
  105.3 0.1 shard_map.166
  105.3 0.9 collective-permute-start.23
  106.2 1.9 %collective-permute-start.24 = (bf16[48,2048]{1,0:T(8,128)(2,1)S(1)}, bf16[48,2048]{1,0:T(8,128)(2,1)S(1)}, u32[]{:S(2)}, u32[]{:S(2)}) collective-permute-start(bf16[48,2048]{1,0:T(8,128)(2,1)S(1)} %get-tuple-element.86), channel_id=1, source_target_pairs={{0,6},{2,0},{4,2},{6,4},{1,7},{3,1},{5,3},{7,5},{8,14},{10,8},{12,... | collective-permute-start | bytes 589832 | tf_op jit(solution)/shard_map/ppermute | solution.py:27
  108.1 3.7 %collective-permute-done.23 = bf16[48,2048]{1,0:T(8,128)(2,1)S(1)} collective-permute-done((bf16[48,2048]{1,0:T(8,128)(2,1)S(1)}, bf16[48,2048]{1,0:T(8,128)(2,1)S(1)}, u32[]{:S(2)}, u32[]{:S(2)}) %collective-permute-start.23) | collective-permute-done | bytes 196640 | tf_op jit(solution)/shard_map/ppermute | solution.py:27
  111.8 0.0 collective-permute-done.24
  111.8 0.7 add_convert_fusion
  (42 shorter events, 0.1 us)
Async XLA Ops:
  0.0 19.9 %copy-start.13 = (bf16[2048]{0:T(1024)(128)(2,1)S(1)}, bf16[2048]{0:T(1024)(128)(2,1)}, u32[]{:S(2)}) copy-start(bf16[2048]{0:T(1024)(128)(2,1)} %param.17) | copy-start | bytes 12292
  2.5 23.3 %all-to-all-start = ((bf16[8,64,384]{2,1,0:T(8,128)(2,1)}), bf16[8,64,384]{2,1,0:T(8,128)(2,1)S(1)}, u32[]{:S(2)}, u32[]{:S(2)}) async-start(bf16[8,64,384]{2,1,0:T(8,128)(2,1)} %get-tuple-element.54), calls=%async_computation | async-start | bytes 786432 | tf_op jit(solution)/shard_map/all_to_all | solution.py:368
  11.5 16.8 %collective-permute-start = (bf16[64,768]{1,0:T(8,128)(2,1)S(1)}, bf16[64,768]{1,0:T(8,128)(2,1)S(1)}, u32[]{:S(2)}, u32[]{:S(2)}) collective-permute-start(bf16[64,768]{1,0:T(8,128)(2,1)S(1)} %get-tuple-element.55.own), channel_id=1, source_target_pairs={{0,24},{8,0},{16,8},{24,16},{1,25},{9,1},{17,9},{25,17},{2,26},{10... | collective-permute-start | bytes 294920 | tf_op jit(solution)/shard_map/ppermute | solution.py:27
  14.0 14.3 %collective-permute-start.1 = (bf16[64,768]{1,0:T(8,128)(2,1)S(1)}, bf16[64,768]{1,0:T(8,128)(2,1)S(1)}, u32[]{:S(2)}, u32[]{:S(2)}) collective-permute-start(bf16[64,768]{1,0:T(8,128)(2,1)S(1)} %get-tuple-element.55.own), channel_id=1, source_target_pairs={{0,16},{8,24},{16,0},{24,8},{1,17},{9,25},{17,1},{25,9},{2,18},{10... | collective-permute-start | bytes 294920 | tf_op jit(solution)/shard_map/ppermute | solution.py:27
  14.5 13.8 %collective-permute-start.2 = (bf16[64,768]{1,0:T(8,128)(2,1)S(1)}, bf16[64,768]{1,0:T(8,128)(2,1)S(1)}, u32[]{:S(2)}, u32[]{:S(2)}) collective-permute-start(bf16[64,768]{1,0:T(8,128)(2,1)S(1)} %get-tuple-element.55.own), channel_id=1, source_target_pairs={{0,8},{8,16},{16,24},{24,0},{1,9},{9,17},{17,25},{25,1},{2,10},{10... | collective-permute-start | bytes 294920 | tf_op jit(solution)/shard_map/ppermute | solution.py:27
  15.1 9.3 %collective-permute-start.3 = (bf16[16,2048]{1,0:T(8,128)(2,1)S(1)}, bf16[16,2048]{1,0:T(8,128)(2,1)S(1)}, u32[]{:S(2)}, u32[]{:S(2)}) collective-permute-start(bf16[16,2048]{1,0:T(8,128)(2,1)S(1)} %get-tuple-element.49), channel_id=1, source_target_pairs={{0,8},{8,16},{16,24},{24,32},{32,40},{40,48},{48,56},{56,64},{64,7... | collective-permute-start | bytes 196616 | tf_op jit(solution)/shard_map/ppermute | solution.py:33
  18.5 9.7 %collective-permute-start.4 = (bf16[16,2048]{1,0:T(8,128)(2,1)S(1)}, bf16[16,2048]{1,0:T(8,128)(2,1)S(1)}, u32[]{:S(2)}, u32[]{:S(2)}) collective-permute-start(bf16[16,2048]{1,0:T(8,128)(2,1)S(1)} %get-tuple-element.50), channel_id=1, source_target_pairs={{8,0},{16,8},{24,16},{32,24},{40,32},{48,40},{56,48},{64,56},{72,6... | collective-permute-start | bytes 196616 | tf_op jit(solution)/shard_map/ppermute | solution.py:33
  23.2 1.2 %copy-start = (bf16[384,2048]{1,0:T(8,128)(2,1)}, bf16[384,2048]{1,0:T(8,128)(2,1)S(1)}, u32[]{:S(2)}) copy-start(bf16[384,2048]{1,0:T(8,128)(2,1)S(1)} %get-tuple-element.51.normed) | copy-start | bytes 4718596
  25.8 9.3 %collective-permute-start.5 = (bf16[512,384]{1,0:T(8,128)(2,1)S(1)}, bf16[512,384]{1,0:T(8,128)(2,1)S(1)}, u32[]{:S(2)}, u32[]{:S(2)}) collective-permute-start(bf16[512,384]{1,0:T(8,128)(2,1)S(1)} %bitcast.11), channel_id=1, source_target_pairs={{0,24},{8,0},{16,8},{24,16},{1,25},{9,1},{17,9},{25,17},{2,26},{10... | collective-permute-start | bytes 1179656 | tf_op jit(solution)/shard_map/ppermute | solution.py:27
  28.3 6.8 %copy-start.11 = (bf16[16,2048]{1,0:T(8,128)(2,1)}, bf16[16,2048]{1,0:T(8,128)(2,1)S(1)}, u32[]{:S(2)}) copy-start(bf16[16,2048]{1,0:T(8,128)(2,1)S(1)} %collective-permute-done.4) | copy-start | bytes 196612
  28.3 9.9 %collective-permute-start.6 = (bf16[512,384]{1,0:T(8,128)(2,1)S(1)}, bf16[512,384]{1,0:T(8,128)(2,1)S(1)}, u32[]{:S(2)}, u32[]{:S(2)}) collective-permute-start(bf16[512,384]{1,0:T(8,128)(2,1)S(1)} %bitcast.12), channel_id=1, source_target_pairs={{0,8},{8,16},{16,24},{24,0},{1,9},{9,17},{17,25},{25,1},{2,10},{10... | collective-permute-start | bytes 1179656 | tf_op jit(solution)/shard_map/ppermute | solution.py:27
  29.1 16.5 %copy-start.14 = (f32[2,384,1]{1,2,0:T(1,128)S(1)}, f32[2,384,1]{1,2,0:T(1,128)}, u32[]{:S(2)}) copy-start(f32[2,384,1]{1,2,0:T(1,128)} %param.26) | copy-start | bytes 9220
  29.1 22.5 %copy-start.3 = (f32[2,128]{1,0:T(2,128)S(1)}, f32[2,128]{1,0:T(2,128)}, u32[]{:S(2)}) copy-start(f32[2,128]{1,0:T(2,128)} %slack.1) | copy-start | bytes 3076
  29.1 9.8 %collective-permute-start.7 = (bf16[256,768]{1,0:T(8,128)(2,1)}, bf16[256,768]{1,0:T(8,128)(2,1)S(1)}, u32[]{:S(2)}, u32[]{:S(2)}) collective-permute-start(bf16[256,768]{1,0:T(8,128)(2,1)} %shard_map.157.refs_0_), channel_id=1, source_target_pairs={{0,32},{32,64},{64,96},{96,128},{128,160},{160,192},{192,224},{224... | collective-permute-start | bytes 1179656 | tf_op jit(solution)/shard_map/ppermute | solution.py:27
  30.8 8.1 %collective-permute-start.8 = (bf16[256,768]{1,0:T(8,128)(2,1)}, bf16[256,768]{1,0:T(8,128)(2,1)}, u32[]{:S(2)}, u32[]{:S(2)}) collective-permute-start(bf16[256,768]{1,0:T(8,128)(2,1)} %shard_map.157.refs_0_), channel_id=1, source_target_pairs={{0,224},{32,0},{64,32},{96,64},{128,96},{160,128},{192,160},{224,1... | collective-permute-start | bytes 1179656 | tf_op jit(solution)/shard_map/ppermute | solution.py:27
  38.9 14.3 %copy-start.8 = (bf16[256,768]{1,0:T(8,128)(2,1)}, bf16[256,768]{1,0:T(8,128)(2,1)S(1)}, u32[]{:S(2)}) copy-start(bf16[256,768]{1,0:T(8,128)(2,1)S(1)} %collective-permute-done.7.refs_8_) | copy-start | bytes 1179652
  38.9 14.3 %collective-permute-start.11 = (bf16[256,768]{1,0:T(8,128)(2,1)S(1)}, bf16[256,768]{1,0:T(8,128)(2,1)}, u32[]{:S(2)}, u32[]{:S(2)}) collective-permute-start(bf16[256,768]{1,0:T(8,128)(2,1)S(1)} %collective-permute-done.7.refs_8_), channel_id=1, source_target_pairs={{0,32},{32,64},{64,96},{96,128},{128,160},{160,192},{192,224},{224... | collective-permute-start | bytes 1179656 | tf_op jit(solution)/shard_map/ppermute | solution.py:27
  39.5 13.8 %collective-permute-start.12 = (bf16[256,768]{1,0:T(8,128)(2,1)}, bf16[256,768]{1,0:T(8,128)(2,1)}, u32[]{:S(2)}, u32[]{:S(2)}) collective-permute-start(bf16[256,768]{1,0:T(8,128)(2,1)} %collective-permute-done.8.refs_1_), channel_id=1, source_target_pairs={{0,224},{32,0},{64,32},{96,64},{128,96},{160,128},{192,160},{224,1... | collective-permute-start | bytes 1179656 | tf_op jit(solution)/shard_map/ppermute | solution.py:27
  42.4 5.4 %collective-permute-start.10 = (bf16[256,384]{1,0:T(8,128)(2,1)}, bf16[256,384]{1,0:T(8,128)(2,1)S(1)}, u32[]{:S(2)}, u32[]{:S(2)}) collective-permute-start(bf16[256,384]{1,0:T(8,128)(2,1)} %slice.17), channel_id=1, source_target_pairs={{0,24},{8,0},{16,8},{24,16},{1,25},{9,1},{17,9},{25,17},{2,26},{10... | collective-permute-start | bytes 589832 | tf_op jit(solution)/shard_map/ppermute | solution.py:27
  45.6 5.9 %collective-permute-start.9 = (bf16[256,384]{1,0:T(8,128)(2,1)}, bf16[256,384]{1,0:T(8,128)(2,1)S(1)}, u32[]{:S(2)}, u32[]{:S(2)}) collective-permute-start(bf16[256,384]{1,0:T(8,128)(2,1)} %slice.16), channel_id=1, source_target_pairs={{0,8},{8,16},{16,24},{24,0},{1,9},{9,17},{17,25},{25,1},{2,10},{10... | collective-permute-start | bytes 589832 | tf_op jit(solution)/shard_map/ppermute | solution.py:27
  53.2 19.5 %copy-start.12 = (bf16[16,2048]{1,0:T(8,128)(2,1)S(1)}, bf16[16,2048]{1,0:T(8,128)(2,1)}, u32[]{:S(2)}) copy-start(bf16[16,2048]{1,0:T(8,128)(2,1)} %copy-done.11) | copy-start | bytes 196612
  53.2 26.0 %copy-start.1 = (bf16[384,2048]{1,0:T(8,128)(2,1)S(1)}, bf16[384,2048]{1,0:T(8,128)(2,1)}, u32[]{:S(2)}) copy-start(bf16[384,2048]{1,0:T(8,128)(2,1)} %copy-done) | copy-start | bytes 4718596
  53.2 26.0 %copy-start.2 = (bf16[31,128]{1,0:T(8,128)(2,1)S(1)}, bf16[31,128]{1,0:T(8,128)(2,1)}, u32[]{:S(2)}) copy-start(bf16[31,128]{1,0:T(8,128)(2,1)} %refs_14_.1) | copy-start | bytes 23812
  53.3 26.0 %copy-start.5 = (bf16[128]{0:T(256)(128)(2,1)S(1)}, bf16[128]{0:T(256)(128)(2,1)}, u32[]{:S(2)}) copy-start(bf16[128]{0:T(256)(128)(2,1)} %param.29) | copy-start | bytes 772
  53.3 16.5 %collective-permute-start.16 = (bf16[256,768]{1,0:T(8,128)(2,1)}, bf16[256,768]{1,0:T(8,128)(2,1)S(1)}, u32[]{:S(2)}, u32[]{:S(2)}) collective-permute-start(bf16[256,768]{1,0:T(8,128)(2,1)} %collective-permute-done.11.refs_7_), channel_id=1, source_target_pairs={{0,32},{32,64},{64,96},{96,128},{128,160},{160,192},{192,224},{224... | collective-permute-start | bytes 1179656 | tf_op jit(solution)/shard_map/ppermute | solution.py:27
  54.1 15.8 %collective-permute-start.17 = (bf16[256,768]{1,0:T(8,128)(2,1)}, bf16[256,768]{1,0:T(8,128)(2,1)S(1)}, u32[]{:S(2)}, u32[]{:S(2)}) collective-permute-start(bf16[256,768]{1,0:T(8,128)(2,1)} %collective-permute-done.12.refs_2_), channel_id=1, source_target_pairs={{0,224},{32,0},{64,32},{96,64},{128,96},{160,128},{192,160},{224,1... | collective-permute-start | bytes 1179656 | tf_op jit(solution)/shard_map/ppermute | solution.py:27
  56.2 3.2 %collective-permute-start.13 = (bf16[2,144,128]{2,1,0:T(8,128)(2,1)S(1)}, bf16[2,144,128]{2,1,0:T(8,128)(2,1)S(1)}, u32[]{:S(2)}, u32[]{:S(2)}) collective-permute-start(bf16[2,144,128]{2,1,0:T(8,128)(2,1)S(1)} %get-tuple-element.62.own), channel_id=1, source_target_pairs={{0,24},{8,0},{16,8},{24,16},{1,25},{9,1},{17,9},{25,17},{2,26},{10... | collective-permute-start | bytes 221192 | tf_op jit(solution)/shard_map/ppermute | solution.py:27
  56.2 4.7 %collective-permute-start.14 = (bf16[2,144,128]{2,1,0:T(8,128)(2,1)S(1)}, bf16[2,144,128]{2,1,0:T(8,128)(2,1)S(1)}, u32[]{:S(2)}, u32[]{:S(2)}) collective-permute-start(bf16[2,144,128]{2,1,0:T(8,128)(2,1)S(1)} %get-tuple-element.62.own), channel_id=1, source_target_pairs={{0,16},{8,24},{16,0},{24,8},{1,17},{9,25},{17,1},{25,9},{2,18},{10... | collective-permute-start | bytes 221192 | tf_op jit(solution)/shard_map/ppermute | solution.py:27
  57.2 4.6 %collective-permute-start.15 = (bf16[2,144,128]{2,1,0:T(8,128)(2,1)S(1)}, bf16[2,144,128]{2,1,0:T(8,128)(2,1)S(1)}, u32[]{:S(2)}, u32[]{:S(2)}) collective-permute-start(bf16[2,144,128]{2,1,0:T(8,128)(2,1)S(1)} %get-tuple-element.62.own), channel_id=1, source_target_pairs={{0,8},{8,16},{16,24},{24,0},{1,9},{9,17},{17,25},{25,1},{2,10},{10... | collective-permute-start | bytes 221192 | tf_op jit(solution)/shard_map/ppermute | solution.py:27
  63.2 23.0 %all-to-all-start.1 = ((bf16[8,144,128]{2,1,0:T(8,128)(2,1)}), bf16[8,144,128]{2,1,0:T(8,128)(2,1)S(1)}, u32[]{:S(2)}, u32[]{:S(2)}) async-start(bf16[8,144,128]{2,1,0:T(8,128)(2,1)} %get-tuple-element.65), calls=%async_computation.1 | async-start | bytes 589824 | tf_op jit(solution)/shard_map/all_to_all | solution.py:433
  69.8 8.7 %copy-start.6 = (bf16[256,768]{1,0:T(8,128)(2,1)}, bf16[256,768]{1,0:T(8,128)(2,1)S(1)}, u32[]{:S(2)}) copy-start(bf16[256,768]{1,0:T(8,128)(2,1)S(1)} %collective-permute-done.16.refs_6_) | copy-start | bytes 1179652
  69.8 8.7 %copy-start.7 = (bf16[256,768]{1,0:T(8,128)(2,1)}, bf16[256,768]{1,0:T(8,128)(2,1)S(1)}, u32[]{:S(2)}) copy-start(bf16[256,768]{1,0:T(8,128)(2,1)S(1)} %collective-permute-done.17.refs_3_) | copy-start | bytes 1179652
  69.9 8.6 %collective-permute-start.18 = (bf16[128,768]{1,0:T(8,128)(2,1)S(1)}, bf16[128,768]{1,0:T(8,128)(2,1)S(1)}, u32[]{:S(2)}, u32[]{:S(2)}) collective-permute-start(bf16[128,768]{1,0:T(8,128)(2,1)S(1)} %slice.14), channel_id=1, source_target_pairs={{0,32},{32,64},{64,96},{96,128},{128,160},{160,192},{192,224},{224... | collective-permute-start | bytes 589832 | tf_op jit(solution)/shard_map/ppermute | solution.py:27
  71.4 7.1 %collective-permute-start.19 = (bf16[128,768]{1,0:T(8,128)(2,1)S(1)}, bf16[128,768]{1,0:T(8,128)(2,1)S(1)}, u32[]{:S(2)}, u32[]{:S(2)}) collective-permute-start(bf16[128,768]{1,0:T(8,128)(2,1)S(1)} %slice.15), channel_id=1, source_target_pairs={{0,224},{32,0},{64,32},{96,64},{128,96},{160,128},{192,160},{224,1... | collective-permute-start | bytes 589832 | tf_op jit(solution)/shard_map/ppermute | solution.py:27
  78.5 0.7 copy-start.9
  78.5 0.7 copy-start.10
  79.3 7.0 %copy-start.4 = (bf16[128]{0:T(256)(128)(2,1)S(1)}, bf16[128]{0:T(256)(128)(2,1)}, u32[]{:S(2)}) copy-start(bf16[128]{0:T(256)(128)(2,1)} %param.27) | copy-start | bytes 772
  88.4 10.8 %collective-permute-start.20 = (bf16[4,48,2048]{2,1,0:T(8,128)(2,1)S(1)}, bf16[4,48,2048]{2,1,0:T(8,128)(2,1)S(1)}, u32[]{:S(2)}, u32[]{:S(2)}) collective-permute-start(bf16[4,48,2048]{2,1,0:T(8,128)(2,1)S(1)} %shard_map.164), channel_id=1, source_target_pairs={{0,1},{1,0},{2,3},{3,2},{4,5},{5,4},{6,7},{7,6},{8,9},{9,8},{10,11... | collective-permute-start | bytes 2359304 | tf_op jit(solution)/shard_map/ppermute | solution.py:27
  99.9 5.4 %collective-permute-start.21 = (bf16[48,1024]{1,0:T(8,128)(2,1)S(1)}, bf16[48,1024]{1,0:T(8,128)(2,1)S(1)}, u32[]{:S(2)}, u32[]{:S(2)}) collective-permute-start(bf16[48,1024]{1,0:T(8,128)(2,1)S(1)} %get-tuple-element.83), channel_id=1, source_target_pairs={{0,2},{2,4},{4,6},{6,0},{1,3},{3,5},{5,7},{7,1},{8,10},{10,12},{12... | collective-permute-start | bytes 294920 | tf_op jit(solution)/shard_map/ppermute | solution.py:27
  101.3 4.0 %collective-permute-start.22 = (bf16[48,1024]{1,0:T(8,128)(2,1)S(1)}, bf16[48,1024]{1,0:T(8,128)(2,1)S(1)}, u32[]{:S(2)}, u32[]{:S(2)}) collective-permute-start(bf16[48,1024]{1,0:T(8,128)(2,1)S(1)} %get-tuple-element.84), channel_id=1, source_target_pairs={{0,6},{2,0},{4,2},{6,4},{1,7},{3,1},{5,3},{7,5},{8,14},{10,8},{12,... | collective-permute-start | bytes 294920 | tf_op jit(solution)/shard_map/ppermute | solution.py:27
  105.3 6.5 %collective-permute-start.23 = (bf16[48,2048]{1,0:T(8,128)(2,1)S(1)}, bf16[48,2048]{1,0:T(8,128)(2,1)S(1)}, u32[]{:S(2)}, u32[]{:S(2)}) collective-permute-start(bf16[48,2048]{1,0:T(8,128)(2,1)S(1)} %get-tuple-element.85), channel_id=1, source_target_pairs={{0,2},{2,4},{4,6},{6,0},{1,3},{3,5},{5,7},{7,1},{8,10},{10,12},{12... | collective-permute-start | bytes 589832 | tf_op jit(solution)/shard_map/ppermute | solution.py:27
  106.2 5.6 %collective-permute-start.24 = (bf16[48,2048]{1,0:T(8,128)(2,1)S(1)}, bf16[48,2048]{1,0:T(8,128)(2,1)S(1)}, u32[]{:S(2)}, u32[]{:S(2)}) collective-permute-start(bf16[48,2048]{1,0:T(8,128)(2,1)S(1)} %get-tuple-element.86), channel_id=1, source_target_pairs={{0,6},{2,0},{4,2},{6,4},{1,7},{3,1},{5,3},{7,5},{8,14},{10,8},{12,... | collective-permute-start | bytes 589832 | tf_op jit(solution)/shard_map/ppermute | solution.py:27
where the time goes:
time: 114 us; the launch traced here: 113 us
  starting transfers between devices  56.4 us (49%)
  waiting for transfers between devices  30 us (26%)
  Pallas kernels  21.5 us (19%)
  local copies, waits for them, and re-layouts  3.55 us (3%)
    ppermute x23, starting transfers between devices, shift(): return lax.ppermute(array, axis, ring(lax.axis_size(axis), step))  36.1 us
    ppermute x23, waiting for transfers between devices, shift(): return lax.ppermute(array, axis, ring(lax.axis_size(axis), step))  28.6 us
    pallas_call x13, Pallas kernels, kernel_call(): pl.pallas_call(body, out_shape=tuple(outs), in_specs=[SMEM if o.dtype ==...  21.5 us
    all_to_all x1, starting transfers between devices, layer(): first = lax.all_to_all(first, 'z', 0, 0, tiled=True).reshape(512, 384)  9.02 us
    all_to_all x1, starting transfers between devices, layer(): every = lax.all_to_all(send, 'z', 0, 0, tiled=True)  6.57 us
    ppermute x2, starting transfers between devices, line(): return lax.ppermute(array, axes, pairs)  4.71 us
  transfers between devices with their start and end apart: 27, of which 12 were waited for; matrix products, arithmetic and copies ran while one was open for 2% of the time, Pallas kernels for 14%

commit v1 on v0

--- a/solution.py
+++ b/solution.py
@@ -121,7 +121,9 @@
 
 
 def normalized(place, x, gain, count):
-    outs = [pltpu.VMEM(x.shape, BF)] * count
+    outs = [pltpu.VMEM(x.shape, BF), pltpu.VMEM(x.shape, BF)][:count]
+    if count == 2:
+        outs[0] = pltpu.HBM(x.shape, BF)
     return kernel_call(normalize_kernel, 3, outs, place, x, gain)
 
 
@@ -202,32 +204,89 @@
         send[k] = jnp.where(k > z, messages[0], messages[1])
 
 
-def later_kernel(place, normed, edges, *refs):
-    pieces = refs[:9]
-    values, gap, cum, start, passed, taps, scale = refs[9:16]
-    local_o, lifted_o, gate_o, conv_o, columns_o, query, glu, weights, done = refs[16:]
-    x, z_here = place[2], place[0]
+def spread(place, pieces, steps):
+    z = place[0]
+    found = []
+    for piece, (step, inside) in zip(pieces, steps):
+        at = pl.multiple_of(lax.rem(z + step, 8) * 256 + inside, 128)
+        found.append((piece, at, piece.shape[0]))
+    return found
+
+
+NEAR_STEPS = ((0, 0), (1, 0), (2, 0), (6, 0), (7, 0))
+FAR_STEPS = ((3, 0), (4, 0), (4, 128), (5, 0))
+
+
+def early_kernel(place, normed, edges, *refs):
+    pieces = refs[:5]
+    gap, cum = refs[5:7]
+    scores_o, edge_o, lowered_o, grown_o, held, done = refs[7:]
     copies = []
     for k, piece in enumerate(pieces):
-        step, inside = (k, 0) if k < 5 else (k - 1, 128 if k == 5 else 0)
-        to = pl.multiple_of(lax.rem(z_here + step, 8) * 256 + inside, 128)
-        into = weights.at[pl.ds(to, piece.shape[0])]
-        copies.append(pltpu.make_async_copy(piece, into, done.at[k]))
+        copies.append(pltpu.make_async_copy(piece.at[:, :512], held.at[k], done.at[k]))
         copies[-1].start()
+    for d in range(2):
+        grown = jnp.exp(cum[d])
+        grown_o[d] = grown
+        lowered_o[d] = (gap[d] * jnp.exp(-cum[d])).astype(BF)
     for copy in copies:
         copy.wait()
+    total, edge = None, None
+    for k, (piece, at, count) in enumerate(spread(place, pieces, NEAR_STEPS)):
+        part = dot(normed[:, pl.ds(at, count)], held[k])
+        total = part if total is None else total + part
+        part = dot(edges[:, pl.ds(at, count)], held[k, :, 256:])
+        edge = part if edge is None else edge + part
+    scores_o[...] = total
+    edge_o[...] = edge
+
+
+def later_kernel(place, normed, edges, scores, edge_scores, *refs):
+    near, far = refs[:5], refs[5:9]
+    values, lowered, grown, start, passed, taps, scale = refs[9:16]
+    local_o, lifted_o, gate_o, conv_o, columns_o, query, glu, held, done, placed = refs[16:]
+    x = place[2]
     length = normed.shape[0]
     blocks = length // BLOCK
-    pre = dot(normed[...], weights[:, :256])
+    copies = []
+    spots = spread(place, far, FAR_STEPS)
+    at = 0
+    for k, (piece, _, count) in enumerate(spots):
+        into = held.at[at : at + count]
+        copies.append(pltpu.make_async_copy(piece.at[:, :512], into, done.at[k]))
+        copies[-1].start()
+        at += count
+    moves = []
+    for piece, feature, count in spread(place, near + far, NEAR_STEPS + FAR_STEPS):
+        base = lax.div(feature, 256) * 256
+        first = 2 if piece is far[2] else 0
+        for k in range(count // 64):
+            to = pl.multiple_of(base + lax.rem(x + first + k, 4) * 64, 64)
+            source = piece.at[k * 64 : (k + 1) * 64, 512:768]
+            moves.append(
+                pltpu.make_async_copy(source, columns_o.at[pl.ds(to, 64)], placed.at[len(moves)])
+            )
+            moves[-1].start()
+    for copy in copies:
+        copy.wait()
+
+    def finished(rows, before, columns):
+        total, at = before, 0
+        for _, feature, count in spots:
+            total = total + dot(rows[:, pl.ds(feature, count)], held[at : at + count, columns])
+            at += count
+        return total
+
+    pre = finished(normed, scores[:, :256], slice(0, 256))
     query[...] = pre[:, :HEAD] * jax.nn.sigmoid(pre[:, :HEAD])
     gate_o[...] = pre[:, HEAD:] * jax.nn.sigmoid(pre[:, HEAD:])
 
-    def gated(rows):
-        pair = dot(rows, weights[:, 256:512])
+    def gated(rows, before):
+        pair = finished(rows, before, slice(256, 512))
         return (pair[:, :HEAD] * jax.nn.sigmoid(pair[:, HEAD:])).astype(BF).astype(F32)
 
-    glu[16 : 16 + length] = gated(normed[...])
-    edge = gated(edges[...])
+    glu[16 : 16 + length] = gated(normed, scores[:, 256:])
+    edge = gated(edges, edge_scores[...])
     glu[:16] = edge[:16]
     glu[16 + length :] = edge[16:]
     framed = glu[...]
@@ -245,13 +304,6 @@
     standard = centred * lax.rsqrt(variance + 1e-05) * scale[...].astype(F32)
     conv_o[...] = (standard * jax.nn.sigmoid(standard)).astype(BF)
 
-    for k in range(4):
-        turn = lax.rem(x + k, 4)
-        for z in range(8):
-            to = pl.multiple_of((z * 4 + turn) * 64, 64)
-            at = (z * 4 + k) * 64
-            columns_o[pl.ds(to, 64)] = weights[at : at + 64, 512:768]
-
     t = lax.broadcasted_iota(jnp.int32, (BLOCK, BLOCK), 0)
     s = lax.broadcasted_iota(jnp.int32, (BLOCK, BLOCK), 1)
     for n in range(blocks):
@@ -260,15 +312,15 @@
         v = values[rows]
         total = jnp.zeros((BLOCK, HEAD), F32)
         for d in range(2):
-            c = cum[d, rows]
-            lifted = q * jnp.exp(c)
-            lowered = gap[d, rows] * jnp.exp(-c)
-            scores = nt(lifted.astype(BF), lowered.astype(BF))
-            scores = jnp.where(s <= t if d == 0 else s >= t, scores, 0.0)
-            total = total + dot(scores.astype(BF), v)
+            lifted = q * grown[d, rows]
+            scored = nt(lifted.astype(BF), lowered[d, rows])
+            scored = jnp.where(s <= t if d == 0 else s >= t, scored, 0.0)
+            total = total + dot(scored.astype(BF), v)
             total = total + nt(lifted.astype(BF), start[d, n])
             lifted_o[d, rows] = (lifted * jnp.exp(passed[d, n : n + 1])).astype(BF)
         local_o[rows] = total
+    for move in moves:
+        move.wait()
 
 
 def readout_kernel(place, local, lifted, every, before, rescale, gate, out):
@@ -365,12 +417,14 @@
         scratch=(pltpu.SemaphoreType.DMA((2,)),),
         left=(0,),
     )
-    first = lax.all_to_all(first, "z", 0, 0, tiled=True).reshape(512, 384)
+    first = lax.all_to_all(first, "z", 0, 0, tiled=True)
+    first = first.reshape(512, 384)
     ahead, far, behind = shift(shard, "x", -1), shift(shard, "x", 2), shift(shard, "x", 1)
     normed, normed_first = normalized(place, far_off(sequence_embeddings), gain, 2)
-    low, high = line(bottom, ("z", "x"), 1), line(top, ("z", "x"), -1)
-    normed, normed_first, shard, ahead, far, behind, low, high = lax.optimization_barrier(
-        (normed, normed_first, shard, ahead, far, behind, low, high)
+    low = line(bottom, ("z", "x"), 1)
+    high = line(top, ("z", "x"), -1)
+    normed, normed_first, shard, ahead, far, behind, low = lax.optimization_barrier(
+        (normed, normed_first, shard, ahead, far, behind, low)
     )
     (edges,) = normalized(place, jnp.concatenate([low, high], axis=0), gain, 1)
     (later,) = kernel_call(
@@ -387,6 +441,7 @@
     up1, down1 = shift(later, "z", 1), shift(later, "z", -1)
     far_low, far_high = shift(behind[:256], "x", 1), shift(ahead[256:], "x", -1)
     normed_first = keep(normed_first)
+    _, seen = ordered(high, behind)
     (near,) = kernel_call(
         near_scores_kernel,
         2,
@@ -394,7 +449,7 @@
         normed_first,
         keep(first),
         keep(ahead),
-        keep(behind),
+        keep(seen),
     )
     _, up1, down1 = ordered(near, up1, down1)
     up2, down2 = shift(up1, "z", 1), shift(down1, "z", -1)
@@ -432,6 +487,26 @@
     low4, high4 = shift(up3[:128], "z", 1), shift(down3[128:], "z", -1)
     every = lax.all_to_all(send, "z", 0, 0, tiled=True)
 
+    near_blocks = [far_off(a) for a in (later, down1, down2, up2, up1)]
+    far_blocks = [far_off(down3), low4, high4, far_off(up3)]
+    scores, edge_scores, lowered, grown = kernel_call(
+        early_kernel,
+        3,
+        [
+            pltpu.HBM((length, 512), F32),
+            pltpu.HBM((32, 256), F32),
+            pltpu.HBM((2, length, HEAD), BF),
+            pltpu.HBM((2, length, HEAD), F32),
+        ],
+        place,
+        far_off(normed),
+        keep(edges),
+        *near_blocks,
+        far_off(gap),
+        far_off(cum),
+        scratch=(pltpu.VMEM((5, 256, 512), BF), pltpu.SemaphoreType.DMA((5,))),
+        left=range(3, 8),
+    )
     local, lifted, gate, conv_out, columns = kernel_call(
         later_kernel,
         0.5,
@@ -443,19 +518,23 @@
             pltpu.VMEM((2048, 256), BF),
         ],
         place,
-        keep(normed),
+        far_off(normed),
         keep(edges),
-        *(far_off(a) for a in (later, down1, down2, down3, low4, high4, up3, up2, up1)),
-        *(far_off(a) for a in (values, gap, cum, start, passed)),
+        far_off(scores),
+        far_off(edge_scores),
+        *near_blocks,
+        *far_blocks,
+        *(far_off(a) for a in (values, lowered, grown, start, passed)),
         filter_kernel_coefs,
         channel_cluster_scale[None],
         scratch=(
             pltpu.VMEM((length, HEAD), F32),
             pltpu.VMEM((length + 32, HEAD), F32),
-            pltpu.VMEM((2048, 768), BF),
-            pltpu.SemaphoreType.DMA((9,)),
+            pltpu.VMEM((768, 512), BF),
+            pltpu.SemaphoreType.DMA((4,)),
+            pltpu.SemaphoreType.DMA((32,)),
         ),
-        left=range(3, 12),
+        left=range(5, 14),
     )
     (rec_out,) = kernel_call(
         readout_kernel,

time: 114 us -> 111 us (0.974)
  Pallas kernels: 21.5 us -> 26.8 us
  waiting for transfers between devices: 30 us -> 26.4 us
  local copies, waits for them, and re-layouts: 3.55 us -> 0.97 us
  starting transfers between devices: 56.4 us -> 54.5 us
    ppermute x23, waiting for transfers between devices: 28.6 us -> 18.8 us  [shift(): return lax.ppermute(array, axis, ring(lax.axis_size(axis), step))]
    pallas_call x13 -> x14, Pallas kernels: 21.5 us -> 26.8 us  [kernel_call(): pl.pallas_call(body, out_shape=tuple(outs), in_specs=[SMEM if o.dtype ==...]
    ppermute x2, waiting for transfers between devices: 0.01 us -> 4.81 us  [line(): return lax.ppermute(array, axes, pairs)]
    all_to_all x1, starting transfers between devices: 6.57 us -> 4.45 us  [layer(): every = lax.all_to_all(send, 'z', 0, 0, tiled=True)]
    unnamed x31 -> x17, local copies, waits for them, and re-layouts: 2.13 us -> 0.22 us
    all_to_all x1, waiting for transfers between devices: 1.35 us -> 2.8 us  [layer(): first = lax.all_to_all(first, 'z', 0, 0, tiled=True)]
  transfers between devices with their start and end apart: 27 -> 27, of which waited for: 12 -> 12; matrix products, arithmetic and copies ran while one was open for 2% -> 1% of each run, Pallas kernels for 14% -> 20%
where the time goes in v1:
time: 111 us; the launch traced here: 110 us
  starting transfers between devices  54.5 us (49%)
  Pallas kernels  26.8 us (24%)
  waiting for transfers between devices  26.4 us (24%)
    ppermute x23, starting transfers between devices, shift(): return lax.ppermute(array, axis, ring(lax.axis_size(axis), step))  36.2 us
    pallas_call x14, Pallas kernels, kernel_call(): pl.pallas_call(body, out_shape=tuple(outs), in_specs=[SMEM if o.dtype ==...  26.8 us
    ppermute x23, waiting for transfers between devices, shift(): return lax.ppermute(array, axis, ring(lax.axis_size(axis), step))  18.8 us
    all_to_all x1, starting transfers between devices, layer(): first = lax.all_to_all(first, 'z', 0, 0, tiled=True)  9.02 us
    ppermute x2, starting transfers between devices, line(): return lax.ppermute(array, axes, pairs)  4.83 us
    ppermute x2, waiting for transfers between devices, line(): return lax.ppermute(array, axes, pairs)  4.81 us
    all_to_all x1, starting transfers between devices, layer(): every = lax.all_to_all(send, 'z', 0, 0, tiled=True)  4.45 us
    all_to_all x1, waiting for transfers between devices, layer(): first = lax.all_to_all(first, 'z', 0, 0, tiled=True)  2.8 us
  transfers between devices with their start and end apart: 27, of which 12 were waited for; matrix products, arithmetic and copies ran while one was open for 1% of the time, Pallas kernels for 20%

profile of v1, /device:TPU:1, one launch (start us, length us, event | category | flops | bytes accessed | tf_op | source)
XLA Modules:
  0.0 109.9 jit_solution(16036789552888772493)
XLA Ops:
  0.0 2.5 %shard_map.155 = (bf16[8,64,384]{2,1,0:T(8,128)(2,1)}, bf16[64,768]{1,0:T(8,128)(2,1)S(1)}, bf16[16,2048]{1,0:T(8,128)(2,1)S(1)}, bf16[16,2048]{1,0:T(8,128)(2,1)S(1)}) custom-call(bf16[384,2048]{1,0:T(8,128)(2,1)} %x.3, bf16[64,128]{1,0:T(8,128)(2,1)} %refs_0_.1, bf16[64,128]{1,0:T(8,128)(2,1)} %refs_1_.1, bf16[64,128]{1,0:T(8,128)(2,1)} %refs_2_.1, ...), custom_call_target="tpu_custom_call" | custom-call | flops 8000000 | tf_op jit(solution)/shard_map/pallas_call | solution.py:49
  2.5 9.0 %all-to-all-start = ((bf16[8,64,384]{2,1,0:T(8,128)(2,1)}), bf16[8,64,384]{2,1,0:T(8,128)(2,1)S(1)}, u32[]{:S(2)}, u32[]{:S(2)}) async-start(bf16[8,64,384]{2,1,0:T(8,128)(2,1)} %get-tuple-element.57), calls=%async_computation | async-start | bytes 786432 | tf_op jit(solution)/shard_map/all_to_all | solution.py:420
  11.5 2.5 %collective-permute-start = (bf16[64,768]{1,0:T(8,128)(2,1)S(1)}, bf16[64,768]{1,0:T(8,128)(2,1)S(1)}, u32[]{:S(2)}, u32[]{:S(2)}) collective-permute-start(bf16[64,768]{1,0:T(8,128)(2,1)S(1)} %get-tuple-element.58.own), channel_id=1, source_target_pairs={{0,24},{8,0},{16,8},{24,16},{1,25},{9,1},{17,9},{25,17},{2,26},{10... | collective-permute-start | bytes 294920 | tf_op jit(solution)/shard_map/ppermute | solution.py:27
  14.0 0.5 collective-permute-start.1
  14.5 0.6 collective-permute-start.2
  15.1 3.4 %collective-permute-start.3 = (bf16[16,2048]{1,0:T(8,128)(2,1)S(1)}, bf16[16,2048]{1,0:T(8,128)(2,1)S(1)}, u32[]{:S(2)}, u32[]{:S(2)}) collective-permute-start(bf16[16,2048]{1,0:T(8,128)(2,1)S(1)} %get-tuple-element.53), channel_id=1, source_target_pairs={{0,8},{8,16},{16,24},{24,32},{32,40},{40,48},{48,56},{56,64},{64,7... | collective-permute-start | bytes 196616 | tf_op jit(solution)/shard_map/ppermute | solution.py:33
  18.6 0.1 pad_add_fusion.place
  18.7 4.3 %shard_map.154 = (bf16[384,2048]{1,0:T(8,128)(2,1)}, bf16[384,2048]{1,0:T(8,128)(2,1)S(1)}) custom-call(s32[4]{0:T(128)S(1)} %pad_add_fusion.place, bf16[384,2048]{1,0:T(8,128)(2,1)} %x.3, bf16[1,2048]{1,0:T(2,128)(2,1)S(1)} %broadcast_in_dim.16.gain), custom_call_target="tpu_custom_call" | custom-call | flops 12000000 | tf_op jit(solution)/shard_map/pallas_call | solution.py:49
  23.0 2.8 %all-to-all-done = bf16[8,64,384]{2,1,0:T(8,128)(2,1)S(1)} async-done(((bf16[8,64,384]{2,1,0:T(8,128)(2,1)}), bf16[8,64,384]{2,1,0:T(8,128)(2,1)S(1)}, u32[]{:S(2)}, u32[]{:S(2)}) %all-to-all-start) | async-done | bytes 393248 | tf_op jit(solution)/shard_map/all_to_all | solution.py:420
  25.8 1.2 %collective-permute-start.6 = (bf16[512,384]{1,0:T(8,128)(2,1)S(1)}, bf16[512,384]{1,0:T(8,128)(2,1)S(1)}, u32[]{:S(2)}, u32[]{:S(2)}) collective-permute-start(bf16[512,384]{1,0:T(8,128)(2,1)S(1)} %bitcast.11), channel_id=1, source_target_pairs={{0,8},{8,16},{16,24},{24,0},{1,9},{9,17},{17,25},{25,1},{2,10},{10... | collective-permute-start | bytes 1179656 | tf_op jit(solution)/shard_map/ppermute | solution.py:27
  27.0 1.5 %collective-permute-start.5 = (bf16[512,384]{1,0:T(8,128)(2,1)S(1)}, bf16[512,384]{1,0:T(8,128)(2,1)S(1)}, u32[]{:S(2)}, u32[]{:S(2)}) collective-permute-start(bf16[512,384]{1,0:T(8,128)(2,1)S(1)} %bitcast.12), channel_id=1, source_target_pairs={{0,24},{8,0},{16,8},{24,16},{1,25},{9,1},{17,9},{25,17},{2,26},{10... | collective-permute-start | bytes 1179656 | tf_op jit(solution)/shard_map/ppermute | solution.py:27
  28.5 0.0 collective-permute-done.1.far
  28.5 0.0 collective-permute-done.2.behind
  28.5 0.8 shard_map.157.refs_0_
  29.2 0.0 collective-permute-start.7
  29.2 2.7 %collective-permute-start.8 = (bf16[256,768]{1,0:T(8,128)(2,1)}, bf16[256,768]{1,0:T(8,128)(2,1)}, u32[]{:S(2)}, u32[]{:S(2)}) collective-permute-start(bf16[256,768]{1,0:T(8,128)(2,1)} %shard_map.157.refs_0_), channel_id=1, source_target_pairs={{0,224},{32,0},{64,32},{96,64},{128,96},{160,128},{192,160},{224,1... | collective-permute-start | bytes 1179656 | tf_op jit(solution)/shard_map/ppermute | solution.py:27
  31.9 1.4 %collective-permute-start.4 = (bf16[16,2048]{1,0:T(8,128)(2,1)S(1)}, bf16[16,2048]{1,0:T(8,128)(2,1)S(1)}, u32[]{:S(2)}, u32[]{:S(2)}) collective-permute-start(bf16[16,2048]{1,0:T(8,128)(2,1)S(1)} %get-tuple-element.56), channel_id=1, source_target_pairs={{8,0},{16,8},{24,16},{32,24},{40,32},{48,40},{56,48},{64,56},{72,6... | collective-permute-start | bytes 196616 | tf_op jit(solution)/shard_map/ppermute | solution.py:33
  33.3 4.8 %collective-permute-done.4 = bf16[16,2048]{1,0:T(8,128)(2,1)S(1)} collective-permute-done((bf16[16,2048]{1,0:T(8,128)(2,1)S(1)}, bf16[16,2048]{1,0:T(8,128)(2,1)S(1)}, u32[]{:S(2)}, u32[]{:S(2)}) %collective-permute-start.4) | collective-permute-done | bytes 65568 | tf_op jit(solution)/shard_map/ppermute | solution.py:33
  38.2 0.8 shard_map.158.near
  38.9 0.6 collective-permute-done.7.refs_4_
  39.5 0.0 collective-permute-done.8.refs_1_
  39.5 0.0 collective-permute-start.11
  39.5 2.7 %collective-permute-start.12 = (bf16[256,768]{1,0:T(8,128)(2,1)}, bf16[256,768]{1,0:T(8,128)(2,1)}, u32[]{:S(2)}, u32[]{:S(2)}) collective-permute-start(bf16[256,768]{1,0:T(8,128)(2,1)} %collective-permute-done.8.refs_1_), channel_id=1, source_target_pairs={{0,224},{32,0},{64,32},{96,64},{128,96},{160,128},{192,160},{224,1... | collective-permute-start | bytes 1179656 | tf_op jit(solution)/shard_map/ppermute | solution.py:27
  42.2 2.6 %collective-permute-start.10 = (bf16[256,384]{1,0:T(8,128)(2,1)S(1)}, bf16[256,384]{1,0:T(8,128)(2,1)S(1)}, u32[]{:S(2)}, u32[]{:S(2)}) collective-permute-start(bf16[256,384]{1,0:T(8,128)(2,1)S(1)} %slice.17), channel_id=1, source_target_pairs={{0,24},{8,0},{16,8},{24,16},{1,25},{9,1},{17,9},{25,17},{2,26},{10... | collective-permute-start | bytes 589832 | tf_op jit(solution)/shard_map/ppermute | solution.py:27
  44.8 0.7 slice.16
  45.5 0.2 copy.17.extra
  45.7 1.7 %collective-permute-done.10.far_high = bf16[256,384]{1,0:T(8,128)(2,1)S(1)} collective-permute-done((bf16[256,384]{1,0:T(8,128)(2,1)S(1)}, bf16[256,384]{1,0:T(8,128)(2,1)S(1)}, u32[]{:S(2)}, u32[]{:S(2)}) %collective-permute-start.10) | collective-permute-done | bytes 196640 | tf_op jit(solution)/shard_map/ppermute | solution.py:27
  47.4 4.4 %collective-permute-done.9.far_low = bf16[256,384]{1,0:T(8,128)(2,1)S(1)} collective-permute-done((bf16[256,384]{1,0:T(8,128)(2,1)}, bf16[256,384]{1,0:T(8,128)(2,1)S(1)}, u32[]{:S(2)}, u32[]{:S(2)}) %collective-permute-start.9) | collective-permute-done | bytes 196640 | tf_op jit(solution)/shard_map/ppermute | solution.py:27
  51.8 1.7 %shard_map.159 = (bf16[384,128]{1,0:T(8,128)(2,1)}, f32[2,384,128]{2,1,0:T(8,128)}, f32[2,384,128]{2,1,0:T(8,128)}, bf16[2,6,128,128]{3,2,1,0:T(8,128)(2,1)}, f3...) custom-call(f32[384,384]{1,0:T(8,128)S(1)} %shard_map.158.near, bf16[384,2048]{1,0:T(8,128)(2,1)S(1)} %get-tuple-element.63.normed, ...), custom_call_target="tpu_custom_call" | custom-call | flops 12000000 | tf_op jit(solution)/shard_map/pallas_call | solution.py:49
  53.5 0.2 collective-permute-start.16
  53.8 2.7 %collective-permute-start.17 = (bf16[256,768]{1,0:T(8,128)(2,1)}, bf16[256,768]{1,0:T(8,128)(2,1)S(1)}, u32[]{:S(2)}, u32[]{:S(2)}) collective-permute-start(bf16[256,768]{1,0:T(8,128)(2,1)} %collective-permute-done.12.refs_2_), channel_id=1, source_target_pairs={{0,224},{32,0},{64,32},{96,64},{128,96},{160,128},{192,160},{224,1... | collective-permute-start | bytes 1179656 | tf_op jit(solution)/shard_map/ppermute | solution.py:27
  56.4 0.0 collective-permute-start.13
  56.4 0.6 collective-permute-start.14
  57.0 0.9 collective-permute-start.15
  57.9 1.7 %collective-permute-done.13.ahead = bf16[2,144,128]{2,1,0:T(8,128)(2,1)S(1)} collective-permute-done((bf16[2,144,128]{2,1,0:T(8,128)(2,1)S(1)}, bf16[2,144,128]{2,1,0:T(8,128)(2,1)S(1)}, u32[]{:S(2)}, u32[]{:S(2)}) %collective-permute-start.13) | collective-permute-done | bytes 73760 | tf_op jit(solution)/shard_map/ppermute | solution.py:27
  59.6 1.5 %collective-permute-done.14.far = bf16[2,144,128]{2,1,0:T(8,128)(2,1)S(1)} collective-permute-done((bf16[2,144,128]{2,1,0:T(8,128)(2,1)S(1)}, bf16[2,144,128]{2,1,0:T(8,128)(2,1)S(1)}, u32[]{:S(2)}, u32[]{:S(2)}) %collective-permute-start.14) | collective-permute-done | bytes 73760 | tf_op jit(solution)/shard_map/ppermute | solution.py:27
  61.1 0.9 collective-permute-done.15.behind
  62.0 1.4 %shard_map.161 = (f32[2,136,128]{2,1,0:T(8,128)}, bf16[8,144,128]{2,1,0:T(8,128)(2,1)}) custom-call(s32[4]{0:T(128)S(1)} %pad_add_fusion.place, bf16[2,144,128]{2,1,0:T(8,128)(2,1)S(1)} %get-tuple-element.66.own, bf16[2,144,128]{2,1,0:T(8,128)(2,1)S(1)} %collective-permute-done.13.ahead, bf16[2,144,128]{2,1,0:T(8,128)(2,1)S(1)} %collective-permute-done.14.far, ...), custom_call_target="tpu_custom_call" | custom-call | flops 4000000 | tf_op jit(solution)/shard_map/pallas_call | solution.py:49
  63.4 4.4 %all-to-all-start.1 = ((bf16[8,144,128]{2,1,0:T(8,128)(2,1)}), bf16[8,144,128]{2,1,0:T(8,128)(2,1)S(1)}, u32[]{:S(2)}, u32[]{:S(2)}) async-start(bf16[8,144,128]{2,1,0:T(8,128)(2,1)} %get-tuple-element.74), calls=%async_computation.1 | async-start | bytes 589824 | tf_op jit(solution)/shard_map/all_to_all | solution.py:488
  67.9 0.0 collective-permute-done.16.refs_8_
  67.9 0.0 collective-permute-done.17.refs_5_
  68.0 1.5 %collective-permute-start.18 = (bf16[128,768]{1,0:T(8,128)(2,1)S(1)}, bf16[128,768]{1,0:T(8,128)(2,1)S(1)}, u32[]{:S(2)}, u32[]{:S(2)}) collective-permute-start(bf16[128,768]{1,0:T(8,128)(2,1)S(1)} %slice.14), channel_id=1, source_target_pairs={{0,32},{32,64},{64,96},{96,128},{128,160},{160,192},{192,224},{224... | collective-permute-start | bytes 589832 | tf_op jit(solution)/shard_map/ppermute | solution.py:27
  69.5 1.3 %collective-permute-start.19 = (bf16[128,768]{1,0:T(8,128)(2,1)S(1)}, bf16[128,768]{1,0:T(8,128)(2,1)S(1)}, u32[]{:S(2)}, u32[]{:S(2)}) collective-permute-start(bf16[128,768]{1,0:T(8,128)(2,1)S(1)} %slice.15), channel_id=1, source_target_pairs={{0,224},{32,0},{64,32},{96,64},{128,96},{160,128},{192,160},{224,1... | collective-permute-start | bytes 589832 | tf_op jit(solution)/shard_map/ppermute | solution.py:27
  70.8 0.8 shard_map.156.edges
  71.6 0.0 copy-start
  71.6 0.0 copy-start.3
  71.6 4.6 %shard_map.160 = (f32[384,512]{1,0:T(8,128)}, f32[32,256]{1,0:T(8,128)}, bf16[2,384,128]{2,1,0:T(8,128)(2,1)}, f32[2,384,128]{2,1,0:T(8,128)}) custom-call(s32[4]{0:T(128)S(1)} %pad_add_fusion.place, bf16[384,2048]{1,0:T(8,128)(2,1)} %get-tuple-element.54.normed, bf16[32,2048]{1,0:T(8,128)(2,1)S(1)} %shard_map.156.edges, ...), custom_call_target="tpu_custom_call" | custom-call | flops 12000000 | tf_op jit(solution)/shard_map/pallas_call | solution.py:49
  76.3 0.3 collective-permute-done.18.refs_6_
  76.6 0.0 copy-start.2
  76.6 6.7 %shard_map.162 = (f32[384,128]{1,0:T(8,128)}, bf16[2,384,128]{2,1,0:T(8,128)(2,1)}, f32[384,128]{1,0:T(8,128)}, bf16[384,128]{1,0:T(8,128)(2,1)S(1)}, bf16[2048,256]{1,0:T(8,128)(2,1)S(1)}) custom-call(s32[4]{0:T(128)S(1)} %pad_add_fusion.place, bf16[384,2048]{1,0:T(8,128)(2,1)} %get-tuple-element.54.normed, bf16[32,2048]{1,0:T(8,128)(2,1)S(1)} %shard_map.156.edges, ...), custom_call_target="tpu_custom_call" | custom-call | flops 2000000 | tf_op jit(solution)/shard_map/pallas_call | solution.py:49
  83.3 1.6 %shard_map.163.rec = bf16[384,128]{1,0:T(8,128)(2,1)S(1)} custom-call(s32[4]{0:T(128)S(1)} %pad_add_fusion.place, f32[384,128]{1,0:T(8,128)} %get-tuple-element.82.local, bf16[2,384,128]{2,1,0:T(8,128)(2,1)} %get-tuple-element.83.lifted, bf16[8,144,128]{2,1,0:T(8,128)(2,1)S(1)} %all-to-all-done.1.every, f32[2,136,128]{2,1,0:T(8,128)} %get-tuple-element.84.before, ...), custom_call_target="tpu_custom_call" | custom-call | flops 4000000 | tf_op jit(solution)/shard_map/pallas_call | solution.py:49
  84.9 0.5 shard_map.165
  85.5 9.2 %collective-permute-start.20 = (bf16[4,48,2048]{2,1,0:T(8,128)(2,1)S(1)}, bf16[4,48,2048]{2,1,0:T(8,128)(2,1)S(1)}, u32[]{:S(2)}, u32[]{:S(2)}) collective-permute-start(bf16[4,48,2048]{2,1,0:T(8,128)(2,1)S(1)} %shard_map.165), channel_id=1, source_target_pairs={{0,1},{1,0},{2,3},{3,2},{4,5},{5,4},{6,7},{7,6},{8,9},{9,8},{10,11... | collective-permute-start | bytes 2359304 | tf_op jit(solution)/shard_map/ppermute | solution.py:27
  94.6 0.5 shard_map.164.mine
  95.1 1.4 %collective-permute-done.20.got = bf16[4,48,2048]{2,1,0:T(8,128)(2,1)S(1)} collective-permute-done((bf16[4,48,2048]{2,1,0:T(8,128)(2,1)S(1)}, bf16[4,48,2048]{2,1,0:T(8,128)(2,1)S(1)}, u32[]{:S(2)}, u32[]{:S(2)}) %collective-permute-start.20) | collective-permute-done | bytes 786464 | tf_op jit(solution)/shard_map/ppermute | solution.py:27
  96.5 0.7 shard_map.166
  97.2 1.4 %collective-permute-start.21 = (bf16[48,1024]{1,0:T(8,128)(2,1)S(1)}, bf16[48,1024]{1,0:T(8,128)(2,1)S(1)}, u32[]{:S(2)}, u32[]{:S(2)}) collective-permute-start(bf16[48,1024]{1,0:T(8,128)(2,1)S(1)} %get-tuple-element.91), channel_id=1, source_target_pairs={{0,2},{2,4},{4,6},{6,0},{1,3},{3,5},{5,7},{7,1},{8,10},{10,12},{12... | collective-permute-start | bytes 294920 | tf_op jit(solution)/shard_map/ppermute | solution.py:27
  98.6 1.5 %collective-permute-start.22 = (bf16[48,1024]{1,0:T(8,128)(2,1)S(1)}, bf16[48,1024]{1,0:T(8,128)(2,1)S(1)}, u32[]{:S(2)}, u32[]{:S(2)}) collective-permute-start(bf16[48,1024]{1,0:T(8,128)(2,1)S(1)} %get-tuple-element.92), channel_id=1, source_target_pairs={{0,6},{2,0},{4,2},{6,4},{1,7},{3,1},{5,3},{7,5},{8,14},{10,8},{12,... | collective-permute-start | bytes 294920 | tf_op jit(solution)/shard_map/ppermute | solution.py:27
  100.1 2.5 %collective-permute-done.21.low = bf16[48,1024]{1,0:T(8,128)(2,1)S(1)} collective-permute-done((bf16[48,1024]{1,0:T(8,128)(2,1)S(1)}, bf16[48,1024]{1,0:T(8,128)(2,1)S(1)}, u32[]{:S(2)}, u32[]{:S(2)}) %collective-permute-start.21) | collective-permute-done | bytes 98336 | tf_op jit(solution)/shard_map/ppermute | solution.py:27
  102.6 0.1 shard_map.167
  102.7 0.9 collective-permute-start.23
  103.5 1.9 %collective-permute-start.24 = (bf16[48,2048]{1,0:T(8,128)(2,1)S(1)}, bf16[48,2048]{1,0:T(8,128)(2,1)S(1)}, u32[]{:S(2)}, u32[]{:S(2)}) collective-permute-start(bf16[48,2048]{1,0:T(8,128)(2,1)S(1)} %get-tuple-element.94), channel_id=1, source_target_pairs={{0,6},{2,0},{4,2},{6,4},{1,7},{3,1},{5,3},{7,5},{8,14},{10,8},{12,... | collective-permute-start | bytes 589832 | tf_op jit(solution)/shard_map/ppermute | solution.py:27
  105.4 3.7 %collective-permute-done.23 = bf16[48,2048]{1,0:T(8,128)(2,1)S(1)} collective-permute-done((bf16[48,2048]{1,0:T(8,128)(2,1)S(1)}, bf16[48,2048]{1,0:T(8,128)(2,1)S(1)}, u32[]{:S(2)}, u32[]{:S(2)}) %collective-permute-start.23) | collective-permute-done | bytes 196640 | tf_op jit(solution)/shard_map/ppermute | solution.py:27
  109.2 0.7 add_convert_fusion
  (29 shorter events, 0.1 us)
Async XLA Ops:
  0.0 18.6 %copy-start.6 = (bf16[2048]{0:T(1024)(128)(2,1)S(1)}, bf16[2048]{0:T(1024)(128)(2,1)}, u32[]{:S(2)}) copy-start(bf16[2048]{0:T(1024)(128)(2,1)} %param.17) | copy-start | bytes 12292
  2.5 23.3 %all-to-all-start = ((bf16[8,64,384]{2,1,0:T(8,128)(2,1)}), bf16[8,64,384]{2,1,0:T(8,128)(2,1)S(1)}, u32[]{:S(2)}, u32[]{:S(2)}) async-start(bf16[8,64,384]{2,1,0:T(8,128)(2,1)} %get-tuple-element.57), calls=%async_computation | async-start | bytes 786432 | tf_op jit(solution)/shard_map/all_to_all | solution.py:420
  11.5 16.9 %collective-permute-start = (bf16[64,768]{1,0:T(8,128)(2,1)S(1)}, bf16[64,768]{1,0:T(8,128)(2,1)S(1)}, u32[]{:S(2)}, u32[]{:S(2)}) collective-permute-start(bf16[64,768]{1,0:T(8,128)(2,1)S(1)} %get-tuple-element.58.own), channel_id=1, source_target_pairs={{0,24},{8,0},{16,8},{24,16},{1,25},{9,1},{17,9},{25,17},{2,26},{10... | collective-permute-start | bytes 294920 | tf_op jit(solution)/shard_map/ppermute | solution.py:27
  14.0 14.5 %collective-permute-start.1 = (bf16[64,768]{1,0:T(8,128)(2,1)S(1)}, bf16[64,768]{1,0:T(8,128)(2,1)S(1)}, u32[]{:S(2)}, u32[]{:S(2)}) collective-permute-start(bf16[64,768]{1,0:T(8,128)(2,1)S(1)} %get-tuple-element.58.own), channel_id=1, source_target_pairs={{0,16},{8,24},{16,0},{24,8},{1,17},{9,25},{17,1},{25,9},{2,18},{10... | collective-permute-start | bytes 294920 | tf_op jit(solution)/shard_map/ppermute | solution.py:27
  14.5 14.0 %collective-permute-start.2 = (bf16[64,768]{1,0:T(8,128)(2,1)S(1)}, bf16[64,768]{1,0:T(8,128)(2,1)S(1)}, u32[]{:S(2)}, u32[]{:S(2)}) collective-permute-start(bf16[64,768]{1,0:T(8,128)(2,1)S(1)} %get-tuple-element.58.own), channel_id=1, source_target_pairs={{0,8},{8,16},{16,24},{24,0},{1,9},{9,17},{17,25},{25,1},{2,10},{10... | collective-permute-start | bytes 294920 | tf_op jit(solution)/shard_map/ppermute | solution.py:27
  15.1 11.9 %collective-permute-start.3 = (bf16[16,2048]{1,0:T(8,128)(2,1)S(1)}, bf16[16,2048]{1,0:T(8,128)(2,1)S(1)}, u32[]{:S(2)}, u32[]{:S(2)}) collective-permute-start(bf16[16,2048]{1,0:T(8,128)(2,1)S(1)} %get-tuple-element.53), channel_id=1, source_target_pairs={{0,8},{8,16},{16,24},{24,32},{32,40},{40,48},{48,56},{56,64},{64,7... | collective-permute-start | bytes 196616 | tf_op jit(solution)/shard_map/ppermute | solution.py:33
  25.8 12.4 %collective-permute-start.6 = (bf16[512,384]{1,0:T(8,128)(2,1)S(1)}, bf16[512,384]{1,0:T(8,128)(2,1)S(1)}, u32[]{:S(2)}, u32[]{:S(2)}) collective-permute-start(bf16[512,384]{1,0:T(8,128)(2,1)S(1)} %bitcast.11), channel_id=1, source_target_pairs={{0,8},{8,16},{16,24},{24,0},{1,9},{9,17},{17,25},{25,1},{2,10},{10... | collective-permute-start | bytes 1179656 | tf_op jit(solution)/shard_map/ppermute | solution.py:27
  27.0 11.2 %collective-permute-start.5 = (bf16[512,384]{1,0:T(8,128)(2,1)S(1)}, bf16[512,384]{1,0:T(8,128)(2,1)S(1)}, u32[]{:S(2)}, u32[]{:S(2)}) collective-permute-start(bf16[512,384]{1,0:T(8,128)(2,1)S(1)} %bitcast.12), channel_id=1, source_target_pairs={{0,24},{8,0},{16,8},{24,16},{1,25},{9,1},{17,9},{25,17},{2,26},{10... | collective-permute-start | bytes 1179656 | tf_op jit(solution)/shard_map/ppermute | solution.py:27
  29.2 10.3 %collective-permute-start.7 = (bf16[256,768]{1,0:T(8,128)(2,1)}, bf16[256,768]{1,0:T(8,128)(2,1)}, u32[]{:S(2)}, u32[]{:S(2)}) collective-permute-start(bf16[256,768]{1,0:T(8,128)(2,1)} %shard_map.157.refs_0_), channel_id=1, source_target_pairs={{0,32},{32,64},{64,96},{96,128},{128,160},{160,192},{192,224},{224... | collective-permute-start | bytes 1179656 | tf_op jit(solution)/shard_map/ppermute | solution.py:27
  29.2 10.3 %collective-permute-start.8 = (bf16[256,768]{1,0:T(8,128)(2,1)}, bf16[256,768]{1,0:T(8,128)(2,1)}, u32[]{:S(2)}, u32[]{:S(2)}) collective-permute-start(bf16[256,768]{1,0:T(8,128)(2,1)} %shard_map.157.refs_0_), channel_id=1, source_target_pairs={{0,224},{32,0},{64,32},{96,64},{128,96},{160,128},{192,160},{224,1... | collective-permute-start | bytes 1179656 | tf_op jit(solution)/shard_map/ppermute | solution.py:27
  31.9 13.6 %copy-start.7 = (f32[2,384,1]{1,2,0:T(1,128)S(1)}, f32[2,384,1]{1,2,0:T(1,128)}, u32[]{:S(2)}) copy-start(f32[2,384,1]{1,2,0:T(1,128)} %param.26) | copy-start | bytes 9220
  31.9 19.9 %copy-start.1 = (f32[2,128]{1,0:T(2,128)S(1)}, f32[2,128]{1,0:T(2,128)}, u32[]{:S(2)}) copy-start(f32[2,128]{1,0:T(2,128)} %slack.1) | copy-start | bytes 3076
  31.9 6.2 %collective-permute-start.4 = (bf16[16,2048]{1,0:T(8,128)(2,1)S(1)}, bf16[16,2048]{1,0:T(8,128)(2,1)S(1)}, u32[]{:S(2)}, u32[]{:S(2)}) collective-permute-start(bf16[16,2048]{1,0:T(8,128)(2,1)S(1)} %get-tuple-element.56), channel_id=1, source_target_pairs={{8,0},{16,8},{24,16},{32,24},{40,32},{48,40},{56,48},{64,56},{72,6... | collective-permute-start | bytes 196616 | tf_op jit(solution)/shard_map/ppermute | solution.py:33
  39.5 14.0 %collective-permute-start.11 = (bf16[256,768]{1,0:T(8,128)(2,1)}, bf16[256,768]{1,0:T(8,128)(2,1)}, u32[]{:S(2)}, u32[]{:S(2)}) collective-permute-start(bf16[256,768]{1,0:T(8,128)(2,1)} %collective-permute-done.7.refs_4_), channel_id=1, source_target_pairs={{0,32},{32,64},{64,96},{96,128},{128,160},{160,192},{192,224},{224... | collective-permute-start | bytes 1179656 | tf_op jit(solution)/shard_map/ppermute | solution.py:27
  39.5 14.0 %collective-permute-start.12 = (bf16[256,768]{1,0:T(8,128)(2,1)}, bf16[256,768]{1,0:T(8,128)(2,1)}, u32[]{:S(2)}, u32[]{:S(2)}) collective-permute-start(bf16[256,768]{1,0:T(8,128)(2,1)} %collective-permute-done.8.refs_1_), channel_id=1, source_target_pairs={{0,224},{32,0},{64,32},{96,64},{128,96},{160,128},{192,160},{224,1... | collective-permute-start | bytes 1179656 | tf_op jit(solution)/shard_map/ppermute | solution.py:27
  42.2 5.2 %collective-permute-start.10 = (bf16[256,384]{1,0:T(8,128)(2,1)S(1)}, bf16[256,384]{1,0:T(8,128)(2,1)S(1)}, u32[]{:S(2)}, u32[]{:S(2)}) collective-permute-start(bf16[256,384]{1,0:T(8,128)(2,1)S(1)} %slice.17), channel_id=1, source_target_pairs={{0,24},{8,0},{16,8},{24,16},{1,25},{9,1},{17,9},{25,17},{2,26},{10... | collective-permute-start | bytes 589832 | tf_op jit(solution)/shard_map/ppermute | solution.py:27
  45.5 6.3 %collective-permute-start.9 = (bf16[256,384]{1,0:T(8,128)(2,1)}, bf16[256,384]{1,0:T(8,128)(2,1)S(1)}, u32[]{:S(2)}, u32[]{:S(2)}) collective-permute-start(bf16[256,384]{1,0:T(8,128)(2,1)} %slice.16), channel_id=1, source_target_pairs={{0,8},{8,16},{16,24},{24,0},{1,9},{9,17},{17,25},{25,1},{2,10},{10... | collective-permute-start | bytes 589832 | tf_op jit(solution)/shard_map/ppermute | solution.py:27
  53.5 14.4 %collective-permute-start.16 = (bf16[256,768]{1,0:T(8,128)(2,1)}, bf16[256,768]{1,0:T(8,128)(2,1)S(1)}, u32[]{:S(2)}, u32[]{:S(2)}) collective-permute-start(bf16[256,768]{1,0:T(8,128)(2,1)} %collective-permute-done.11.refs_3_), channel_id=1, source_target_pairs={{0,32},{32,64},{64,96},{96,128},{128,160},{160,192},{192,224},{224... | collective-permute-start | bytes 1179656 | tf_op jit(solution)/shard_map/ppermute | solution.py:27
  53.8 14.1 %collective-permute-start.17 = (bf16[256,768]{1,0:T(8,128)(2,1)}, bf16[256,768]{1,0:T(8,128)(2,1)S(1)}, u32[]{:S(2)}, u32[]{:S(2)}) collective-permute-start(bf16[256,768]{1,0:T(8,128)(2,1)} %collective-permute-done.12.refs_2_), channel_id=1, source_target_pairs={{0,224},{32,0},{64,32},{96,64},{128,96},{160,128},{192,160},{224,1... | collective-permute-start | bytes 1179656 | tf_op jit(solution)/shard_map/ppermute | solution.py:27
  56.4 3.2 %collective-permute-start.13 = (bf16[2,144,128]{2,1,0:T(8,128)(2,1)S(1)}, bf16[2,144,128]{2,1,0:T(8,128)(2,1)S(1)}, u32[]{:S(2)}, u32[]{:S(2)}) collective-permute-start(bf16[2,144,128]{2,1,0:T(8,128)(2,1)S(1)} %get-tuple-element.66.own), channel_id=1, source_target_pairs={{0,24},{8,0},{16,8},{24,16},{1,25},{9,1},{17,9},{25,17},{2,26},{10... | collective-permute-start | bytes 221192 | tf_op jit(solution)/shard_map/ppermute | solution.py:27
  56.4 4.7 %collective-permute-start.14 = (bf16[2,144,128]{2,1,0:T(8,128)(2,1)S(1)}, bf16[2,144,128]{2,1,0:T(8,128)(2,1)S(1)}, u32[]{:S(2)}, u32[]{:S(2)}) collective-permute-start(bf16[2,144,128]{2,1,0:T(8,128)(2,1)S(1)} %get-tuple-element.66.own), channel_id=1, source_target_pairs={{0,16},{8,24},{16,0},{24,8},{1,17},{9,25},{17,1},{25,9},{2,18},{10... | collective-permute-start | bytes 221192 | tf_op jit(solution)/shard_map/ppermute | solution.py:27
  57.0 5.0 %collective-permute-start.15 = (bf16[2,144,128]{2,1,0:T(8,128)(2,1)S(1)}, bf16[2,144,128]{2,1,0:T(8,128)(2,1)S(1)}, u32[]{:S(2)}, u32[]{:S(2)}) collective-permute-start(bf16[2,144,128]{2,1,0:T(8,128)(2,1)S(1)} %get-tuple-element.66.own), channel_id=1, source_target_pairs={{0,8},{8,16},{16,24},{24,0},{1,9},{9,17},{17,25},{25,1},{2,10},{10... | collective-permute-start | bytes 221192 | tf_op jit(solution)/shard_map/ppermute | solution.py:27
  63.4 19.8 %all-to-all-start.1 = ((bf16[8,144,128]{2,1,0:T(8,128)(2,1)}), bf16[8,144,128]{2,1,0:T(8,128)(2,1)S(1)}, u32[]{:S(2)}, u32[]{:S(2)}) async-start(bf16[8,144,128]{2,1,0:T(8,128)(2,1)} %get-tuple-element.74), calls=%async_computation.1 | async-start | bytes 589824 | tf_op jit(solution)/shard_map/all_to_all | solution.py:488
  67.9 8.3 %copy-start.4 = (bf16[256,768]{1,0:T(8,128)(2,1)}, bf16[256,768]{1,0:T(8,128)(2,1)S(1)}, u32[]{:S(2)}) copy-start(bf16[256,768]{1,0:T(8,128)(2,1)S(1)} %collective-permute-done.16.refs_8_) | copy-start | bytes 1179652
  67.9 8.3 %copy-start.5 = (bf16[256,768]{1,0:T(8,128)(2,1)}, bf16[256,768]{1,0:T(8,128)(2,1)S(1)}, u32[]{:S(2)}) copy-start(bf16[256,768]{1,0:T(8,128)(2,1)S(1)} %collective-permute-done.17.refs_5_) | copy-start | bytes 1179652
  68.0 8.6 %collective-permute-start.18 = (bf16[128,768]{1,0:T(8,128)(2,1)S(1)}, bf16[128,768]{1,0:T(8,128)(2,1)S(1)}, u32[]{:S(2)}, u32[]{:S(2)}) collective-permute-start(bf16[128,768]{1,0:T(8,128)(2,1)S(1)} %slice.14), channel_id=1, source_target_pairs={{0,32},{32,64},{64,96},{96,128},{128,160},{160,192},{192,224},{224... | collective-permute-start | bytes 589832 | tf_op jit(solution)/shard_map/ppermute | solution.py:27
  69.5 7.1 %collective-permute-start.19 = (bf16[128,768]{1,0:T(8,128)(2,1)S(1)}, bf16[128,768]{1,0:T(8,128)(2,1)S(1)}, u32[]{:S(2)}, u32[]{:S(2)}) collective-permute-start(bf16[128,768]{1,0:T(8,128)(2,1)S(1)} %slice.15), channel_id=1, source_target_pairs={{0,224},{32,0},{64,32},{96,64},{128,96},{160,128},{192,160},{224,1... | collective-permute-start | bytes 589832 | tf_op jit(solution)/shard_map/ppermute | solution.py:27
  71.6 5.0 %copy-start = (bf16[31,128]{1,0:T(8,128)(2,1)S(1)}, bf16[31,128]{1,0:T(8,128)(2,1)}, u32[]{:S(2)}) copy-start(bf16[31,128]{1,0:T(8,128)(2,1)} %refs_14_.1) | copy-start | bytes 23812
  71.6 5.0 %copy-start.3 = (bf16[128]{0:T(256)(128)(2,1)S(1)}, bf16[128]{0:T(256)(128)(2,1)}, u32[]{:S(2)}) copy-start(bf16[128]{0:T(256)(128)(2,1)} %param.29) | copy-start | bytes 772
  76.6 6.7 %copy-start.2 = (bf16[128]{0:T(256)(128)(2,1)S(1)}, bf16[128]{0:T(256)(128)(2,1)}, u32[]{:S(2)}) copy-start(bf16[128]{0:T(256)(128)(2,1)} %param.27) | copy-start | bytes 772
  85.5 11.1 %collective-permute-start.20 = (bf16[4,48,2048]{2,1,0:T(8,128)(2,1)S(1)}, bf16[4,48,2048]{2,1,0:T(8,128)(2,1)S(1)}, u32[]{:S(2)}, u32[]{:S(2)}) collective-permute-start(bf16[4,48,2048]{2,1,0:T(8,128)(2,1)S(1)} %shard_map.165), channel_id=1, source_target_pairs={{0,1},{1,0},{2,3},{3,2},{4,5},{5,4},{6,7},{7,6},{8,9},{9,8},{10,11... | collective-permute-start | bytes 2359304 | tf_op jit(solution)/shard_map/ppermute | solution.py:27
  97.2 5.4 %collective-permute-start.21 = (bf16[48,1024]{1,0:T(8,128)(2,1)S(1)}, bf16[48,1024]{1,0:T(8,128)(2,1)S(1)}, u32[]{:S(2)}, u32[]{:S(2)}) collective-permute-start(bf16[48,1024]{1,0:T(8,128)(2,1)S(1)} %get-tuple-element.91), channel_id=1, source_target_pairs={{0,2},{2,4},{4,6},{6,0},{1,3},{3,5},{5,7},{7,1},{8,10},{10,12},{12... | collective-permute-start | bytes 294920 | tf_op jit(solution)/shard_map/ppermute | solution.py:27
  98.6 4.0 %collective-permute-start.22 = (bf16[48,1024]{1,0:T(8,128)(2,1)S(1)}, bf16[48,1024]{1,0:T(8,128)(2,1)S(1)}, u32[]{:S(2)}, u32[]{:S(2)}) collective-permute-start(bf16[48,1024]{1,0:T(8,128)(2,1)S(1)} %get-tuple-element.92), channel_id=1, source_target_pairs={{0,6},{2,0},{4,2},{6,4},{1,7},{3,1},{5,3},{7,5},{8,14},{10,8},{12,... | collective-permute-start | bytes 294920 | tf_op jit(solution)/shard_map/ppermute | solution.py:27
  102.7 6.5 %collective-permute-start.23 = (bf16[48,2048]{1,0:T(8,128)(2,1)S(1)}, bf16[48,2048]{1,0:T(8,128)(2,1)S(1)}, u32[]{:S(2)}, u32[]{:S(2)}) collective-permute-start(bf16[48,2048]{1,0:T(8,128)(2,1)S(1)} %get-tuple-element.93), channel_id=1, source_target_pairs={{0,2},{2,4},{4,6},{6,0},{1,3},{3,5},{5,7},{7,1},{8,10},{10,12},{12... | collective-permute-start | bytes 589832 | tf_op jit(solution)/shard_map/ppermute | solution.py:27
  103.5 5.6 %collective-permute-start.24 = (bf16[48,2048]{1,0:T(8,128)(2,1)S(1)}, bf16[48,2048]{1,0:T(8,128)(2,1)S(1)}, u32[]{:S(2)}, u32[]{:S(2)}) collective-permute-start(bf16[48,2048]{1,0:T(8,128)(2,1)S(1)} %get-tuple-element.94), channel_id=1, source_target_pairs={{0,6},{2,0},{4,2},{6,4},{1,7},{3,1},{5,3},{7,5},{8,14},{10,8},{12,... | collective-permute-start | bytes 589832 | tf_op jit(solution)/shard_map/ppermute | solution.py:27

commit v2 on v1

--- a/solution.py
+++ b/solution.py
@@ -243,19 +243,29 @@
 
 def later_kernel(place, normed, edges, scores, edge_scores, *refs):
     near, far = refs[:5], refs[5:9]
-    values, lowered, grown, start, passed, taps, scale = refs[9:16]
-    local_o, lifted_o, gate_o, conv_o, columns_o, query, glu, held, done, placed = refs[16:]
+    values_i, start_i, passed, lowered, grown, taps, scale = refs[9:16]
+    local_o, lifted_o, gate_o, conv_o, columns_o = refs[16:21]
+    query, glu, held, features, values, start, done, placed = refs[21:]
     x = place[2]
     length = normed.shape[0]
     blocks = length // BLOCK
     copies = []
     spots = spread(place, far, FAR_STEPS)
     at = 0
-    for k, (piece, _, count) in enumerate(spots):
-        into = held.at[at : at + count]
-        copies.append(pltpu.make_async_copy(piece.at[:, :512], into, done.at[k]))
-        copies[-1].start()
+    for piece, feature, count in spots:
+        for source, into in (
+            (piece.at[:, :512], held.at[at : at + count]),
+            (normed.at[:, pl.ds(feature, count)], features.at[:, at : at + count]),
+        ):
+            copies.append(pltpu.make_async_copy(source, into, done.at[len(copies)]))
+            copies[-1].start()
         at += count
+    later_copies = [
+        pltpu.make_async_copy(values_i, values, done.at[8]),
+        pltpu.make_async_copy(start_i, start, done.at[9]),
+    ]
+    for copy in later_copies:
+        copy.start()
     moves = []
     for piece, feature, count in spread(place, near + far, NEAR_STEPS + FAR_STEPS):
         base = lax.div(feature, 256) * 256
@@ -270,23 +280,19 @@
     for copy in copies:
         copy.wait()
 
-    def finished(rows, before, columns):
-        total, at = before, 0
-        for _, feature, count in spots:
-            total = total + dot(rows[:, pl.ds(feature, count)], held[at : at + count, columns])
-            at += count
-        return total
-
-    pre = finished(normed, scores[:, :256], slice(0, 256))
+    pre = scores[:, :256] + dot(features[...], held[:, :256])
     query[...] = pre[:, :HEAD] * jax.nn.sigmoid(pre[:, :HEAD])
     gate_o[...] = pre[:, HEAD:] * jax.nn.sigmoid(pre[:, HEAD:])
 
-    def gated(rows, before):
-        pair = finished(rows, before, slice(256, 512))
+    def gated(pair):
         return (pair[:, :HEAD] * jax.nn.sigmoid(pair[:, HEAD:])).astype(BF).astype(F32)
 
-    glu[16 : 16 + length] = gated(normed, scores[:, 256:])
-    edge = gated(edges, edge_scores[...])
+    glu[16 : 16 + length] = gated(scores[:, 256:] + dot(features[...], held[:, 256:]))
+    edge, at = edge_scores[...], 0
+    for _, feature, count in spots:
+        edge = edge + dot(edges[:, pl.ds(feature, count)], held[at : at + count, 256:])
+        at += count
+    edge = gated(edge)
     glu[:16] = edge[:16]
     glu[16 + length :] = edge[16:]
     framed = glu[...]
@@ -304,6 +310,8 @@
     standard = centred * lax.rsqrt(variance + 1e-05) * scale[...].astype(F32)
     conv_o[...] = (standard * jax.nn.sigmoid(standard)).astype(BF)
 
+    for copy in later_copies:
+        copy.wait()
     t = lax.broadcasted_iota(jnp.int32, (BLOCK, BLOCK), 0)
     s = lax.broadcasted_iota(jnp.int32, (BLOCK, BLOCK), 1)
     for n in range(blocks):
@@ -493,10 +501,10 @@
         early_kernel,
         3,
         [
-            pltpu.HBM((length, 512), F32),
-            pltpu.HBM((32, 256), F32),
-            pltpu.HBM((2, length, HEAD), BF),
-            pltpu.HBM((2, length, HEAD), F32),
+            pltpu.VMEM((length, 512), F32),
+            pltpu.VMEM((32, 256), F32),
+            pltpu.VMEM((2, length, HEAD), BF),
+            pltpu.VMEM((2, length, HEAD), F32),
         ],
         place,
         far_off(normed),
@@ -511,42 +519,49 @@
         later_kernel,
         0.5,
         [
-            pltpu.HBM((length, HEAD), F32),
-            pltpu.HBM((2, length, HEAD), BF),
-            pltpu.HBM((length, HEAD), F32),
+            pltpu.VMEM((length, HEAD), F32),
+            pltpu.VMEM((2, length, HEAD), BF),
+            pltpu.VMEM((length, HEAD), F32),
             pltpu.VMEM((length, HEAD), BF),
             pltpu.VMEM((2048, 256), BF),
         ],
         place,
         far_off(normed),
         keep(edges),
-        far_off(scores),
-        far_off(edge_scores),
+        keep(scores),
+        keep(edge_scores),
         *near_blocks,
         *far_blocks,
-        *(far_off(a) for a in (values, lowered, grown, start, passed)),
+        far_off(values),
+        far_off(start),
+        far_off(passed),
+        keep(lowered),
+        keep(grown),
         filter_kernel_coefs,
         channel_cluster_scale[None],
         scratch=(
             pltpu.VMEM((length, HEAD), F32),
             pltpu.VMEM((length + 32, HEAD), F32),
             pltpu.VMEM((768, 512), BF),
-            pltpu.SemaphoreType.DMA((4,)),
+            pltpu.VMEM((length, 768), BF),
+            pltpu.VMEM((length, HEAD), BF),
+            pltpu.VMEM((2, blocks, HEAD, HEAD), BF),
+            pltpu.SemaphoreType.DMA((10,)),
             pltpu.SemaphoreType.DMA((32,)),
         ),
-        left=range(5, 14),
+        left=(1, *range(5, 16)),
     )
     (rec_out,) = kernel_call(
         readout_kernel,
         1,
         [pltpu.VMEM((length, HEAD), BF)],
         place,
-        far_off(local),
-        far_off(lifted),
+        keep(local),
+        keep(lifted),
         keep(every),
         far_off(before),
         subspace_rescale[None],
-        far_off(gate),
+        keep(gate),
     )
     theirs, mine = (
         kernel_call(

time: 111 us -> 109 us (0.982)
  Pallas kernels: 26.8 us -> 24.1 us
    pallas_call x14, Pallas kernels: 26.8 us -> 24.1 us  [kernel_call(): pl.pallas_call(body, out_shape=tuple(outs), in_specs=[SMEM if o.dtype ==...]
  transfers between devices with their start and end apart: 27 -> 27, of which waited for: 12 -> 12; matrix products, arithmetic and copies ran while one was open for 1% -> 1% of each run, Pallas kernels for 20% -> 18%
where the time goes in v2:
time: 109 us; the launch traced here: 108 us
  starting transfers between devices  54.5 us (50%)
  waiting for transfers between devices  27.4 us (25%)
  Pallas kernels  24.1 us (22%)
    ppermute x23, starting transfers between devices, shift(): return lax.ppermute(array, axis, ring(lax.axis_size(axis), step))  36.2 us
    pallas_call x14, Pallas kernels, kernel_call(): pl.pallas_call(body, out_shape=tuple(outs), in_specs=[SMEM if o.dtype ==...  24.1 us
    ppermute x23, waiting for transfers between devices, shift(): return lax.ppermute(array, axis, ring(lax.axis_size(axis), step))  19.8 us
    all_to_all x1, starting transfers between devices, layer(): first = lax.all_to_all(first, 'z', 0, 0, tiled=True)  9.02 us
    ppermute x2, starting transfers between devices, line(): return lax.ppermute(array, axes, pairs)  4.83 us
    ppermute x2, waiting for transfers between devices, line(): return lax.ppermute(array, axes, pairs)  4.81 us
    all_to_all x1, starting transfers between devices, layer(): every = lax.all_to_all(send, 'z', 0, 0, tiled=True)  4.45 us
    all_to_all x1, waiting for transfers between devices, layer(): first = lax.all_to_all(first, 'z', 0, 0, tiled=True)  2.8 us
  transfers between devices with their start and end apart: 27, of which 12 were waited for; matrix products, arithmetic and copies ran while one was open for 1% of the time, Pallas kernels for 18%

profile of v2, /device:TPU:1, one launch (start us, length us, event | category | flops | bytes accessed | tf_op | source)
XLA Modules:
  0.0 108.1 jit_solution(8482735690137102653)
XLA Ops:
  0.0 2.5 %shard_map.155 = (bf16[8,64,384]{2,1,0:T(8,128)(2,1)}, bf16[64,768]{1,0:T(8,128)(2,1)S(1)}, bf16[16,2048]{1,0:T(8,128)(2,1)S(1)}, bf16[16,2048]{1,0:T(8,128)(2,1)S(1)}) custom-call(bf16[384,2048]{1,0:T(8,128)(2,1)} %x.3, bf16[64,128]{1,0:T(8,128)(2,1)} %refs_0_.1, bf16[64,128]{1,0:T(8,128)(2,1)} %refs_1_.1, bf16[64,128]{1,0:T(8,128)(2,1)} %refs_2_.1, ...), custom_call_target="tpu_custom_call" | custom-call | flops 8000000 | tf_op jit(solution)/shard_map/pallas_call | solution.py:49
  2.5 9.0 %all-to-all-start = ((bf16[8,64,384]{2,1,0:T(8,128)(2,1)}), bf16[8,64,384]{2,1,0:T(8,128)(2,1)S(1)}, u32[]{:S(2)}, u32[]{:S(2)}) async-start(bf16[8,64,384]{2,1,0:T(8,128)(2,1)} %get-tuple-element.57), calls=%async_computation | async-start | bytes 786432 | tf_op jit(solution)/shard_map/all_to_all | solution.py:428
  11.5 2.5 %collective-permute-start = (bf16[64,768]{1,0:T(8,128)(2,1)S(1)}, bf16[64,768]{1,0:T(8,128)(2,1)S(1)}, u32[]{:S(2)}, u32[]{:S(2)}) collective-permute-start(bf16[64,768]{1,0:T(8,128)(2,1)S(1)} %get-tuple-element.58.own), channel_id=1, source_target_pairs={{0,24},{8,0},{16,8},{24,16},{1,25},{9,1},{17,9},{25,17},{2,26},{10... | collective-permute-start | bytes 294920 | tf_op jit(solution)/shard_map/ppermute | solution.py:27
  14.0 0.5 collective-permute-start.1
  14.5 0.6 collective-permute-start.2
  15.1 3.4 %collective-permute-start.3 = (bf16[16,2048]{1,0:T(8,128)(2,1)S(1)}, bf16[16,2048]{1,0:T(8,128)(2,1)S(1)}, u32[]{:S(2)}, u32[]{:S(2)}) collective-permute-start(bf16[16,2048]{1,0:T(8,128)(2,1)S(1)} %get-tuple-element.53), channel_id=1, source_target_pairs={{0,8},{8,16},{16,24},{24,32},{32,40},{40,48},{48,56},{56,64},{64,7... | collective-permute-start | bytes 196616 | tf_op jit(solution)/shard_map/ppermute | solution.py:33
  18.6 0.1 pad_add_fusion.place
  18.7 4.3 %shard_map.154 = (bf16[384,2048]{1,0:T(8,128)(2,1)}, bf16[384,2048]{1,0:T(8,128)(2,1)S(1)}) custom-call(s32[4]{0:T(128)S(1)} %pad_add_fusion.place, bf16[384,2048]{1,0:T(8,128)(2,1)} %x.3, bf16[1,2048]{1,0:T(2,128)(2,1)S(1)} %broadcast_in_dim.16.gain), custom_call_target="tpu_custom_call" | custom-call | flops 12000000 | tf_op jit(solution)/shard_map/pallas_call | solution.py:49
  23.0 2.8 %all-to-all-done = bf16[8,64,384]{2,1,0:T(8,128)(2,1)S(1)} async-done(((bf16[8,64,384]{2,1,0:T(8,128)(2,1)}), bf16[8,64,384]{2,1,0:T(8,128)(2,1)S(1)}, u32[]{:S(2)}, u32[]{:S(2)}) %all-to-all-start) | async-done | bytes 393248 | tf_op jit(solution)/shard_map/all_to_all | solution.py:428
  25.8 1.2 %collective-permute-start.6 = (bf16[512,384]{1,0:T(8,128)(2,1)S(1)}, bf16[512,384]{1,0:T(8,128)(2,1)S(1)}, u32[]{:S(2)}, u32[]{:S(2)}) collective-permute-start(bf16[512,384]{1,0:T(8,128)(2,1)S(1)} %bitcast.11), channel_id=1, source_target_pairs={{0,8},{8,16},{16,24},{24,0},{1,9},{9,17},{17,25},{25,1},{2,10},{10... | collective-permute-start | bytes 1179656 | tf_op jit(solution)/shard_map/ppermute | solution.py:27
  27.0 1.5 %collective-permute-start.5 = (bf16[512,384]{1,0:T(8,128)(2,1)S(1)}, bf16[512,384]{1,0:T(8,128)(2,1)S(1)}, u32[]{:S(2)}, u32[]{:S(2)}) collective-permute-start(bf16[512,384]{1,0:T(8,128)(2,1)S(1)} %bitcast.12), channel_id=1, source_target_pairs={{0,24},{8,0},{16,8},{24,16},{1,25},{9,1},{17,9},{25,17},{2,26},{10... | collective-permute-start | bytes 1179656 | tf_op jit(solution)/shard_map/ppermute | solution.py:27
  28.5 0.0 collective-permute-done.1.far
  28.5 0.0 collective-permute-done.2.behind
  28.5 0.8 shard_map.157.refs_0_
  29.2 0.0 collective-permute-start.7
  29.2 2.7 %collective-permute-start.8 = (bf16[256,768]{1,0:T(8,128)(2,1)}, bf16[256,768]{1,0:T(8,128)(2,1)}, u32[]{:S(2)}, u32[]{:S(2)}) collective-permute-start(bf16[256,768]{1,0:T(8,128)(2,1)} %shard_map.157.refs_0_), channel_id=1, source_target_pairs={{0,224},{32,0},{64,32},{96,64},{128,96},{160,128},{192,160},{224,1... | collective-permute-start | bytes 1179656 | tf_op jit(solution)/shard_map/ppermute | solution.py:27
  31.9 1.4 %collective-permute-start.4 = (bf16[16,2048]{1,0:T(8,128)(2,1)S(1)}, bf16[16,2048]{1,0:T(8,128)(2,1)S(1)}, u32[]{:S(2)}, u32[]{:S(2)}) collective-permute-start(bf16[16,2048]{1,0:T(8,128)(2,1)S(1)} %get-tuple-element.56), channel_id=1, source_target_pairs={{8,0},{16,8},{24,16},{32,24},{40,32},{48,40},{56,48},{64,56},{72,6... | collective-permute-start | bytes 196616 | tf_op jit(solution)/shard_map/ppermute | solution.py:33
  33.3 4.8 %collective-permute-done.4 = bf16[16,2048]{1,0:T(8,128)(2,1)S(1)} collective-permute-done((bf16[16,2048]{1,0:T(8,128)(2,1)S(1)}, bf16[16,2048]{1,0:T(8,128)(2,1)S(1)}, u32[]{:S(2)}, u32[]{:S(2)}) %collective-permute-start.4) | collective-permute-done | bytes 65568 | tf_op jit(solution)/shard_map/ppermute | solution.py:33
  38.1 0.0 collective-permute-done.6.behind
  38.1 0.8 shard_map.158.near
  38.9 0.6 collective-permute-done.7.refs_4_
  39.5 2.7 %collective-permute-start.12 = (bf16[256,768]{1,0:T(8,128)(2,1)}, bf16[256,768]{1,0:T(8,128)(2,1)}, u32[]{:S(2)}, u32[]{:S(2)}) collective-permute-start(bf16[256,768]{1,0:T(8,128)(2,1)} %collective-permute-done.8.refs_1_), channel_id=1, source_target_pairs={{0,224},{32,0},{64,32},{96,64},{128,96},{160,128},{192,160},{224,1... | collective-permute-start | bytes 1179656 | tf_op jit(solution)/shard_map/ppermute | solution.py:27
  42.2 2.6 %collective-permute-start.10 = (bf16[256,384]{1,0:T(8,128)(2,1)S(1)}, bf16[256,384]{1,0:T(8,128)(2,1)S(1)}, u32[]{:S(2)}, u32[]{:S(2)}) collective-permute-start(bf16[256,384]{1,0:T(8,128)(2,1)S(1)} %slice.17), channel_id=1, source_target_pairs={{0,24},{8,0},{16,8},{24,16},{1,25},{9,1},{17,9},{25,17},{2,26},{10... | collective-permute-start | bytes 589832 | tf_op jit(solution)/shard_map/ppermute | solution.py:27
  44.8 0.7 slice.16
  45.5 0.0 collective-permute-start.9
  45.5 0.2 copy.17.extra
  45.7 1.7 %collective-permute-done.10.far_high = bf16[256,384]{1,0:T(8,128)(2,1)S(1)} collective-permute-done((bf16[256,384]{1,0:T(8,128)(2,1)S(1)}, bf16[256,384]{1,0:T(8,128)(2,1)S(1)}, u32[]{:S(2)}, u32[]{:S(2)}) %collective-permute-start.10) | collective-permute-done | bytes 196640 | tf_op jit(solution)/shard_map/ppermute | solution.py:27
  47.4 4.4 %collective-permute-done.9.far_low = bf16[256,384]{1,0:T(8,128)(2,1)S(1)} collective-permute-done((bf16[256,384]{1,0:T(8,128)(2,1)}, bf16[256,384]{1,0:T(8,128)(2,1)S(1)}, u32[]{:S(2)}, u32[]{:S(2)}) %collective-permute-start.9) | collective-permute-done | bytes 196640 | tf_op jit(solution)/shard_map/ppermute | solution.py:27
  51.8 1.7 %shard_map.159 = (bf16[384,128]{1,0:T(8,128)(2,1)}, f32[2,384,128]{2,1,0:T(8,128)}, f32[2,384,128]{2,1,0:T(8,128)}, bf16[2,6,128,128]{3,2,1,0:T(8,128)(2,1)}, f3...) custom-call(f32[384,384]{1,0:T(8,128)S(1)} %shard_map.158.near, bf16[384,2048]{1,0:T(8,128)(2,1)S(1)} %get-tuple-element.63.normed, ...), custom_call_target="tpu_custom_call" | custom-call | flops 12000000 | tf_op jit(solution)/shard_map/pallas_call | solution.py:49
  53.5 0.0 collective-permute-done.11.refs_3_
  53.5 0.0 collective-permute-done.12.refs_2_
  53.5 0.2 collective-permute-start.16
  53.8 2.7 %collective-permute-start.17 = (bf16[256,768]{1,0:T(8,128)(2,1)}, bf16[256,768]{1,0:T(8,128)(2,1)S(1)}, u32[]{:S(2)}, u32[]{:S(2)}) collective-permute-start(bf16[256,768]{1,0:T(8,128)(2,1)} %collective-permute-done.12.refs_2_), channel_id=1, source_target_pairs={{0,224},{32,0},{64,32},{96,64},{128,96},{160,128},{192,160},{224,1... | collective-permute-start | bytes 1179656 | tf_op jit(solution)/shard_map/ppermute | solution.py:27
  56.4 0.6 collective-permute-start.14
  57.0 0.9 collective-permute-start.15
  57.9 1.7 %collective-permute-done.13.ahead = bf16[2,144,128]{2,1,0:T(8,128)(2,1)S(1)} collective-permute-done((bf16[2,144,128]{2,1,0:T(8,128)(2,1)S(1)}, bf16[2,144,128]{2,1,0:T(8,128)(2,1)S(1)}, u32[]{:S(2)}, u32[]{:S(2)}) %collective-permute-start.13) | collective-permute-done | bytes 73760 | tf_op jit(solution)/shard_map/ppermute | solution.py:27
  59.6 1.5 %collective-permute-done.14.far = bf16[2,144,128]{2,1,0:T(8,128)(2,1)S(1)} collective-permute-done((bf16[2,144,128]{2,1,0:T(8,128)(2,1)S(1)}, bf16[2,144,128]{2,1,0:T(8,128)(2,1)S(1)}, u32[]{:S(2)}, u32[]{:S(2)}) %collective-permute-start.14) | collective-permute-done | bytes 73760 | tf_op jit(solution)/shard_map/ppermute | solution.py:27
  61.1 0.9 collective-permute-done.15.behind
  62.0 1.4 %shard_map.161 = (f32[2,136,128]{2,1,0:T(8,128)}, bf16[8,144,128]{2,1,0:T(8,128)(2,1)}) custom-call(s32[4]{0:T(128)S(1)} %pad_add_fusion.place, bf16[2,144,128]{2,1,0:T(8,128)(2,1)S(1)} %get-tuple-element.66.own, bf16[2,144,128]{2,1,0:T(8,128)(2,1)S(1)} %collective-permute-done.13.ahead, bf16[2,144,128]{2,1,0:T(8,128)(2,1)S(1)} %collective-permute-done.14.far, ...), custom_call_target="tpu_custom_call" | custom-call | flops 4000000 | tf_op jit(solution)/shard_map/pallas_call | solution.py:49
  63.4 4.5 %all-to-all-start.1 = ((bf16[8,144,128]{2,1,0:T(8,128)(2,1)}), bf16[8,144,128]{2,1,0:T(8,128)(2,1)S(1)}, u32[]{:S(2)}, u32[]{:S(2)}) async-start(bf16[8,144,128]{2,1,0:T(8,128)(2,1)} %get-tuple-element.74), calls=%async_computation.1 | async-start | bytes 589824 | tf_op jit(solution)/shard_map/all_to_all | solution.py:496
  67.9 0.0 collective-permute-done.17.refs_5_
  68.0 1.5 %collective-permute-start.18 = (bf16[128,768]{1,0:T(8,128)(2,1)S(1)}, bf16[128,768]{1,0:T(8,128)(2,1)S(1)}, u32[]{:S(2)}, u32[]{:S(2)}) collective-permute-start(bf16[128,768]{1,0:T(8,128)(2,1)S(1)} %slice.14), channel_id=1, source_target_pairs={{0,32},{32,64},{64,96},{96,128},{128,160},{160,192},{192,224},{224... | collective-permute-start | bytes 589832 | tf_op jit(solution)/shard_map/ppermute | solution.py:27
  69.5 1.3 %collective-permute-start.19 = (bf16[128,768]{1,0:T(8,128)(2,1)S(1)}, bf16[128,768]{1,0:T(8,128)(2,1)S(1)}, u32[]{:S(2)}, u32[]{:S(2)}) collective-permute-start(bf16[128,768]{1,0:T(8,128)(2,1)S(1)} %slice.15), channel_id=1, source_target_pairs={{0,224},{32,0},{64,32},{96,64},{128,96},{160,128},{192,160},{224,1... | collective-permute-start | bytes 589832 | tf_op jit(solution)/shard_map/ppermute | solution.py:27
  70.8 0.8 shard_map.156.edges
  71.6 0.0 copy-start
  71.6 0.0 copy-start.3
  71.6 3.7 %shard_map.160 = (f32[384,512]{1,0:T(8,128)S(1)}, f32[32,256]{1,0:T(8,128)S(1)}, bf16[2,384,128]{2,1,0:T(8,128)(2,1)S(1)}, f32[2,384,128]{2,1,0:T(8,128)S(1)}) custom-call(s32[4]{0:T(128)S(1)} %pad_add_fusion.place, bf16[384,2048]{1,0:T(8,128)(2,1)} %get-tuple-element.54.normed, bf16[32,2048]{1,0:T(8,128)(2,1)S(1)} %shard_map.156.edges, ...), custom_call_target="tpu_custom_call" | custom-call | flops 12000000 | tf_op jit(solution)/shard_map/pallas_call | solution.py:49
  75.3 1.3 %collective-permute-done.18.refs_6_ = bf16[128,768]{1,0:T(8,128)(2,1)S(1)} collective-permute-done((bf16[128,768]{1,0:T(8,128)(2,1)S(1)}, bf16[128,768]{1,0:T(8,128)(2,1)S(1)}, u32[]{:S(2)}, u32[]{:S(2)}) %collective-permute-start.18) | collective-permute-done | bytes 196640 | tf_op jit(solution)/shard_map/ppermute | solution.py:27
  76.6 0.0 copy-start.2
  76.6 5.2 %shard_map.162 = (f32[384,128]{1,0:T(8,128)S(1)}, bf16[2,384,128]{2,1,0:T(8,128)(2,1)S(1)}, f32[384,128]{1,0:T(8,128)S(1)}, bf16[384,128]{1,0:T(8,128)(2,1)S(1)}, bf16[2048,256]{1,0:T(8,128)(2,1)S(1)}) custom-call(s32[4]{0:T(128)S(1)} %pad_add_fusion.place, bf16[384,2048]{1,0:T(8,128)(2,1)} %get-tuple-element.54.normed, ...), custom_call_target="tpu_custom_call" | custom-call | flops 2000000 | tf_op jit(solution)/shard_map/pallas_call | solution.py:49
  81.8 1.4 %shard_map.163.rec = bf16[384,128]{1,0:T(8,128)(2,1)S(1)} custom-call(s32[4]{0:T(128)S(1)} %pad_add_fusion.place, f32[384,128]{1,0:T(8,128)S(1)} %get-tuple-element.82.local, bf16[2,384,128]{2,1,0:T(8,128)(2,1)S(1)} %get-tuple-element.83.lifted, bf16[8,144,128]{2,1,0:T(8,128)(2,1)S(1)} %all-to-all-done.1.every, f32[2,136,128]{2,1,0:T(8,128)} %get-tuple-element.84.before, ...), custom_call_target="tpu_custom_call" | custom-call | flops 4000000 | tf_op jit(solution)/shard_map/pallas_call | solution.py:49
  83.2 0.5 shard_map.165
  83.7 9.2 %collective-permute-start.20 = (bf16[4,48,2048]{2,1,0:T(8,128)(2,1)S(1)}, bf16[4,48,2048]{2,1,0:T(8,128)(2,1)S(1)}, u32[]{:S(2)}, u32[]{:S(2)}) collective-permute-start(bf16[4,48,2048]{2,1,0:T(8,128)(2,1)S(1)} %shard_map.165), channel_id=1, source_target_pairs={{0,1},{1,0},{2,3},{3,2},{4,5},{5,4},{6,7},{7,6},{8,9},{9,8},{10,11... | collective-permute-start | bytes 2359304 | tf_op jit(solution)/shard_map/ppermute | solution.py:27
  92.9 0.5 shard_map.164.mine
  93.4 1.4 %collective-permute-done.20.got = bf16[4,48,2048]{2,1,0:T(8,128)(2,1)S(1)} collective-permute-done((bf16[4,48,2048]{2,1,0:T(8,128)(2,1)S(1)}, bf16[4,48,2048]{2,1,0:T(8,128)(2,1)S(1)}, u32[]{:S(2)}, u32[]{:S(2)}) %collective-permute-start.20) | collective-permute-done | bytes 786464 | tf_op jit(solution)/shard_map/ppermute | solution.py:27
  94.8 0.7 shard_map.166
  95.5 1.4 %collective-permute-start.21 = (bf16[48,1024]{1,0:T(8,128)(2,1)S(1)}, bf16[48,1024]{1,0:T(8,128)(2,1)S(1)}, u32[]{:S(2)}, u32[]{:S(2)}) collective-permute-start(bf16[48,1024]{1,0:T(8,128)(2,1)S(1)} %get-tuple-element.91), channel_id=1, source_target_pairs={{0,2},{2,4},{4,6},{6,0},{1,3},{3,5},{5,7},{7,1},{8,10},{10,12},{12... | collective-permute-start | bytes 294920 | tf_op jit(solution)/shard_map/ppermute | solution.py:27
  96.8 1.5 %collective-permute-start.22 = (bf16[48,1024]{1,0:T(8,128)(2,1)S(1)}, bf16[48,1024]{1,0:T(8,128)(2,1)S(1)}, u32[]{:S(2)}, u32[]{:S(2)}) collective-permute-start(bf16[48,1024]{1,0:T(8,128)(2,1)S(1)} %get-tuple-element.92), channel_id=1, source_target_pairs={{0,6},{2,0},{4,2},{6,4},{1,7},{3,1},{5,3},{7,5},{8,14},{10,8},{12,... | collective-permute-start | bytes 294920 | tf_op jit(solution)/shard_map/ppermute | solution.py:27
  98.4 2.5 %collective-permute-done.21.low = bf16[48,1024]{1,0:T(8,128)(2,1)S(1)} collective-permute-done((bf16[48,1024]{1,0:T(8,128)(2,1)S(1)}, bf16[48,1024]{1,0:T(8,128)(2,1)S(1)}, u32[]{:S(2)}, u32[]{:S(2)}) %collective-permute-start.21) | collective-permute-done | bytes 98336 | tf_op jit(solution)/shard_map/ppermute | solution.py:27
  100.8 0.1 shard_map.167
  100.9 0.9 collective-permute-start.23
  101.8 1.9 %collective-permute-start.24 = (bf16[48,2048]{1,0:T(8,128)(2,1)S(1)}, bf16[48,2048]{1,0:T(8,128)(2,1)S(1)}, u32[]{:S(2)}, u32[]{:S(2)}) collective-permute-start(bf16[48,2048]{1,0:T(8,128)(2,1)S(1)} %get-tuple-element.94), channel_id=1, source_target_pairs={{0,6},{2,0},{4,2},{6,4},{1,7},{3,1},{5,3},{7,5},{8,14},{10,8},{12,... | collective-permute-start | bytes 589832 | tf_op jit(solution)/shard_map/ppermute | solution.py:27
  103.7 3.7 %collective-permute-done.23 = bf16[48,2048]{1,0:T(8,128)(2,1)S(1)} collective-permute-done((bf16[48,2048]{1,0:T(8,128)(2,1)S(1)}, bf16[48,2048]{1,0:T(8,128)(2,1)S(1)}, u32[]{:S(2)}, u32[]{:S(2)}) %collective-permute-start.23) | collective-permute-done | bytes 196640 | tf_op jit(solution)/shard_map/ppermute | solution.py:27
  107.4 0.7 add_convert_fusion
  (29 shorter events, 0.1 us)
Async XLA Ops:
  0.0 18.6 %copy-start.6 = (bf16[2048]{0:T(1024)(128)(2,1)S(1)}, bf16[2048]{0:T(1024)(128)(2,1)}, u32[]{:S(2)}) copy-start(bf16[2048]{0:T(1024)(128)(2,1)} %param.17) | copy-start | bytes 12292
  2.5 23.3 %all-to-all-start = ((bf16[8,64,384]{2,1,0:T(8,128)(2,1)}), bf16[8,64,384]{2,1,0:T(8,128)(2,1)S(1)}, u32[]{:S(2)}, u32[]{:S(2)}) async-start(bf16[8,64,384]{2,1,0:T(8,128)(2,1)} %get-tuple-element.57), calls=%async_computation | async-start | bytes 786432 | tf_op jit(solution)/shard_map/all_to_all | solution.py:428
  11.5 16.9 %collective-permute-start = (bf16[64,768]{1,0:T(8,128)(2,1)S(1)}, bf16[64,768]{1,0:T(8,128)(2,1)S(1)}, u32[]{:S(2)}, u32[]{:S(2)}) collective-permute-start(bf16[64,768]{1,0:T(8,128)(2,1)S(1)} %get-tuple-element.58.own), channel_id=1, source_target_pairs={{0,24},{8,0},{16,8},{24,16},{1,25},{9,1},{17,9},{25,17},{2,26},{10... | collective-permute-start | bytes 294920 | tf_op jit(solution)/shard_map/ppermute | solution.py:27
  14.0 14.5 %collective-permute-start.1 = (bf16[64,768]{1,0:T(8,128)(2,1)S(1)}, bf16[64,768]{1,0:T(8,128)(2,1)S(1)}, u32[]{:S(2)}, u32[]{:S(2)}) collective-permute-start(bf16[64,768]{1,0:T(8,128)(2,1)S(1)} %get-tuple-element.58.own), channel_id=1, source_target_pairs={{0,16},{8,24},{16,0},{24,8},{1,17},{9,25},{17,1},{25,9},{2,18},{10... | collective-permute-start | bytes 294920 | tf_op jit(solution)/shard_map/ppermute | solution.py:27
  14.5 14.0 %collective-permute-start.2 = (bf16[64,768]{1,0:T(8,128)(2,1)S(1)}, bf16[64,768]{1,0:T(8,128)(2,1)S(1)}, u32[]{:S(2)}, u32[]{:S(2)}) collective-permute-start(bf16[64,768]{1,0:T(8,128)(2,1)S(1)} %get-tuple-element.58.own), channel_id=1, source_target_pairs={{0,8},{8,16},{16,24},{24,0},{1,9},{9,17},{17,25},{25,1},{2,10},{10... | collective-permute-start | bytes 294920 | tf_op jit(solution)/shard_map/ppermute | solution.py:27
  15.1 11.9 %collective-permute-start.3 = (bf16[16,2048]{1,0:T(8,128)(2,1)S(1)}, bf16[16,2048]{1,0:T(8,128)(2,1)S(1)}, u32[]{:S(2)}, u32[]{:S(2)}) collective-permute-start(bf16[16,2048]{1,0:T(8,128)(2,1)S(1)} %get-tuple-element.53), channel_id=1, source_target_pairs={{0,8},{8,16},{16,24},{24,32},{32,40},{40,48},{48,56},{56,64},{64,7... | collective-permute-start | bytes 196616 | tf_op jit(solution)/shard_map/ppermute | solution.py:33
  25.8 12.4 %collective-permute-start.6 = (bf16[512,384]{1,0:T(8,128)(2,1)S(1)}, bf16[512,384]{1,0:T(8,128)(2,1)S(1)}, u32[]{:S(2)}, u32[]{:S(2)}) collective-permute-start(bf16[512,384]{1,0:T(8,128)(2,1)S(1)} %bitcast.11), channel_id=1, source_target_pairs={{0,8},{8,16},{16,24},{24,0},{1,9},{9,17},{17,25},{25,1},{2,10},{10... | collective-permute-start | bytes 1179656 | tf_op jit(solution)/shard_map/ppermute | solution.py:27
  27.0 11.2 %collective-permute-start.5 = (bf16[512,384]{1,0:T(8,128)(2,1)S(1)}, bf16[512,384]{1,0:T(8,128)(2,1)S(1)}, u32[]{:S(2)}, u32[]{:S(2)}) collective-permute-start(bf16[512,384]{1,0:T(8,128)(2,1)S(1)} %bitcast.12), channel_id=1, source_target_pairs={{0,24},{8,0},{16,8},{24,16},{1,25},{9,1},{17,9},{25,17},{2,26},{10... | collective-permute-start | bytes 1179656 | tf_op jit(solution)/shard_map/ppermute | solution.py:27
  29.2 10.3 %collective-permute-start.7 = (bf16[256,768]{1,0:T(8,128)(2,1)}, bf16[256,768]{1,0:T(8,128)(2,1)}, u32[]{:S(2)}, u32[]{:S(2)}) collective-permute-start(bf16[256,768]{1,0:T(8,128)(2,1)} %shard_map.157.refs_0_), channel_id=1, source_target_pairs={{0,32},{32,64},{64,96},{96,128},{128,160},{160,192},{192,224},{224... | collective-permute-start | bytes 1179656 | tf_op jit(solution)/shard_map/ppermute | solution.py:27
  29.2 10.3 %collective-permute-start.8 = (bf16[256,768]{1,0:T(8,128)(2,1)}, bf16[256,768]{1,0:T(8,128)(2,1)}, u32[]{:S(2)}, u32[]{:S(2)}) collective-permute-start(bf16[256,768]{1,0:T(8,128)(2,1)} %shard_map.157.refs_0_), channel_id=1, source_target_pairs={{0,224},{32,0},{64,32},{96,64},{128,96},{160,128},{192,160},{224,1... | collective-permute-start | bytes 1179656 | tf_op jit(solution)/shard_map/ppermute | solution.py:27
  31.9 13.6 %copy-start.7 = (f32[2,384,1]{1,2,0:T(1,128)S(1)}, f32[2,384,1]{1,2,0:T(1,128)}, u32[]{:S(2)}) copy-start(f32[2,384,1]{1,2,0:T(1,128)} %param.26) | copy-start | bytes 9220
  31.9 19.9 %copy-start.1 = (f32[2,128]{1,0:T(2,128)S(1)}, f32[2,128]{1,0:T(2,128)}, u32[]{:S(2)}) copy-start(f32[2,128]{1,0:T(2,128)} %slack.1) | copy-start | bytes 3076
  31.9 6.2 %collective-permute-start.4 = (bf16[16,2048]{1,0:T(8,128)(2,1)S(1)}, bf16[16,2048]{1,0:T(8,128)(2,1)S(1)}, u32[]{:S(2)}, u32[]{:S(2)}) collective-permute-start(bf16[16,2048]{1,0:T(8,128)(2,1)S(1)} %get-tuple-element.56), channel_id=1, source_target_pairs={{8,0},{16,8},{24,16},{32,24},{40,32},{48,40},{56,48},{64,56},{72,6... | collective-permute-start | bytes 196616 | tf_op jit(solution)/shard_map/ppermute | solution.py:33
  39.5 14.0 %collective-permute-start.11 = (bf16[256,768]{1,0:T(8,128)(2,1)}, bf16[256,768]{1,0:T(8,128)(2,1)}, u32[]{:S(2)}, u32[]{:S(2)}) collective-permute-start(bf16[256,768]{1,0:T(8,128)(2,1)} %collective-permute-done.7.refs_4_), channel_id=1, source_target_pairs={{0,32},{32,64},{64,96},{96,128},{128,160},{160,192},{192,224},{224... | collective-permute-start | bytes 1179656 | tf_op jit(solution)/shard_map/ppermute | solution.py:27
  39.5 14.0 %collective-permute-start.12 = (bf16[256,768]{1,0:T(8,128)(2,1)}, bf16[256,768]{1,0:T(8,128)(2,1)}, u32[]{:S(2)}, u32[]{:S(2)}) collective-permute-start(bf16[256,768]{1,0:T(8,128)(2,1)} %collective-permute-done.8.refs_1_), channel_id=1, source_target_pairs={{0,224},{32,0},{64,32},{96,64},{128,96},{160,128},{192,160},{224,1... | collective-permute-start | bytes 1179656 | tf_op jit(solution)/shard_map/ppermute | solution.py:27
  42.2 5.2 %collective-permute-start.10 = (bf16[256,384]{1,0:T(8,128)(2,1)S(1)}, bf16[256,384]{1,0:T(8,128)(2,1)S(1)}, u32[]{:S(2)}, u32[]{:S(2)}) collective-permute-start(bf16[256,384]{1,0:T(8,128)(2,1)S(1)} %slice.17), channel_id=1, source_target_pairs={{0,24},{8,0},{16,8},{24,16},{1,25},{9,1},{17,9},{25,17},{2,26},{10... | collective-permute-start | bytes 589832 | tf_op jit(solution)/shard_map/ppermute | solution.py:27
  45.5 6.3 %collective-permute-start.9 = (bf16[256,384]{1,0:T(8,128)(2,1)}, bf16[256,384]{1,0:T(8,128)(2,1)S(1)}, u32[]{:S(2)}, u32[]{:S(2)}) collective-permute-start(bf16[256,384]{1,0:T(8,128)(2,1)} %slice.16), channel_id=1, source_target_pairs={{0,8},{8,16},{16,24},{24,0},{1,9},{9,17},{17,25},{25,1},{2,10},{10... | collective-permute-start | bytes 589832 | tf_op jit(solution)/shard_map/ppermute | solution.py:27
  53.5 14.4 %collective-permute-start.16 = (bf16[256,768]{1,0:T(8,128)(2,1)}, bf16[256,768]{1,0:T(8,128)(2,1)S(1)}, u32[]{:S(2)}, u32[]{:S(2)}) collective-permute-start(bf16[256,768]{1,0:T(8,128)(2,1)} %collective-permute-done.11.refs_3_), channel_id=1, source_target_pairs={{0,32},{32,64},{64,96},{96,128},{128,160},{160,192},{192,224},{224... | collective-permute-start | bytes 1179656 | tf_op jit(solution)/shard_map/ppermute | solution.py:27
  53.8 14.1 %collective-permute-start.17 = (bf16[256,768]{1,0:T(8,128)(2,1)}, bf16[256,768]{1,0:T(8,128)(2,1)S(1)}, u32[]{:S(2)}, u32[]{:S(2)}) collective-permute-start(bf16[256,768]{1,0:T(8,128)(2,1)} %collective-permute-done.12.refs_2_), channel_id=1, source_target_pairs={{0,224},{32,0},{64,32},{96,64},{128,96},{160,128},{192,160},{224,1... | collective-permute-start | bytes 1179656 | tf_op jit(solution)/shard_map/ppermute | solution.py:27
  56.4 3.2 %collective-permute-start.13 = (bf16[2,144,128]{2,1,0:T(8,128)(2,1)S(1)}, bf16[2,144,128]{2,1,0:T(8,128)(2,1)S(1)}, u32[]{:S(2)}, u32[]{:S(2)}) collective-permute-start(bf16[2,144,128]{2,1,0:T(8,128)(2,1)S(1)} %get-tuple-element.66.own), channel_id=1, source_target_pairs={{0,24},{8,0},{16,8},{24,16},{1,25},{9,1},{17,9},{25,17},{2,26},{10... | collective-permute-start | bytes 221192 | tf_op jit(solution)/shard_map/ppermute | solution.py:27
  56.4 4.7 %collective-permute-start.14 = (bf16[2,144,128]{2,1,0:T(8,128)(2,1)S(1)}, bf16[2,144,128]{2,1,0:T(8,128)(2,1)S(1)}, u32[]{:S(2)}, u32[]{:S(2)}) collective-permute-start(bf16[2,144,128]{2,1,0:T(8,128)(2,1)S(1)} %get-tuple-element.66.own), channel_id=1, source_target_pairs={{0,16},{8,24},{16,0},{24,8},{1,17},{9,25},{17,1},{25,9},{2,18},{10... | collective-permute-start | bytes 221192 | tf_op jit(solution)/shard_map/ppermute | solution.py:27
  57.0 5.0 %collective-permute-start.15 = (bf16[2,144,128]{2,1,0:T(8,128)(2,1)S(1)}, bf16[2,144,128]{2,1,0:T(8,128)(2,1)S(1)}, u32[]{:S(2)}, u32[]{:S(2)}) collective-permute-start(bf16[2,144,128]{2,1,0:T(8,128)(2,1)S(1)} %get-tuple-element.66.own), channel_id=1, source_target_pairs={{0,8},{8,16},{16,24},{24,0},{1,9},{9,17},{17,25},{25,1},{2,10},{10... | collective-permute-start | bytes 221192 | tf_op jit(solution)/shard_map/ppermute | solution.py:27
  63.4 18.4 %all-to-all-start.1 = ((bf16[8,144,128]{2,1,0:T(8,128)(2,1)}), bf16[8,144,128]{2,1,0:T(8,128)(2,1)S(1)}, u32[]{:S(2)}, u32[]{:S(2)}) async-start(bf16[8,144,128]{2,1,0:T(8,128)(2,1)} %get-tuple-element.74), calls=%async_computation.1 | async-start | bytes 589824 | tf_op jit(solution)/shard_map/all_to_all | solution.py:496
  67.9 7.4 %copy-start.4 = (bf16[256,768]{1,0:T(8,128)(2,1)}, bf16[256,768]{1,0:T(8,128)(2,1)S(1)}, u32[]{:S(2)}) copy-start(bf16[256,768]{1,0:T(8,128)(2,1)S(1)} %collective-permute-done.16.refs_8_) | copy-start | bytes 1179652
  67.9 7.4 %copy-start.5 = (bf16[256,768]{1,0:T(8,128)(2,1)}, bf16[256,768]{1,0:T(8,128)(2,1)S(1)}, u32[]{:S(2)}) copy-start(bf16[256,768]{1,0:T(8,128)(2,1)S(1)} %collective-permute-done.17.refs_5_) | copy-start | bytes 1179652
  68.0 8.6 %collective-permute-start.18 = (bf16[128,768]{1,0:T(8,128)(2,1)S(1)}, bf16[128,768]{1,0:T(8,128)(2,1)S(1)}, u32[]{:S(2)}, u32[]{:S(2)}) collective-permute-start(bf16[128,768]{1,0:T(8,128)(2,1)S(1)} %slice.14), channel_id=1, source_target_pairs={{0,32},{32,64},{64,96},{96,128},{128,160},{160,192},{192,224},{224... | collective-permute-start | bytes 589832 | tf_op jit(solution)/shard_map/ppermute | solution.py:27
  69.5 7.1 %collective-permute-start.19 = (bf16[128,768]{1,0:T(8,128)(2,1)S(1)}, bf16[128,768]{1,0:T(8,128)(2,1)S(1)}, u32[]{:S(2)}, u32[]{:S(2)}) collective-permute-start(bf16[128,768]{1,0:T(8,128)(2,1)S(1)} %slice.15), channel_id=1, source_target_pairs={{0,224},{32,0},{64,32},{96,64},{128,96},{160,128},{192,160},{224,1... | collective-permute-start | bytes 589832 | tf_op jit(solution)/shard_map/ppermute | solution.py:27
  71.6 5.0 %copy-start = (bf16[31,128]{1,0:T(8,128)(2,1)S(1)}, bf16[31,128]{1,0:T(8,128)(2,1)}, u32[]{:S(2)}) copy-start(bf16[31,128]{1,0:T(8,128)(2,1)} %refs_14_.1) | copy-start | bytes 23812
  71.6 5.0 %copy-start.3 = (bf16[128]{0:T(256)(128)(2,1)S(1)}, bf16[128]{0:T(256)(128)(2,1)}, u32[]{:S(2)}) copy-start(bf16[128]{0:T(256)(128)(2,1)} %param.29) | copy-start | bytes 772
  76.6 5.2 %copy-start.2 = (bf16[128]{0:T(256)(128)(2,1)S(1)}, bf16[128]{0:T(256)(128)(2,1)}, u32[]{:S(2)}) copy-start(bf16[128]{0:T(256)(128)(2,1)} %param.27) | copy-start | bytes 772
  83.7 11.1 %collective-permute-start.20 = (bf16[4,48,2048]{2,1,0:T(8,128)(2,1)S(1)}, bf16[4,48,2048]{2,1,0:T(8,128)(2,1)S(1)}, u32[]{:S(2)}, u32[]{:S(2)}) collective-permute-start(bf16[4,48,2048]{2,1,0:T(8,128)(2,1)S(1)} %shard_map.165), channel_id=1, source_target_pairs={{0,1},{1,0},{2,3},{3,2},{4,5},{5,4},{6,7},{7,6},{8,9},{9,8},{10,11... | collective-permute-start | bytes 2359304 | tf_op jit(solution)/shard_map/ppermute | solution.py:27
  95.5 5.4 %collective-permute-start.21 = (bf16[48,1024]{1,0:T(8,128)(2,1)S(1)}, bf16[48,1024]{1,0:T(8,128)(2,1)S(1)}, u32[]{:S(2)}, u32[]{:S(2)}) collective-permute-start(bf16[48,1024]{1,0:T(8,128)(2,1)S(1)} %get-tuple-element.91), channel_id=1, source_target_pairs={{0,2},{2,4},{4,6},{6,0},{1,3},{3,5},{5,7},{7,1},{8,10},{10,12},{12... | collective-permute-start | bytes 294920 | tf_op jit(solution)/shard_map/ppermute | solution.py:27
  96.8 4.0 %collective-permute-start.22 = (bf16[48,1024]{1,0:T(8,128)(2,1)S(1)}, bf16[48,1024]{1,0:T(8,128)(2,1)S(1)}, u32[]{:S(2)}, u32[]{:S(2)}) collective-permute-start(bf16[48,1024]{1,0:T(8,128)(2,1)S(1)} %get-tuple-element.92), channel_id=1, source_target_pairs={{0,6},{2,0},{4,2},{6,4},{1,7},{3,1},{5,3},{7,5},{8,14},{10,8},{12,... | collective-permute-start | bytes 294920 | tf_op jit(solution)/shard_map/ppermute | solution.py:27
  100.9 6.5 %collective-permute-start.23 = (bf16[48,2048]{1,0:T(8,128)(2,1)S(1)}, bf16[48,2048]{1,0:T(8,128)(2,1)S(1)}, u32[]{:S(2)}, u32[]{:S(2)}) collective-permute-start(bf16[48,2048]{1,0:T(8,128)(2,1)S(1)} %get-tuple-element.93), channel_id=1, source_target_pairs={{0,2},{2,4},{4,6},{6,0},{1,3},{3,5},{5,7},{7,1},{8,10},{10,12},{12... | collective-permute-start | bytes 589832 | tf_op jit(solution)/shard_map/ppermute | solution.py:27
  101.8 5.6 %collective-permute-start.24 = (bf16[48,2048]{1,0:T(8,128)(2,1)S(1)}, bf16[48,2048]{1,0:T(8,128)(2,1)S(1)}, u32[]{:S(2)}, u32[]{:S(2)}) collective-permute-start(bf16[48,2048]{1,0:T(8,128)(2,1)S(1)} %get-tuple-element.94), channel_id=1, source_target_pairs={{0,6},{2,0},{4,2},{6,4},{1,7},{3,1},{5,3},{7,5},{8,14},{10,8},{12,... | collective-permute-start | bytes 589832 | tf_op jit(solution)/shard_map/ppermute | solution.py:27

commit v3 on v2

--- a/solution.py
+++ b/solution.py
@@ -73,21 +73,23 @@
     return jnp.dot(a, b, preferred_element_type=F32)
 
 
+def collect_first_kernel(a, b, c, first):
+    for k, ref in enumerate((a, b, c)):
+        for z in range(8):
+            first[z, :, k * HEAD : (k + 1) * HEAD] = ref[...]
+
+
 def collect_kernel(x, *refs):
-    first, later, top, bottom, done = refs[-5:]
+    later, top, bottom, done = refs[-4:]
     edge = top.shape[0]
-    rows = (x.at[:edge], x.at[x.shape[0] - edge :])
+    pairs = [(x.at[:edge], top), (x.at[x.shape[0] - edge :], bottom)]
+    for k, ref in enumerate(refs[:-4]):
+        pairs.append((ref, later.at[:, k * HEAD : (k + 1) * HEAD]))
     copies = [
-        pltpu.make_async_copy(source, into, done.at[k])
-        for k, (source, into) in enumerate(zip(rows, (top, bottom)))
+        pltpu.make_async_copy(source, into, done.at[k]) for k, (source, into) in enumerate(pairs)
     ]
     for copy in copies:
         copy.start()
-    for k, ref in enumerate(refs[:3]):
-        for z in range(8):
-            first[z, :, k * HEAD : (k + 1) * HEAD] = ref[...]
-    for k, ref in enumerate(refs[3:-5]):
-        later[:, k * HEAD : (k + 1) * HEAD] = ref[...]
     for copy in copies:
         copy.wait()
 
@@ -346,30 +348,27 @@
 
 
 def project_out_kernel(place, rec, conv, columns, out):
-    core = place[0]
-    at = [pl.multiple_of(k * 96 + core * 48, 16) for k in range(4)]
+    core, first = place[0], place[1]
+    count = out.shape[0]
+    at = [pl.multiple_of(lax.rem(first + k, 4) * 96 + core * 48, 16) for k in range(count)]
     left = jnp.concatenate([rec[pl.ds(k, 48)] for k in at], axis=0)
     right = jnp.concatenate([conv[pl.ds(k, 48)] for k in at], axis=0)
     rows = jnp.concatenate([left, right], axis=1)
     for c in range(0, 2048, 512):
         part = nt(rows, columns[c : c + 512])
-        for k in range(4):
+        for k in range(count):
             out[k, :, c : c + 512] = part[k * 48 : (k + 1) * 48].astype(out.dtype)
 
 
-def meet_kernel(place, mine, got, far_low, far_high, ahead, behind, own):
-    y = place[3]
-
-    def block(step):
-        k = lax.rem(y + step, 4)
-        return mine[k] + got[k].astype(F32)
-
-    far = block(2)
-    far_low[...] = far[:, :1024].astype(BF)
-    far_high[...] = far[:, 1024:].astype(BF)
-    ahead[...] = block(1)
-    behind[...] = block(3)
-    own[...] = block(0)
+def meet_far_kernel(mine, got, far_low, far_high):
+    far_low[...] = (mine[0, :, :1024] + got[0, :, :1024].astype(F32)).astype(BF)
+    far_high[...] = (mine[0, :, 1024:] + got[0, :, 1024:].astype(F32)).astype(BF)
+
+
+def meet_kernel(mine, got, ahead, behind, own):
+    behind[...] = mine[1] + got[0].astype(F32)
+    own[...] = mine[2] + got[1].astype(F32)
+    ahead[...] = mine[3] + got[2].astype(F32)
 
 
 def relay_kernel(ahead, behind, low, high, ahead_o, behind_o):
@@ -403,17 +402,22 @@
     gain = entry_rescale_vector[None]
     place = jnp.stack([z, lax.rem(4 - x, 4) * 64, x, y]).astype(jnp.int32)
     edge = pltpu.VMEM((16, sequence_embeddings.shape[1]), BF)
-    first, shard, top, bottom = kernel_call(
+    (first,) = kernel_call(
+        collect_first_kernel,
+        1,
+        [pltpu.HBM((8, 64, 384), BF)],
+        far_off(onward_retain_matrix),
+        far_off(reverse_retain_matrix),
+        far_off(content_matrix),
+    )
+    shard, top, bottom = kernel_call(
         collect_kernel,
-        2,
-        [pltpu.VMEM((8, 64, 384), BF), pltpu.VMEM((64, 768), BF), edge, edge],
+        1,
+        [pltpu.VMEM((64, 768), BF), edge, edge],
         far_off(sequence_embeddings),
         *(
             far_off(weight)
             for weight in (
-                onward_retain_matrix,
-                reverse_retain_matrix,
-                content_matrix,
                 probe_matrix,
                 emission_switch_matrix,
                 pointwise_content_matrix,
@@ -422,17 +426,16 @@
                 filter_readout_matrix.T,
             )
         ),
-        scratch=(pltpu.SemaphoreType.DMA((2,)),),
-        left=(0,),
+        scratch=(pltpu.SemaphoreType.DMA((8,)),),
+        left=range(7),
     )
     first = lax.all_to_all(first, "z", 0, 0, tiled=True)
     first = first.reshape(512, 384)
     ahead, far, behind = shift(shard, "x", -1), shift(shard, "x", 2), shift(shard, "x", 1)
     normed, normed_first = normalized(place, far_off(sequence_embeddings), gain, 2)
-    low = line(bottom, ("z", "x"), 1)
-    high = line(top, ("z", "x"), -1)
-    normed, normed_first, shard, ahead, far, behind, low = lax.optimization_barrier(
-        (normed, normed_first, shard, ahead, far, behind, low)
+    low, high = line(bottom, ("z", "x"), 1), line(top, ("z", "x"), -1)
+    normed, normed_first, shard, ahead, far, behind = lax.optimization_barrier(
+        (normed, normed_first, shard, ahead, far, behind)
     )
     (edges,) = normalized(place, jnp.concatenate([low, high], axis=0), gain, 1)
     (later,) = kernel_call(
@@ -449,7 +452,7 @@
     up1, down1 = shift(later, "z", 1), shift(later, "z", -1)
     far_low, far_high = shift(behind[:256], "x", 1), shift(ahead[256:], "x", -1)
     normed_first = keep(normed_first)
-    _, seen = ordered(high, behind)
+    _, _, seen = ordered(low, high, behind)
     (near,) = kernel_call(
         near_scores_kernel,
         2,
@@ -563,39 +566,32 @@
         subspace_rescale[None],
         keep(gate),
     )
-    theirs, mine = (
-        kernel_call(
+
+    def projected(side, first, count, kind):
+        spot = jnp.stack([side, lax.rem(y + first, 4)]).astype(jnp.int32)
+        return kernel_call(
             project_out_kernel,
-            1,
-            [pltpu.VMEM((4, 48, 2048), kind)],
-            side[None].astype(jnp.int32),
+            count / 4,
+            [pltpu.VMEM((count, 48, 2048), kind)],
+            spot,
             keep(rec_out),
             keep(conv_out),
             keep(columns),
         )[0]
-        for side, kind in ((1 - core, BF), (core, F32))
-    )
+
     half, whole, final = (
         pltpu.VMEM((48, 1024), BF),
         pltpu.VMEM((48, 2048), F32),
         pltpu.VMEM((48, 2048), BF),
     )
-    far_low, far_high, ahead, behind, own = kernel_call(
-        meet_kernel,
-        1,
-        [half, half, whole, whole, whole],
-        place,
-        keep(mine),
-        keep(shift(theirs, "core", 1)),
-    )
+    far_got = shift(projected(1 - core, 2, 1, BF), "core", 1)
+    rest_got = shift(projected(1 - core, 3, 3, BF), "core", 1)
+    mine = keep(projected(core, 2, 4, F32))
+    far_low, far_high = kernel_call(meet_far_kernel, 0.3, [half, half], mine, keep(far_got))
+    low, high = shift(far_low, "y", 1), shift(far_high, "y", -1)
+    ahead, behind, own = kernel_call(meet_kernel, 1, [whole, whole, whole], mine, keep(rest_got))
     ahead, behind = kernel_call(
-        relay_kernel,
-        0.5,
-        [final, final],
-        keep(ahead),
-        keep(behind),
-        keep(shift(far_low, "y", 1)),
-        keep(shift(far_high, "y", -1)),
+        relay_kernel, 0.5, [final, final], keep(ahead), keep(behind), keep(low), keep(high)
     )
     ahead, behind = shift(ahead, "y", 1), shift(behind, "y", -1)
     return (own + ahead.astype(F32) + behind.astype(F32)).astype(BF)

time: 109 us -> 113 us (1.037)
  waiting for transfers between devices: 27.4 us -> 29.8 us
  Pallas kernels: 24.1 us -> 25.7 us
    all_to_all x1, waiting for transfers between devices: 2.8 us -> 5.2 us  [layer(): first = lax.all_to_all(first, 'z', 0, 0, tiled=True)]
    ppermute x23 -> x24, starting transfers between devices: 36.2 us -> 38.5 us  [shift(): return lax.ppermute(array, axis, ring(lax.axis_size(axis), step))]
    ppermute x23 -> x24, waiting for transfers between devices: 19.8 us -> 17.9 us  [shift(): return lax.ppermute(array, axis, ring(lax.axis_size(axis), step))]
    ppermute x2, waiting for transfers between devices: 4.81 us -> 6.66 us  [line(): return lax.ppermute(array, axes, pairs)]
    pallas_call x14 -> x17, Pallas kernels: 24.1 us -> 25.7 us  [kernel_call(): pl.pallas_call(body, out_shape=tuple(outs), in_specs=[SMEM if o.dtype ==...]
    ppermute x2, starting transfers between devices: 4.83 us -> 3.31 us  [line(): return lax.ppermute(array, axes, pairs)]
  transfers between devices with their start and end apart: 27 -> 28, of which waited for: 12 -> 12; matrix products, arithmetic and copies ran while one was open for 1% -> 1% of each run, Pallas kernels for 18% -> 19%
where the time goes in v3:
time: 113 us; the launch traced here: 112 us
  starting transfers between devices  54.2 us (48%)
  waiting for transfers between devices  29.8 us (26%)
  Pallas kernels  25.7 us (23%)
    ppermute x24, starting transfers between devices, shift(): return lax.ppermute(array, axis, ring(lax.axis_size(axis), step))  38.5 us
    pallas_call x17, Pallas kernels, kernel_call(): pl.pallas_call(body, out_shape=tuple(outs), in_specs=[SMEM if o.dtype ==...  25.7 us
    ppermute x24, waiting for transfers between devices, shift(): return lax.ppermute(array, axis, ring(lax.axis_size(axis), step))  17.9 us
    all_to_all x1, starting transfers between devices, layer(): first = lax.all_to_all(first, 'z', 0, 0, tiled=True)  9 us
    ppermute x2, waiting for transfers between devices, line(): return lax.ppermute(array, axes, pairs)  6.66 us
    all_to_all x1, waiting for transfers between devices, layer(): first = lax.all_to_all(first, 'z', 0, 0, tiled=True)  5.2 us
    all_to_all x1, starting transfers between devices, layer(): every = lax.all_to_all(send, 'z', 0, 0, tiled=True)  3.42 us
    ppermute x2, starting transfers between devices, line(): return lax.ppermute(array, axes, pairs)  3.31 us
  transfers between devices with their start and end apart: 28, of which 12 were waited for; matrix products, arithmetic and copies ran while one was open for 1% of the time, Pallas kernels for 19%

profile of v3, /device:TPU:1, one launch (start us, length us, event | category | flops | bytes accessed | tf_op | source)
XLA Modules:
  0.0 112.0 jit_solution(7498462166182979072)
XLA Ops:
  0.0 1.6 %shard_map.157 = bf16[8,64,384]{2,1,0:T(8,128)(2,1)} custom-call(bf16[64,128]{1,0:T(8,128)(2,1)} %a.1, bf16[64,128]{1,0:T(8,128)(2,1)} %b.1, bf16[64,128]{1,0:T(8,128)(2,1)} %c.1), custom_call_target="tpu_custom_call" | custom-call | flops 4000000 | tf_op jit(solution)/shard_map/pallas_call | solution.py:49
  1.6 9.0 %all-to-all-start = ((bf16[8,64,384]{2,1,0:T(8,128)(2,1)}), bf16[8,64,384]{2,1,0:T(8,128)(2,1)S(1)}, u32[]{:S(2)}, u32[]{:S(2)}) async-start(bf16[8,64,384]{2,1,0:T(8,128)(2,1)} %shard_map.157), calls=%async_computation | async-start | bytes 786432 | tf_op jit(solution)/shard_map/all_to_all | solution.py:432
  10.6 0.9 shard_map.155
  11.5 2.6 %collective-permute-start = (bf16[64,768]{1,0:T(8,128)(2,1)S(1)}, bf16[64,768]{1,0:T(8,128)(2,1)S(1)}, u32[]{:S(2)}, u32[]{:S(2)}) collective-permute-start(bf16[64,768]{1,0:T(8,128)(2,1)S(1)} %get-tuple-element.54.own), channel_id=1, source_target_pairs={{0,24},{8,0},{16,8},{24,16},{1,25},{9,1},{17,9},{25,17},{2,26},{10... | collective-permute-start | bytes 294920 | tf_op jit(solution)/shard_map/ppermute | solution.py:27
  14.1 0.5 collective-permute-start.1
  14.6 0.6 collective-permute-start.2
  15.2 0.1 pad_add_fusion.1.place
  15.3 4.3 %shard_map.154 = (bf16[384,2048]{1,0:T(8,128)(2,1)}, bf16[384,2048]{1,0:T(8,128)(2,1)S(1)}) custom-call(s32[4]{0:T(128)S(1)} %pad_add_fusion.1.place, bf16[384,2048]{1,0:T(8,128)(2,1)} %x.3, bf16[1,2048]{1,0:T(2,128)(2,1)S(1)} %broadcast_in_dim.9.gain), custom_call_target="tpu_custom_call" | custom-call | flops 12000000 | tf_op jit(solution)/shard_map/pallas_call | solution.py:49
  19.6 5.2 %all-to-all-done = bf16[8,64,384]{2,1,0:T(8,128)(2,1)S(1)} async-done(((bf16[8,64,384]{2,1,0:T(8,128)(2,1)}), bf16[8,64,384]{2,1,0:T(8,128)(2,1)S(1)}, u32[]{:S(2)}, u32[]{:S(2)}) %all-to-all-start) | async-done | bytes 393248 | tf_op jit(solution)/shard_map/all_to_all | solution.py:432
  24.8 1.2 %collective-permute-start.6 = (bf16[512,384]{1,0:T(8,128)(2,1)S(1)}, bf16[512,384]{1,0:T(8,128)(2,1)S(1)}, u32[]{:S(2)}, u32[]{:S(2)}) collective-permute-start(bf16[512,384]{1,0:T(8,128)(2,1)S(1)} %bitcast.13), channel_id=1, source_target_pairs={{0,8},{8,16},{16,24},{24,0},{1,9},{9,17},{17,25},{25,1},{2,10},{10... | collective-permute-start | bytes 1179656 | tf_op jit(solution)/shard_map/ppermute | solution.py:27
  26.0 1.5 %collective-permute-start.5 = (bf16[512,384]{1,0:T(8,128)(2,1)S(1)}, bf16[512,384]{1,0:T(8,128)(2,1)S(1)}, u32[]{:S(2)}, u32[]{:S(2)}) collective-permute-start(bf16[512,384]{1,0:T(8,128)(2,1)S(1)} %bitcast.14), channel_id=1, source_target_pairs={{0,24},{8,0},{16,8},{24,16},{1,25},{9,1},{17,9},{25,17},{2,26},{10... | collective-permute-start | bytes 1179656 | tf_op jit(solution)/shard_map/ppermute | solution.py:27
  27.5 0.0 collective-permute-done.ahead
  27.5 0.0 collective-permute-done.1.far
  27.5 0.8 shard_map.158.refs_0_
  28.3 2.7 %collective-permute-start.8 = (bf16[256,768]{1,0:T(8,128)(2,1)}, bf16[256,768]{1,0:T(8,128)(2,1)}, u32[]{:S(2)}, u32[]{:S(2)}) collective-permute-start(bf16[256,768]{1,0:T(8,128)(2,1)} %shard_map.158.refs_0_), channel_id=1, source_target_pairs={{0,224},{32,0},{64,32},{96,64},{128,96},{160,128},{192,160},{224,1... | collective-permute-start | bytes 1179656 | tf_op jit(solution)/shard_map/ppermute | solution.py:27
  31.0 1.9 %collective-permute-start.3 = (bf16[16,2048]{1,0:T(8,128)(2,1)S(1)}, bf16[16,2048]{1,0:T(8,128)(2,1)S(1)}, u32[]{:S(2)}, u32[]{:S(2)}) collective-permute-start(bf16[16,2048]{1,0:T(8,128)(2,1)S(1)} %get-tuple-element.52), channel_id=1, source_target_pairs={{0,8},{8,16},{16,24},{24,32},{32,40},{40,48},{48,56},{56,64},{64,7... | collective-permute-start | bytes 196616 | tf_op jit(solution)/shard_map/ppermute | solution.py:33
  32.9 1.9 %collective-permute-done.3 = bf16[16,2048]{1,0:T(8,128)(2,1)S(1)} collective-permute-done((bf16[16,2048]{1,0:T(8,128)(2,1)S(1)}, bf16[16,2048]{1,0:T(8,128)(2,1)S(1)}, u32[]{:S(2)}, u32[]{:S(2)}) %collective-permute-start.3) | collective-permute-done | bytes 65568 | tf_op jit(solution)/shard_map/ppermute | solution.py:33
  34.8 1.4 %collective-permute-start.4 = (bf16[16,2048]{1,0:T(8,128)(2,1)S(1)}, bf16[16,2048]{1,0:T(8,128)(2,1)S(1)}, u32[]{:S(2)}, u32[]{:S(2)}) collective-permute-start(bf16[16,2048]{1,0:T(8,128)(2,1)S(1)} %get-tuple-element.53), channel_id=1, source_target_pairs={{8,0},{16,8},{24,16},{32,24},{40,32},{48,40},{56,48},{64,56},{72,6... | collective-permute-start | bytes 196616 | tf_op jit(solution)/shard_map/ppermute | solution.py:33
  36.2 4.8 %collective-permute-done.4 = bf16[16,2048]{1,0:T(8,128)(2,1)S(1)} collective-permute-done((bf16[16,2048]{1,0:T(8,128)(2,1)S(1)}, bf16[16,2048]{1,0:T(8,128)(2,1)S(1)}, u32[]{:S(2)}, u32[]{:S(2)}) %collective-permute-start.4) | collective-permute-done | bytes 65568 | tf_op jit(solution)/shard_map/ppermute | solution.py:33
  41.0 0.8 shard_map.159.near
  41.8 3.3 %collective-permute-start.11 = (bf16[256,768]{1,0:T(8,128)(2,1)}, bf16[256,768]{1,0:T(8,128)(2,1)}, u32[]{:S(2)}, u32[]{:S(2)}) collective-permute-start(bf16[256,768]{1,0:T(8,128)(2,1)} %collective-permute-done.7.refs_4_), channel_id=1, source_target_pairs={{0,32},{32,64},{64,96},{96,128},{128,160},{160,192},{192,224},{224... | collective-permute-start | bytes 1179656 | tf_op jit(solution)/shard_map/ppermute | solution.py:27
  45.1 4.1 %collective-permute-start.10 = (bf16[256,384]{1,0:T(8,128)(2,1)S(1)}, bf16[256,384]{1,0:T(8,128)(2,1)S(1)}, u32[]{:S(2)}, u32[]{:S(2)}) collective-permute-start(bf16[256,384]{1,0:T(8,128)(2,1)S(1)} %slice.17), channel_id=1, source_target_pairs={{0,24},{8,0},{16,8},{24,16},{1,25},{9,1},{17,9},{25,17},{2,26},{10... | collective-permute-start | bytes 589832 | tf_op jit(solution)/shard_map/ppermute | solution.py:27
  49.3 0.7 slice.16
  50.0 0.2 copy.17.extra
  50.2 1.7 %collective-permute-done.10.far_high = bf16[256,384]{1,0:T(8,128)(2,1)S(1)} collective-permute-done((bf16[256,384]{1,0:T(8,128)(2,1)S(1)}, bf16[256,384]{1,0:T(8,128)(2,1)S(1)}, u32[]{:S(2)}, u32[]{:S(2)}) %collective-permute-start.10) | collective-permute-done | bytes 196640 | tf_op jit(solution)/shard_map/ppermute | solution.py:27
  51.9 4.0 %collective-permute-done.9.far_low = bf16[256,384]{1,0:T(8,128)(2,1)S(1)} collective-permute-done((bf16[256,384]{1,0:T(8,128)(2,1)}, bf16[256,384]{1,0:T(8,128)(2,1)S(1)}, u32[]{:S(2)}, u32[]{:S(2)}) %collective-permute-start.9) | collective-permute-done | bytes 196640 | tf_op jit(solution)/shard_map/ppermute | solution.py:27
  55.9 1.7 %shard_map.160 = (bf16[384,128]{1,0:T(8,128)(2,1)}, f32[2,384,128]{2,1,0:T(8,128)}, f32[2,384,128]{2,1,0:T(8,128)}, bf16[2,6,128,128]{3,2,1,0:T(8,128)(2,1)}, f3...) custom-call(f32[384,384]{1,0:T(8,128)S(1)} %shard_map.159.near, bf16[384,2048]{1,0:T(8,128)(2,1)S(1)} %get-tuple-element.59.normed, ...), custom_call_target="tpu_custom_call" | custom-call | flops 12000000 | tf_op jit(solution)/shard_map/pallas_call | solution.py:49
  57.6 0.2 collective-permute-start.16
  57.9 2.7 %collective-permute-start.17 = (bf16[256,768]{1,0:T(8,128)(2,1)}, bf16[256,768]{1,0:T(8,128)(2,1)S(1)}, u32[]{:S(2)}, u32[]{:S(2)}) collective-permute-start(bf16[256,768]{1,0:T(8,128)(2,1)} %collective-permute-done.12.refs_2_), channel_id=1, source_target_pairs={{0,224},{32,0},{64,32},{96,64},{128,96},{160,128},{192,160},{224,1... | collective-permute-start | bytes 1179656 | tf_op jit(solution)/shard_map/ppermute | solution.py:27
  60.5 1.0 collective-permute-start.14
  61.5 0.5 collective-permute-start.15
  62.0 1.7 %collective-permute-done.13.ahead = bf16[2,144,128]{2,1,0:T(8,128)(2,1)S(1)} collective-permute-done((bf16[2,144,128]{2,1,0:T(8,128)(2,1)S(1)}, bf16[2,144,128]{2,1,0:T(8,128)(2,1)S(1)}, u32[]{:S(2)}, u32[]{:S(2)}) %collective-permute-start.13) | collective-permute-done | bytes 73760 | tf_op jit(solution)/shard_map/ppermute | solution.py:27
  63.7 1.5 %collective-permute-done.14.far = bf16[2,144,128]{2,1,0:T(8,128)(2,1)S(1)} collective-permute-done((bf16[2,144,128]{2,1,0:T(8,128)(2,1)S(1)}, bf16[2,144,128]{2,1,0:T(8,128)(2,1)S(1)}, u32[]{:S(2)}, u32[]{:S(2)}) %collective-permute-start.14) | collective-permute-done | bytes 73760 | tf_op jit(solution)/shard_map/ppermute | solution.py:27
  65.2 0.9 collective-permute-done.15.behind
  66.1 1.4 %shard_map.162 = (f32[2,136,128]{2,1,0:T(8,128)}, bf16[8,144,128]{2,1,0:T(8,128)(2,1)}) custom-call(s32[4]{0:T(128)S(1)} %pad_add_fusion.1.place, bf16[2,144,128]{2,1,0:T(8,128)(2,1)S(1)} %get-tuple-element.62.own, bf16[2,144,128]{2,1,0:T(8,128)(2,1)S(1)} %collective-permute-done.13.ahead, bf16[2,144,128]{2,1,0:T(8,128)(2,1)S(1)} %collective-permute-done.14.far, ...), custom_call_target="tpu_custom_call" | custom-call | flops 4000000 | tf_op jit(solution)/shard_map/pallas_call | solution.py:49
  67.5 3.4 %all-to-all-start.1 = ((bf16[8,144,128]{2,1,0:T(8,128)(2,1)}), bf16[8,144,128]{2,1,0:T(8,128)(2,1)S(1)}, u32[]{:S(2)}, u32[]{:S(2)}) async-start(bf16[8,144,128]{2,1,0:T(8,128)(2,1)} %get-tuple-element.70), calls=%async_computation.1 | async-start | bytes 589824 | tf_op jit(solution)/shard_map/all_to_all | solution.py:499
  71.0 0.1 pad_add_fusion.2.place
  71.1 1.4 %collective-permute-start.18 = (bf16[128,768]{1,0:T(8,128)(2,1)S(1)}, bf16[128,768]{1,0:T(8,128)(2,1)S(1)}, u32[]{:S(2)}, u32[]{:S(2)}) collective-permute-start(bf16[128,768]{1,0:T(8,128)(2,1)S(1)} %slice.14), channel_id=1, source_target_pairs={{0,32},{32,64},{64,96},{96,128},{128,160},{160,192},{192,224},{224... | collective-permute-start | bytes 589832 | tf_op jit(solution)/shard_map/ppermute | solution.py:27
  72.5 1.4 %collective-permute-start.19 = (bf16[128,768]{1,0:T(8,128)(2,1)S(1)}, bf16[128,768]{1,0:T(8,128)(2,1)S(1)}, u32[]{:S(2)}, u32[]{:S(2)}) collective-permute-start(bf16[128,768]{1,0:T(8,128)(2,1)S(1)} %slice.15), channel_id=1, source_target_pairs={{0,224},{32,0},{64,32},{96,64},{128,96},{160,128},{192,160},{224,1... | collective-permute-start | bytes 589832 | tf_op jit(solution)/shard_map/ppermute | solution.py:27
  74.0 0.8 shard_map.156.edges
  74.7 0.0 copy-start
  74.7 0.0 copy-start.3
  74.7 3.7 %shard_map.161 = (f32[384,512]{1,0:T(8,128)S(1)}, f32[32,256]{1,0:T(8,128)S(1)}, bf16[2,384,128]{2,1,0:T(8,128)(2,1)S(1)}, f32[2,384,128]{2,1,0:T(8,128)S(1)}) custom-call(s32[4]{0:T(128)S(1)} %pad_add_fusion.1.place, bf16[384,2048]{1,0:T(8,128)(2,1)} %get-tuple-element.51.normed, bf16[32,2048]{1,0:T(8,128)(2,1)S(1)} %shard_map.156.edges, ...), custom_call_target="tpu_custom_call" | custom-call | flops 12000000 | tf_op jit(solution)/shard_map/pallas_call | solution.py:49
  78.5 1.2 %collective-permute-done.18.refs_6_ = bf16[128,768]{1,0:T(8,128)(2,1)S(1)} collective-permute-done((bf16[128,768]{1,0:T(8,128)(2,1)S(1)}, bf16[128,768]{1,0:T(8,128)(2,1)S(1)}, u32[]{:S(2)}, u32[]{:S(2)}) %collective-permute-start.18) | collective-permute-done | bytes 196640 | tf_op jit(solution)/shard_map/ppermute | solution.py:27
  79.6 0.0 copy-start.2
  79.6 5.2 %shard_map.163 = (f32[384,128]{1,0:T(8,128)S(1)}, bf16[2,384,128]{2,1,0:T(8,128)(2,1)S(1)}, f32[384,128]{1,0:T(8,128)S(1)}, bf16[384,128]{1,0:T(8,128)(2,1)S(1)}, bf16[2048,256]{1,0:T(8,128)(2,1)S(1)}) custom-call(s32[4]{0:T(128)S(1)} %pad_add_fusion.1.place, bf16[384,2048]{1,0:T(8,128)(2,1)} %get-tuple-element.51.normed, ...), custom_call_target="tpu_custom_call" | custom-call | flops 2000000 | tf_op jit(solution)/shard_map/pallas_call | solution.py:49
  84.8 1.3 %shard_map.164.rec = bf16[384,128]{1,0:T(8,128)(2,1)S(1)} custom-call(s32[4]{0:T(128)S(1)} %pad_add_fusion.1.place, f32[384,128]{1,0:T(8,128)S(1)} %get-tuple-element.78.local, bf16[2,384,128]{2,1,0:T(8,128)(2,1)S(1)} %get-tuple-element.79.lifted, bf16[8,144,128]{2,1,0:T(8,128)(2,1)S(1)} %all-to-all-done.1.every, f32[2,136,128]{2,1,0:T(8,128)} %get-tuple-element.80.before, ...), custom_call_target="tpu_custom_call" | custom-call | flops 4000000 | tf_op jit(solution)/shard_map/pallas_call | solution.py:49
  86.2 1.0 shard_map.166
  87.2 9.1 %collective-permute-start.20 = (bf16[3,48,2048]{2,1,0:T(8,128)(2,1)S(1)}, bf16[3,48,2048]{2,1,0:T(8,128)(2,1)S(1)}, u32[]{:S(2)}, u32[]{:S(2)}) collective-permute-start(bf16[3,48,2048]{2,1,0:T(8,128)(2,1)S(1)} %shard_map.166), channel_id=1, source_target_pairs={{0,1},{1,0},{2,3},{3,2},{4,5},{5,4},{6,7},{7,6},{8,9},{9,8},{10,11... | collective-permute-start | bytes 1769480 | tf_op jit(solution)/shard_map/ppermute | solution.py:27
  96.3 0.1 pad_add_fusion.3.place
  96.3 1.0 shard_map.168
  97.3 0.1 collective-permute-start.21
  97.4 0.1 pad_add_fusion.place
  97.5 1.0 shard_map.165.mine
  98.5 0.3 collective-permute-done.21.got
  98.9 1.4 %collective-permute-start.22 = (bf16[48,1024]{1,0:T(8,128)(2,1)S(1)}, bf16[48,1024]{1,0:T(8,128)(2,1)S(1)}, u32[]{:S(2)}, u32[]{:S(2)}) collective-permute-start(bf16[48,1024]{1,0:T(8,128)(2,1)S(1)} %get-tuple-element.87), channel_id=1, source_target_pairs={{0,2},{2,4},{4,6},{6,0},{1,3},{3,5},{5,7},{7,1},{8,10},{10,12},{12... | collective-permute-start | bytes 294920 | tf_op jit(solution)/shard_map/ppermute | solution.py:27
  100.2 1.5 %collective-permute-start.23 = (bf16[48,1024]{1,0:T(8,128)(2,1)S(1)}, bf16[48,1024]{1,0:T(8,128)(2,1)S(1)}, u32[]{:S(2)}, u32[]{:S(2)}) collective-permute-start(bf16[48,1024]{1,0:T(8,128)(2,1)S(1)} %get-tuple-element.88), channel_id=1, source_target_pairs={{0,6},{2,0},{4,2},{6,4},{1,7},{3,1},{5,3},{7,5},{8,14},{10,8},{12,... | collective-permute-start | bytes 294920 | tf_op jit(solution)/shard_map/ppermute | solution.py:27
  101.8 0.1 shard_map.167
  101.9 2.6 %collective-permute-done.22.low = bf16[48,1024]{1,0:T(8,128)(2,1)S(1)} collective-permute-done((bf16[48,1024]{1,0:T(8,128)(2,1)S(1)}, bf16[48,1024]{1,0:T(8,128)(2,1)S(1)}, u32[]{:S(2)}, u32[]{:S(2)}) %collective-permute-start.22) | collective-permute-done | bytes 98336 | tf_op jit(solution)/shard_map/ppermute | solution.py:27
  104.4 0.1 shard_map.170
  104.5 1.0 collective-permute-start.24
  105.6 1.7 %collective-permute-start.25 = (bf16[48,2048]{1,0:T(8,128)(2,1)S(1)}, bf16[48,2048]{1,0:T(8,128)(2,1)S(1)}, u32[]{:S(2)}, u32[]{:S(2)}) collective-permute-start(bf16[48,2048]{1,0:T(8,128)(2,1)S(1)} %get-tuple-element.90), channel_id=1, source_target_pairs={{0,6},{2,0},{4,2},{6,4},{1,7},{3,1},{5,3},{7,5},{8,14},{10,8},{12,... | collective-permute-start | bytes 589832 | tf_op jit(solution)/shard_map/ppermute | solution.py:27
  107.3 4.0 %collective-permute-done.24 = bf16[48,2048]{1,0:T(8,128)(2,1)S(1)} collective-permute-done((bf16[48,2048]{1,0:T(8,128)(2,1)S(1)}, bf16[48,2048]{1,0:T(8,128)(2,1)S(1)}, u32[]{:S(2)}, u32[]{:S(2)}) %collective-permute-start.24) | collective-permute-done | bytes 196640 | tf_op jit(solution)/shard_map/ppermute | solution.py:27
  111.3 0.7 add_convert_fusion
  (37 shorter events, 0.2 us)
Async XLA Ops:
  0.0 15.2 %copy-start.6 = (bf16[2048]{0:T(1024)(128)(2,1)S(1)}, bf16[2048]{0:T(1024)(128)(2,1)}, u32[]{:S(2)}) copy-start(bf16[2048]{0:T(1024)(128)(2,1)} %param.17) | copy-start | bytes 12292
  1.6 23.3 %all-to-all-start = ((bf16[8,64,384]{2,1,0:T(8,128)(2,1)}), bf16[8,64,384]{2,1,0:T(8,128)(2,1)S(1)}, u32[]{:S(2)}, u32[]{:S(2)}) async-start(bf16[8,64,384]{2,1,0:T(8,128)(2,1)} %shard_map.157), calls=%async_computation | async-start | bytes 786432 | tf_op jit(solution)/shard_map/all_to_all | solution.py:432
  11.5 16.0 %collective-permute-start = (bf16[64,768]{1,0:T(8,128)(2,1)S(1)}, bf16[64,768]{1,0:T(8,128)(2,1)S(1)}, u32[]{:S(2)}, u32[]{:S(2)}) collective-permute-start(bf16[64,768]{1,0:T(8,128)(2,1)S(1)} %get-tuple-element.54.own), channel_id=1, source_target_pairs={{0,24},{8,0},{16,8},{24,16},{1,25},{9,1},{17,9},{25,17},{2,26},{10... | collective-permute-start | bytes 294920 | tf_op jit(solution)/shard_map/ppermute | solution.py:27
  14.1 13.4 %collective-permute-start.1 = (bf16[64,768]{1,0:T(8,128)(2,1)S(1)}, bf16[64,768]{1,0:T(8,128)(2,1)S(1)}, u32[]{:S(2)}, u32[]{:S(2)}) collective-permute-start(bf16[64,768]{1,0:T(8,128)(2,1)S(1)} %get-tuple-element.54.own), channel_id=1, source_target_pairs={{0,16},{8,24},{16,0},{24,8},{1,17},{9,25},{17,1},{25,9},{2,18},{10... | collective-permute-start | bytes 294920 | tf_op jit(solution)/shard_map/ppermute | solution.py:27
  14.6 12.9 %collective-permute-start.2 = (bf16[64,768]{1,0:T(8,128)(2,1)S(1)}, bf16[64,768]{1,0:T(8,128)(2,1)S(1)}, u32[]{:S(2)}, u32[]{:S(2)}) collective-permute-start(bf16[64,768]{1,0:T(8,128)(2,1)S(1)} %get-tuple-element.54.own), channel_id=1, source_target_pairs={{0,8},{8,16},{16,24},{24,0},{1,9},{9,17},{17,25},{25,1},{2,10},{10... | collective-permute-start | bytes 294920 | tf_op jit(solution)/shard_map/ppermute | solution.py:27
  24.8 16.1 %collective-permute-start.6 = (bf16[512,384]{1,0:T(8,128)(2,1)S(1)}, bf16[512,384]{1,0:T(8,128)(2,1)S(1)}, u32[]{:S(2)}, u32[]{:S(2)}) collective-permute-start(bf16[512,384]{1,0:T(8,128)(2,1)S(1)} %bitcast.13), channel_id=1, source_target_pairs={{0,8},{8,16},{16,24},{24,0},{1,9},{9,17},{17,25},{25,1},{2,10},{10... | collective-permute-start | bytes 1179656 | tf_op jit(solution)/shard_map/ppermute | solution.py:27
  26.0 14.9 %collective-permute-start.5 = (bf16[512,384]{1,0:T(8,128)(2,1)S(1)}, bf16[512,384]{1,0:T(8,128)(2,1)S(1)}, u32[]{:S(2)}, u32[]{:S(2)}) collective-permute-start(bf16[512,384]{1,0:T(8,128)(2,1)S(1)} %bitcast.14), channel_id=1, source_target_pairs={{0,24},{8,0},{16,8},{24,16},{1,25},{9,1},{17,9},{25,17},{2,26},{10... | collective-permute-start | bytes 1179656 | tf_op jit(solution)/shard_map/ppermute | solution.py:27
  28.3 13.5 %collective-permute-start.7 = (bf16[256,768]{1,0:T(8,128)(2,1)}, bf16[256,768]{1,0:T(8,128)(2,1)}, u32[]{:S(2)}, u32[]{:S(2)}) collective-permute-start(bf16[256,768]{1,0:T(8,128)(2,1)} %shard_map.158.refs_0_), channel_id=1, source_target_pairs={{0,32},{32,64},{64,96},{96,128},{128,160},{160,192},{192,224},{224... | collective-permute-start | bytes 1179656 | tf_op jit(solution)/shard_map/ppermute | solution.py:27
  28.3 13.5 %collective-permute-start.8 = (bf16[256,768]{1,0:T(8,128)(2,1)}, bf16[256,768]{1,0:T(8,128)(2,1)}, u32[]{:S(2)}, u32[]{:S(2)}) collective-permute-start(bf16[256,768]{1,0:T(8,128)(2,1)} %shard_map.158.refs_0_), channel_id=1, source_target_pairs={{0,224},{32,0},{64,32},{96,64},{128,96},{160,128},{192,160},{224,1... | collective-permute-start | bytes 1179656 | tf_op jit(solution)/shard_map/ppermute | solution.py:27
  31.0 3.8 %collective-permute-start.3 = (bf16[16,2048]{1,0:T(8,128)(2,1)S(1)}, bf16[16,2048]{1,0:T(8,128)(2,1)S(1)}, u32[]{:S(2)}, u32[]{:S(2)}) collective-permute-start(bf16[16,2048]{1,0:T(8,128)(2,1)S(1)} %get-tuple-element.52), channel_id=1, source_target_pairs={{0,8},{8,16},{16,24},{24,32},{32,40},{40,48},{48,56},{56,64},{64,7... | collective-permute-start | bytes 196616 | tf_op jit(solution)/shard_map/ppermute | solution.py:33
  34.8 15.2 %copy-start.7 = (f32[2,384,1]{1,2,0:T(1,128)S(1)}, f32[2,384,1]{1,2,0:T(1,128)}, u32[]{:S(2)}) copy-start(f32[2,384,1]{1,2,0:T(1,128)} %param.26) | copy-start | bytes 9220
  34.8 21.1 %copy-start.1 = (f32[2,128]{1,0:T(2,128)S(1)}, f32[2,128]{1,0:T(2,128)}, u32[]{:S(2)}) copy-start(f32[2,128]{1,0:T(2,128)} %slack.1) | copy-start | bytes 3076
  34.8 6.2 %collective-permute-start.4 = (bf16[16,2048]{1,0:T(8,128)(2,1)S(1)}, bf16[16,2048]{1,0:T(8,128)(2,1)S(1)}, u32[]{:S(2)}, u32[]{:S(2)}) collective-permute-start(bf16[16,2048]{1,0:T(8,128)(2,1)S(1)} %get-tuple-element.53), channel_id=1, source_target_pairs={{8,0},{16,8},{24,16},{32,24},{40,32},{48,40},{56,48},{64,56},{72,6... | collective-permute-start | bytes 196616 | tf_op jit(solution)/shard_map/ppermute | solution.py:33
  41.8 15.8 %collective-permute-start.11 = (bf16[256,768]{1,0:T(8,128)(2,1)}, bf16[256,768]{1,0:T(8,128)(2,1)}, u32[]{:S(2)}, u32[]{:S(2)}) collective-permute-start(bf16[256,768]{1,0:T(8,128)(2,1)} %collective-permute-done.7.refs_4_), channel_id=1, source_target_pairs={{0,32},{32,64},{64,96},{96,128},{128,160},{160,192},{192,224},{224... | collective-permute-start | bytes 1179656 | tf_op jit(solution)/shard_map/ppermute | solution.py:27
  45.1 12.5 %collective-permute-start.12 = (bf16[256,768]{1,0:T(8,128)(2,1)}, bf16[256,768]{1,0:T(8,128)(2,1)}, u32[]{:S(2)}, u32[]{:S(2)}) collective-permute-start(bf16[256,768]{1,0:T(8,128)(2,1)} %collective-permute-done.8.refs_1_), channel_id=1, source_target_pairs={{0,224},{32,0},{64,32},{96,64},{128,96},{160,128},{192,160},{224,1... | collective-permute-start | bytes 1179656 | tf_op jit(solution)/shard_map/ppermute | solution.py:27
  45.1 6.8 %collective-permute-start.10 = (bf16[256,384]{1,0:T(8,128)(2,1)S(1)}, bf16[256,384]{1,0:T(8,128)(2,1)S(1)}, u32[]{:S(2)}, u32[]{:S(2)}) collective-permute-start(bf16[256,384]{1,0:T(8,128)(2,1)S(1)} %slice.17), channel_id=1, source_target_pairs={{0,24},{8,0},{16,8},{24,16},{1,25},{9,1},{17,9},{25,17},{2,26},{10... | collective-permute-start | bytes 589832 | tf_op jit(solution)/shard_map/ppermute | solution.py:27
  50.0 5.9 %collective-permute-start.9 = (bf16[256,384]{1,0:T(8,128)(2,1)}, bf16[256,384]{1,0:T(8,128)(2,1)S(1)}, u32[]{:S(2)}, u32[]{:S(2)}) collective-permute-start(bf16[256,384]{1,0:T(8,128)(2,1)} %slice.16), channel_id=1, source_target_pairs={{0,8},{8,16},{16,24},{24,0},{1,9},{9,17},{17,25},{25,1},{2,10},{10... | collective-permute-start | bytes 589832 | tf_op jit(solution)/shard_map/ppermute | solution.py:27
  57.6 13.4 %collective-permute-start.16 = (bf16[256,768]{1,0:T(8,128)(2,1)}, bf16[256,768]{1,0:T(8,128)(2,1)S(1)}, u32[]{:S(2)}, u32[]{:S(2)}) collective-permute-start(bf16[256,768]{1,0:T(8,128)(2,1)} %collective-permute-done.11.refs_3_), channel_id=1, source_target_pairs={{0,32},{32,64},{64,96},{96,128},{128,160},{160,192},{192,224},{224... | collective-permute-start | bytes 1179656 | tf_op jit(solution)/shard_map/ppermute | solution.py:27
  57.9 13.2 %collective-permute-start.17 = (bf16[256,768]{1,0:T(8,128)(2,1)}, bf16[256,768]{1,0:T(8,128)(2,1)S(1)}, u32[]{:S(2)}, u32[]{:S(2)}) collective-permute-start(bf16[256,768]{1,0:T(8,128)(2,1)} %collective-permute-done.12.refs_2_), channel_id=1, source_target_pairs={{0,224},{32,0},{64,32},{96,64},{128,96},{160,128},{192,160},{224,1... | collective-permute-start | bytes 1179656 | tf_op jit(solution)/shard_map/ppermute | solution.py:27
  60.5 3.2 %collective-permute-start.13 = (bf16[2,144,128]{2,1,0:T(8,128)(2,1)S(1)}, bf16[2,144,128]{2,1,0:T(8,128)(2,1)S(1)}, u32[]{:S(2)}, u32[]{:S(2)}) collective-permute-start(bf16[2,144,128]{2,1,0:T(8,128)(2,1)S(1)} %get-tuple-element.62.own), channel_id=1, source_target_pairs={{0,24},{8,0},{16,8},{24,16},{1,25},{9,1},{17,9},{25,17},{2,26},{10... | collective-permute-start | bytes 221192 | tf_op jit(solution)/shard_map/ppermute | solution.py:27
  60.5 4.7 %collective-permute-start.14 = (bf16[2,144,128]{2,1,0:T(8,128)(2,1)S(1)}, bf16[2,144,128]{2,1,0:T(8,128)(2,1)S(1)}, u32[]{:S(2)}, u32[]{:S(2)}) collective-permute-start(bf16[2,144,128]{2,1,0:T(8,128)(2,1)S(1)} %get-tuple-element.62.own), channel_id=1, source_target_pairs={{0,16},{8,24},{16,0},{24,8},{1,17},{9,25},{17,1},{25,9},{2,18},{10... | collective-permute-start | bytes 221192 | tf_op jit(solution)/shard_map/ppermute | solution.py:27
  61.5 4.6 %collective-permute-start.15 = (bf16[2,144,128]{2,1,0:T(8,128)(2,1)S(1)}, bf16[2,144,128]{2,1,0:T(8,128)(2,1)S(1)}, u32[]{:S(2)}, u32[]{:S(2)}) collective-permute-start(bf16[2,144,128]{2,1,0:T(8,128)(2,1)S(1)} %get-tuple-element.62.own), channel_id=1, source_target_pairs={{0,8},{8,16},{16,24},{24,0},{1,9},{9,17},{17,25},{25,1},{2,10},{10... | collective-permute-start | bytes 221192 | tf_op jit(solution)/shard_map/ppermute | solution.py:27
  67.5 17.3 %all-to-all-start.1 = ((bf16[8,144,128]{2,1,0:T(8,128)(2,1)}), bf16[8,144,128]{2,1,0:T(8,128)(2,1)S(1)}, u32[]{:S(2)}, u32[]{:S(2)}) async-start(bf16[8,144,128]{2,1,0:T(8,128)(2,1)} %get-tuple-element.70), calls=%async_computation.1 | async-start | bytes 589824 | tf_op jit(solution)/shard_map/all_to_all | solution.py:499
  71.1 7.4 %copy-start.4 = (bf16[256,768]{1,0:T(8,128)(2,1)}, bf16[256,768]{1,0:T(8,128)(2,1)S(1)}, u32[]{:S(2)}) copy-start(bf16[256,768]{1,0:T(8,128)(2,1)S(1)} %collective-permute-done.16.refs_8_) | copy-start | bytes 1179652
  71.1 7.4 %copy-start.5 = (bf16[256,768]{1,0:T(8,128)(2,1)}, bf16[256,768]{1,0:T(8,128)(2,1)S(1)}, u32[]{:S(2)}) copy-start(bf16[256,768]{1,0:T(8,128)(2,1)S(1)} %collective-permute-done.17.refs_5_) | copy-start | bytes 1179652
  71.1 8.5 %collective-permute-start.18 = (bf16[128,768]{1,0:T(8,128)(2,1)S(1)}, bf16[128,768]{1,0:T(8,128)(2,1)S(1)}, u32[]{:S(2)}, u32[]{:S(2)}) collective-permute-start(bf16[128,768]{1,0:T(8,128)(2,1)S(1)} %slice.14), channel_id=1, source_target_pairs={{0,32},{32,64},{64,96},{96,128},{128,160},{160,192},{192,224},{224... | collective-permute-start | bytes 589832 | tf_op jit(solution)/shard_map/ppermute | solution.py:27
  72.5 7.1 %collective-permute-start.19 = (bf16[128,768]{1,0:T(8,128)(2,1)S(1)}, bf16[128,768]{1,0:T(8,128)(2,1)S(1)}, u32[]{:S(2)}, u32[]{:S(2)}) collective-permute-start(bf16[128,768]{1,0:T(8,128)(2,1)S(1)} %slice.15), channel_id=1, source_target_pairs={{0,224},{32,0},{64,32},{96,64},{128,96},{160,128},{192,160},{224,1... | collective-permute-start | bytes 589832 | tf_op jit(solution)/shard_map/ppermute | solution.py:27
  74.7 4.9 %copy-start = (bf16[31,128]{1,0:T(8,128)(2,1)S(1)}, bf16[31,128]{1,0:T(8,128)(2,1)}, u32[]{:S(2)}) copy-start(bf16[31,128]{1,0:T(8,128)(2,1)} %refs_14_.1) | copy-start | bytes 23812
  74.7 4.9 %copy-start.3 = (bf16[128]{0:T(256)(128)(2,1)S(1)}, bf16[128]{0:T(256)(128)(2,1)}, u32[]{:S(2)}) copy-start(bf16[128]{0:T(256)(128)(2,1)} %param.29) | copy-start | bytes 772
  79.6 5.2 %copy-start.2 = (bf16[128]{0:T(256)(128)(2,1)S(1)}, bf16[128]{0:T(256)(128)(2,1)}, u32[]{:S(2)}) copy-start(bf16[128]{0:T(256)(128)(2,1)} %param.27) | copy-start | bytes 772
  87.2 14.6 %collective-permute-start.20 = (bf16[3,48,2048]{2,1,0:T(8,128)(2,1)S(1)}, bf16[3,48,2048]{2,1,0:T(8,128)(2,1)S(1)}, u32[]{:S(2)}, u32[]{:S(2)}) collective-permute-start(bf16[3,48,2048]{2,1,0:T(8,128)(2,1)S(1)} %shard_map.166), channel_id=1, source_target_pairs={{0,1},{1,0},{2,3},{3,2},{4,5},{5,4},{6,7},{7,6},{8,9},{9,8},{10,11... | collective-permute-start | bytes 1769480 | tf_op jit(solution)/shard_map/ppermute | solution.py:27
  97.3 1.5 %collective-permute-start.21 = (bf16[1,48,2048]{2,1,0:T(8,128)(2,1)S(1)}, bf16[1,48,2048]{2,1,0:T(8,128)(2,1)S(1)}, u32[]{:S(2)}, u32[]{:S(2)}) collective-permute-start(bf16[1,48,2048]{2,1,0:T(8,128)(2,1)S(1)} %shard_map.168), channel_id=1, source_target_pairs={{0,1},{1,0},{2,3},{3,2},{4,5},{5,4},{6,7},{7,6},{8,9},{9,8},{10,11... | collective-permute-start | bytes 589832 | tf_op jit(solution)/shard_map/ppermute | solution.py:27
  98.9 5.6 %collective-permute-start.22 = (bf16[48,1024]{1,0:T(8,128)(2,1)S(1)}, bf16[48,1024]{1,0:T(8,128)(2,1)S(1)}, u32[]{:S(2)}, u32[]{:S(2)}) collective-permute-start(bf16[48,1024]{1,0:T(8,128)(2,1)S(1)} %get-tuple-element.87), channel_id=1, source_target_pairs={{0,2},{2,4},{4,6},{6,0},{1,3},{3,5},{5,7},{7,1},{8,10},{10,12},{12... | collective-permute-start | bytes 294920 | tf_op jit(solution)/shard_map/ppermute | solution.py:27
  100.2 4.2 %collective-permute-start.23 = (bf16[48,1024]{1,0:T(8,128)(2,1)S(1)}, bf16[48,1024]{1,0:T(8,128)(2,1)S(1)}, u32[]{:S(2)}, u32[]{:S(2)}) collective-permute-start(bf16[48,1024]{1,0:T(8,128)(2,1)S(1)} %get-tuple-element.88), channel_id=1, source_target_pairs={{0,6},{2,0},{4,2},{6,4},{1,7},{3,1},{5,3},{7,5},{8,14},{10,8},{12,... | collective-permute-start | bytes 294920 | tf_op jit(solution)/shard_map/ppermute | solution.py:27
  104.5 6.7 %collective-permute-start.24 = (bf16[48,2048]{1,0:T(8,128)(2,1)S(1)}, bf16[48,2048]{1,0:T(8,128)(2,1)S(1)}, u32[]{:S(2)}, u32[]{:S(2)}) collective-permute-start(bf16[48,2048]{1,0:T(8,128)(2,1)S(1)} %get-tuple-element.89), channel_id=1, source_target_pairs={{0,2},{2,4},{4,6},{6,0},{1,3},{3,5},{5,7},{7,1},{8,10},{10,12},{12... | collective-permute-start | bytes 589832 | tf_op jit(solution)/shard_map/ppermute | solution.py:27
  105.6 5.7 %collective-permute-start.25 = (bf16[48,2048]{1,0:T(8,128)(2,1)S(1)}, bf16[48,2048]{1,0:T(8,128)(2,1)S(1)}, u32[]{:S(2)}, u32[]{:S(2)}) collective-permute-start(bf16[48,2048]{1,0:T(8,128)(2,1)S(1)} %get-tuple-element.90), channel_id=1, source_target_pairs={{0,6},{2,0},{4,2},{6,4},{1,7},{3,1},{5,3},{7,5},{8,14},{10,8},{12,... | collective-permute-start | bytes 589832 | tf_op jit(solution)/shard_map/ppermute | solution.py:27

commit v4 on v2

--- a/solution.py
+++ b/solution.py
@@ -73,21 +73,23 @@
     return jnp.dot(a, b, preferred_element_type=F32)
 
 
+def collect_first_kernel(a, b, c, first):
+    for k, ref in enumerate((a, b, c)):
+        for z in range(8):
+            first[z, :, k * HEAD : (k + 1) * HEAD] = ref[...]
+
+
 def collect_kernel(x, *refs):
-    first, later, top, bottom, done = refs[-5:]
+    later, top, bottom, done = refs[-4:]
     edge = top.shape[0]
-    rows = (x.at[:edge], x.at[x.shape[0] - edge :])
+    pairs = [(x.at[:edge], top), (x.at[x.shape[0] - edge :], bottom)]
+    for k, ref in enumerate(refs[:-4]):
+        pairs.append((ref, later.at[:, k * HEAD : (k + 1) * HEAD]))
     copies = [
-        pltpu.make_async_copy(source, into, done.at[k])
-        for k, (source, into) in enumerate(zip(rows, (top, bottom)))
+        pltpu.make_async_copy(source, into, done.at[k]) for k, (source, into) in enumerate(pairs)
     ]
     for copy in copies:
         copy.start()
-    for k, ref in enumerate(refs[:3]):
-        for z in range(8):
-            first[z, :, k * HEAD : (k + 1) * HEAD] = ref[...]
-    for k, ref in enumerate(refs[3:-5]):
-        later[:, k * HEAD : (k + 1) * HEAD] = ref[...]
     for copy in copies:
         copy.wait()
 
@@ -403,17 +405,22 @@
     gain = entry_rescale_vector[None]
     place = jnp.stack([z, lax.rem(4 - x, 4) * 64, x, y]).astype(jnp.int32)
     edge = pltpu.VMEM((16, sequence_embeddings.shape[1]), BF)
-    first, shard, top, bottom = kernel_call(
+    (first,) = kernel_call(
+        collect_first_kernel,
+        1,
+        [pltpu.HBM((8, 64, 384), BF)],
+        far_off(onward_retain_matrix),
+        far_off(reverse_retain_matrix),
+        far_off(content_matrix),
+    )
+    shard, top, bottom = kernel_call(
         collect_kernel,
-        2,
-        [pltpu.VMEM((8, 64, 384), BF), pltpu.VMEM((64, 768), BF), edge, edge],
+        1,
+        [pltpu.VMEM((64, 768), BF), edge, edge],
         far_off(sequence_embeddings),
         *(
             far_off(weight)
             for weight in (
-                onward_retain_matrix,
-                reverse_retain_matrix,
-                content_matrix,
                 probe_matrix,
                 emission_switch_matrix,
                 pointwise_content_matrix,
@@ -422,17 +429,16 @@
                 filter_readout_matrix.T,
             )
         ),
-        scratch=(pltpu.SemaphoreType.DMA((2,)),),
-        left=(0,),
+        scratch=(pltpu.SemaphoreType.DMA((8,)),),
+        left=range(7),
     )
     first = lax.all_to_all(first, "z", 0, 0, tiled=True)
     first = first.reshape(512, 384)
     ahead, far, behind = shift(shard, "x", -1), shift(shard, "x", 2), shift(shard, "x", 1)
     normed, normed_first = normalized(place, far_off(sequence_embeddings), gain, 2)
-    low = line(bottom, ("z", "x"), 1)
-    high = line(top, ("z", "x"), -1)
-    normed, normed_first, shard, ahead, far, behind, low = lax.optimization_barrier(
-        (normed, normed_first, shard, ahead, far, behind, low)
+    low, high = line(bottom, ("z", "x"), 1), line(top, ("z", "x"), -1)
+    normed, normed_first, shard, ahead, far, behind = lax.optimization_barrier(
+        (normed, normed_first, shard, ahead, far, behind)
     )
     (edges,) = normalized(place, jnp.concatenate([low, high], axis=0), gain, 1)
     (later,) = kernel_call(
@@ -449,7 +455,7 @@
     up1, down1 = shift(later, "z", 1), shift(later, "z", -1)
     far_low, far_high = shift(behind[:256], "x", 1), shift(ahead[256:], "x", -1)
     normed_first = keep(normed_first)
-    _, seen = ordered(high, behind)
+    _, _, seen = ordered(low, high, behind)
     (near,) = kernel_call(
         near_scores_kernel,
         2,

time: 109 us -> 112 us (1.028)
  waiting for transfers between devices: 27.4 us -> 30.6 us
    all_to_all x1, waiting for transfers between devices: 2.8 us -> 5.21 us  [layer(): first = lax.all_to_all(first, 'z', 0, 0, tiled=True)]
    ppermute x23, starting transfers between devices: 36.2 us -> 38.4 us  [shift(): return lax.ppermute(array, axis, ring(lax.axis_size(axis), step))]
    ppermute x2, waiting for transfers between devices: 4.81 us -> 6.66 us  [line(): return lax.ppermute(array, axes, pairs)]
    ppermute x2, starting transfers between devices: 4.83 us -> 3.31 us  [line(): return lax.ppermute(array, axes, pairs)]
    pallas_call x14 -> x15, Pallas kernels: 24.1 us -> 24.2 us  [kernel_call(): pl.pallas_call(body, out_shape=tuple(outs), in_specs=[SMEM if o.dtype ==...]
where the time goes in v4:
time: 112 us; the launch traced here: 111 us
  starting transfers between devices  54.1 us (48%)
  waiting for transfers between devices  30.6 us (27%)
  Pallas kernels  24.2 us (22%)
    ppermute x23, starting transfers between devices, shift(): return lax.ppermute(array, axis, ring(lax.axis_size(axis), step))  38.4 us
    pallas_call x15, Pallas kernels, kernel_call(): pl.pallas_call(body, out_shape=tuple(outs), in_specs=[SMEM if o.dtype ==...  24.2 us
    ppermute x23, waiting for transfers between devices, shift(): return lax.ppermute(array, axis, ring(lax.axis_size(axis), step))  18.7 us
    all_to_all x1, starting transfers between devices, layer(): first = lax.all_to_all(first, 'z', 0, 0, tiled=True)  9 us
    ppermute x2, waiting for transfers between devices, line(): return lax.ppermute(array, axes, pairs)  6.66 us
    all_to_all x1, waiting for transfers between devices, layer(): first = lax.all_to_all(first, 'z', 0, 0, tiled=True)  5.21 us
    all_to_all x1, starting transfers between devices, layer(): every = lax.all_to_all(send, 'z', 0, 0, tiled=True)  3.42 us
    ppermute x2, starting transfers between devices, line(): return lax.ppermute(array, axes, pairs)  3.31 us
  transfers between devices with their start and end apart: 27, of which 12 were waited for; matrix products, arithmetic and copies ran while one was open for 1% of the time, Pallas kernels for 18%

profile of v4, /device:TPU:1, one launch (start us, length us, event | category | flops | bytes accessed | tf_op | source)
XLA Modules:
  0.0 111.0 jit_solution(4956527456477331929)
XLA Ops:
  0.0 1.6 %shard_map.157 = bf16[8,64,384]{2,1,0:T(8,128)(2,1)} custom-call(bf16[64,128]{1,0:T(8,128)(2,1)} %a.1, bf16[64,128]{1,0:T(8,128)(2,1)} %b.1, bf16[64,128]{1,0:T(8,128)(2,1)} %c.1), custom_call_target="tpu_custom_call" | custom-call | flops 4000000 | tf_op jit(solution)/shard_map/pallas_call | solution.py:49
  1.6 9.0 %all-to-all-start = ((bf16[8,64,384]{2,1,0:T(8,128)(2,1)}), bf16[8,64,384]{2,1,0:T(8,128)(2,1)S(1)}, u32[]{:S(2)}, u32[]{:S(2)}) async-start(bf16[8,64,384]{2,1,0:T(8,128)(2,1)} %shard_map.157), calls=%async_computation | async-start | bytes 786432 | tf_op jit(solution)/shard_map/all_to_all | solution.py:435
  10.6 0.9 shard_map.155
  11.5 2.6 %collective-permute-start = (bf16[64,768]{1,0:T(8,128)(2,1)S(1)}, bf16[64,768]{1,0:T(8,128)(2,1)S(1)}, u32[]{:S(2)}, u32[]{:S(2)}) collective-permute-start(bf16[64,768]{1,0:T(8,128)(2,1)S(1)} %get-tuple-element.54.own), channel_id=1, source_target_pairs={{0,24},{8,0},{16,8},{24,16},{1,25},{9,1},{17,9},{25,17},{2,26},{10... | collective-permute-start | bytes 294920 | tf_op jit(solution)/shard_map/ppermute | solution.py:27
  14.1 0.5 collective-permute-start.1
  14.6 0.6 collective-permute-start.2
  15.2 0.1 pad_add_fusion.place
  15.3 4.3 %shard_map.154 = (bf16[384,2048]{1,0:T(8,128)(2,1)}, bf16[384,2048]{1,0:T(8,128)(2,1)S(1)}) custom-call(s32[4]{0:T(128)S(1)} %pad_add_fusion.place, bf16[384,2048]{1,0:T(8,128)(2,1)} %x.3, bf16[1,2048]{1,0:T(2,128)(2,1)S(1)} %broadcast_in_dim.16.gain), custom_call_target="tpu_custom_call" | custom-call | flops 12000000 | tf_op jit(solution)/shard_map/pallas_call | solution.py:49
  19.6 5.2 %all-to-all-done = bf16[8,64,384]{2,1,0:T(8,128)(2,1)S(1)} async-done(((bf16[8,64,384]{2,1,0:T(8,128)(2,1)}), bf16[8,64,384]{2,1,0:T(8,128)(2,1)S(1)}, u32[]{:S(2)}, u32[]{:S(2)}) %all-to-all-start) | async-done | bytes 393248 | tf_op jit(solution)/shard_map/all_to_all | solution.py:435
  24.8 1.2 %collective-permute-start.6 = (bf16[512,384]{1,0:T(8,128)(2,1)S(1)}, bf16[512,384]{1,0:T(8,128)(2,1)S(1)}, u32[]{:S(2)}, u32[]{:S(2)}) collective-permute-start(bf16[512,384]{1,0:T(8,128)(2,1)S(1)} %bitcast.11), channel_id=1, source_target_pairs={{0,8},{8,16},{16,24},{24,0},{1,9},{9,17},{17,25},{25,1},{2,10},{10... | collective-permute-start | bytes 1179656 | tf_op jit(solution)/shard_map/ppermute | solution.py:27
  26.0 1.5 %collective-permute-start.5 = (bf16[512,384]{1,0:T(8,128)(2,1)S(1)}, bf16[512,384]{1,0:T(8,128)(2,1)S(1)}, u32[]{:S(2)}, u32[]{:S(2)}) collective-permute-start(bf16[512,384]{1,0:T(8,128)(2,1)S(1)} %bitcast.12), channel_id=1, source_target_pairs={{0,24},{8,0},{16,8},{24,16},{1,25},{9,1},{17,9},{25,17},{2,26},{10... | collective-permute-start | bytes 1179656 | tf_op jit(solution)/shard_map/ppermute | solution.py:27
  27.5 0.8 shard_map.158.refs_0_
  28.3 0.0 collective-permute-start.7
  28.3 2.7 %collective-permute-start.8 = (bf16[256,768]{1,0:T(8,128)(2,1)}, bf16[256,768]{1,0:T(8,128)(2,1)}, u32[]{:S(2)}, u32[]{:S(2)}) collective-permute-start(bf16[256,768]{1,0:T(8,128)(2,1)} %shard_map.158.refs_0_), channel_id=1, source_target_pairs={{0,224},{32,0},{64,32},{96,64},{128,96},{160,128},{192,160},{224,1... | collective-permute-start | bytes 1179656 | tf_op jit(solution)/shard_map/ppermute | solution.py:27
  31.0 1.9 %collective-permute-start.3 = (bf16[16,2048]{1,0:T(8,128)(2,1)S(1)}, bf16[16,2048]{1,0:T(8,128)(2,1)S(1)}, u32[]{:S(2)}, u32[]{:S(2)}) collective-permute-start(bf16[16,2048]{1,0:T(8,128)(2,1)S(1)} %get-tuple-element.52), channel_id=1, source_target_pairs={{0,8},{8,16},{16,24},{24,32},{32,40},{40,48},{48,56},{56,64},{64,7... | collective-permute-start | bytes 196616 | tf_op jit(solution)/shard_map/ppermute | solution.py:33
  32.9 1.9 %collective-permute-done.3 = bf16[16,2048]{1,0:T(8,128)(2,1)S(1)} collective-permute-done((bf16[16,2048]{1,0:T(8,128)(2,1)S(1)}, bf16[16,2048]{1,0:T(8,128)(2,1)S(1)}, u32[]{:S(2)}, u32[]{:S(2)}) %collective-permute-start.3) | collective-permute-done | bytes 65568 | tf_op jit(solution)/shard_map/ppermute | solution.py:33
  34.8 1.4 %collective-permute-start.4 = (bf16[16,2048]{1,0:T(8,128)(2,1)S(1)}, bf16[16,2048]{1,0:T(8,128)(2,1)S(1)}, u32[]{:S(2)}, u32[]{:S(2)}) collective-permute-start(bf16[16,2048]{1,0:T(8,128)(2,1)S(1)} %get-tuple-element.53), channel_id=1, source_target_pairs={{8,0},{16,8},{24,16},{32,24},{40,32},{48,40},{56,48},{64,56},{72,6... | collective-permute-start | bytes 196616 | tf_op jit(solution)/shard_map/ppermute | solution.py:33
  36.2 4.8 %collective-permute-done.4 = bf16[16,2048]{1,0:T(8,128)(2,1)S(1)} collective-permute-done((bf16[16,2048]{1,0:T(8,128)(2,1)S(1)}, bf16[16,2048]{1,0:T(8,128)(2,1)S(1)}, u32[]{:S(2)}, u32[]{:S(2)}) %collective-permute-start.4) | collective-permute-done | bytes 65568 | tf_op jit(solution)/shard_map/ppermute | solution.py:33
  40.9 0.0 collective-permute-done.5.ahead
  41.0 0.8 shard_map.159.near
  41.7 0.0 collective-permute-done.7.refs_4_
  41.8 3.3 %collective-permute-start.11 = (bf16[256,768]{1,0:T(8,128)(2,1)}, bf16[256,768]{1,0:T(8,128)(2,1)}, u32[]{:S(2)}, u32[]{:S(2)}) collective-permute-start(bf16[256,768]{1,0:T(8,128)(2,1)} %collective-permute-done.7.refs_4_), channel_id=1, source_target_pairs={{0,32},{32,64},{64,96},{96,128},{128,160},{160,192},{192,224},{224... | collective-permute-start | bytes 1179656 | tf_op jit(solution)/shard_map/ppermute | solution.py:27
  45.1 4.1 %collective-permute-start.10 = (bf16[256,384]{1,0:T(8,128)(2,1)S(1)}, bf16[256,384]{1,0:T(8,128)(2,1)S(1)}, u32[]{:S(2)}, u32[]{:S(2)}) collective-permute-start(bf16[256,384]{1,0:T(8,128)(2,1)S(1)} %slice.17), channel_id=1, source_target_pairs={{0,24},{8,0},{16,8},{24,16},{1,25},{9,1},{17,9},{25,17},{2,26},{10... | collective-permute-start | bytes 589832 | tf_op jit(solution)/shard_map/ppermute | solution.py:27
  49.2 0.7 slice.16
  49.9 0.2 copy.17.extra
  50.1 1.7 %collective-permute-done.10.far_high = bf16[256,384]{1,0:T(8,128)(2,1)S(1)} collective-permute-done((bf16[256,384]{1,0:T(8,128)(2,1)S(1)}, bf16[256,384]{1,0:T(8,128)(2,1)S(1)}, u32[]{:S(2)}, u32[]{:S(2)}) %collective-permute-start.10) | collective-permute-done | bytes 196640 | tf_op jit(solution)/shard_map/ppermute | solution.py:27
  51.9 4.0 %collective-permute-done.9.far_low = bf16[256,384]{1,0:T(8,128)(2,1)S(1)} collective-permute-done((bf16[256,384]{1,0:T(8,128)(2,1)}, bf16[256,384]{1,0:T(8,128)(2,1)S(1)}, u32[]{:S(2)}, u32[]{:S(2)}) %collective-permute-start.9) | collective-permute-done | bytes 196640 | tf_op jit(solution)/shard_map/ppermute | solution.py:27
  55.9 1.7 %shard_map.160 = (bf16[384,128]{1,0:T(8,128)(2,1)}, f32[2,384,128]{2,1,0:T(8,128)}, f32[2,384,128]{2,1,0:T(8,128)}, bf16[2,6,128,128]{3,2,1,0:T(8,128)(2,1)}, f3...) custom-call(f32[384,384]{1,0:T(8,128)S(1)} %shard_map.159.near, bf16[384,2048]{1,0:T(8,128)(2,1)S(1)} %get-tuple-element.59.normed, ...), custom_call_target="tpu_custom_call" | custom-call | flops 12000000 | tf_op jit(solution)/shard_map/pallas_call | solution.py:49
  57.6 0.0 collective-permute-done.11.refs_3_
  57.6 0.2 collective-permute-start.16
  57.8 2.7 %collective-permute-start.17 = (bf16[256,768]{1,0:T(8,128)(2,1)}, bf16[256,768]{1,0:T(8,128)(2,1)S(1)}, u32[]{:S(2)}, u32[]{:S(2)}) collective-permute-start(bf16[256,768]{1,0:T(8,128)(2,1)} %collective-permute-done.12.refs_2_), channel_id=1, source_target_pairs={{0,224},{32,0},{64,32},{96,64},{128,96},{160,128},{192,160},{224,1... | collective-permute-start | bytes 1179656 | tf_op jit(solution)/shard_map/ppermute | solution.py:27
  60.5 0.0 collective-permute-start.13
  60.5 1.0 collective-permute-start.14
  61.5 0.5 collective-permute-start.15
  61.9 1.7 %collective-permute-done.13.ahead = bf16[2,144,128]{2,1,0:T(8,128)(2,1)S(1)} collective-permute-done((bf16[2,144,128]{2,1,0:T(8,128)(2,1)S(1)}, bf16[2,144,128]{2,1,0:T(8,128)(2,1)S(1)}, u32[]{:S(2)}, u32[]{:S(2)}) %collective-permute-start.13) | collective-permute-done | bytes 73760 | tf_op jit(solution)/shard_map/ppermute | solution.py:27
  63.7 1.5 %collective-permute-done.14.far = bf16[2,144,128]{2,1,0:T(8,128)(2,1)S(1)} collective-permute-done((bf16[2,144,128]{2,1,0:T(8,128)(2,1)S(1)}, bf16[2,144,128]{2,1,0:T(8,128)(2,1)S(1)}, u32[]{:S(2)}, u32[]{:S(2)}) %collective-permute-start.14) | collective-permute-done | bytes 73760 | tf_op jit(solution)/shard_map/ppermute | solution.py:27
  65.2 0.9 collective-permute-done.15.behind
  66.1 1.4 %shard_map.162 = (f32[2,136,128]{2,1,0:T(8,128)}, bf16[8,144,128]{2,1,0:T(8,128)(2,1)}) custom-call(s32[4]{0:T(128)S(1)} %pad_add_fusion.place, bf16[2,144,128]{2,1,0:T(8,128)(2,1)S(1)} %get-tuple-element.62.own, bf16[2,144,128]{2,1,0:T(8,128)(2,1)S(1)} %collective-permute-done.13.ahead, bf16[2,144,128]{2,1,0:T(8,128)(2,1)S(1)} %collective-permute-done.14.far, ...), custom_call_target="tpu_custom_call" | custom-call | flops 4000000 | tf_op jit(solution)/shard_map/pallas_call | solution.py:49
  67.5 3.4 %all-to-all-start.1 = ((bf16[8,144,128]{2,1,0:T(8,128)(2,1)}), bf16[8,144,128]{2,1,0:T(8,128)(2,1)S(1)}, u32[]{:S(2)}, u32[]{:S(2)}) async-start(bf16[8,144,128]{2,1,0:T(8,128)(2,1)} %get-tuple-element.70), calls=%async_computation.1 | async-start | bytes 589824 | tf_op jit(solution)/shard_map/all_to_all | solution.py:502
  70.9 0.0 collective-permute-done.17.refs_5_
  71.0 1.4 %collective-permute-start.18 = (bf16[128,768]{1,0:T(8,128)(2,1)S(1)}, bf16[128,768]{1,0:T(8,128)(2,1)S(1)}, u32[]{:S(2)}, u32[]{:S(2)}) collective-permute-start(bf16[128,768]{1,0:T(8,128)(2,1)S(1)} %slice.14), channel_id=1, source_target_pairs={{0,32},{32,64},{64,96},{96,128},{128,160},{160,192},{192,224},{224... | collective-permute-start | bytes 589832 | tf_op jit(solution)/shard_map/ppermute | solution.py:27
  72.4 1.4 %collective-permute-start.19 = (bf16[128,768]{1,0:T(8,128)(2,1)S(1)}, bf16[128,768]{1,0:T(8,128)(2,1)S(1)}, u32[]{:S(2)}, u32[]{:S(2)}) collective-permute-start(bf16[128,768]{1,0:T(8,128)(2,1)S(1)} %slice.15), channel_id=1, source_target_pairs={{0,224},{32,0},{64,32},{96,64},{128,96},{160,128},{192,160},{224,1... | collective-permute-start | bytes 589832 | tf_op jit(solution)/shard_map/ppermute | solution.py:27
  73.8 0.8 shard_map.156.edges
  74.6 0.0 copy-start
  74.6 0.0 copy-start.3
  74.6 3.7 %shard_map.161 = (f32[384,512]{1,0:T(8,128)S(1)}, f32[32,256]{1,0:T(8,128)S(1)}, bf16[2,384,128]{2,1,0:T(8,128)(2,1)S(1)}, f32[2,384,128]{2,1,0:T(8,128)S(1)}) custom-call(s32[4]{0:T(128)S(1)} %pad_add_fusion.place, bf16[384,2048]{1,0:T(8,128)(2,1)} %get-tuple-element.51.normed, bf16[32,2048]{1,0:T(8,128)(2,1)S(1)} %shard_map.156.edges, ...), custom_call_target="tpu_custom_call" | custom-call | flops 12000000 | tf_op jit(solution)/shard_map/pallas_call | solution.py:49
  78.4 1.2 %collective-permute-done.18.refs_6_ = bf16[128,768]{1,0:T(8,128)(2,1)S(1)} collective-permute-done((bf16[128,768]{1,0:T(8,128)(2,1)S(1)}, bf16[128,768]{1,0:T(8,128)(2,1)S(1)}, u32[]{:S(2)}, u32[]{:S(2)}) %collective-permute-start.18) | collective-permute-done | bytes 196640 | tf_op jit(solution)/shard_map/ppermute | solution.py:27
  79.6 0.0 copy-start.2
  79.6 5.2 %shard_map.163 = (f32[384,128]{1,0:T(8,128)S(1)}, bf16[2,384,128]{2,1,0:T(8,128)(2,1)S(1)}, f32[384,128]{1,0:T(8,128)S(1)}, bf16[384,128]{1,0:T(8,128)(2,1)S(1)}, bf16[2048,256]{1,0:T(8,128)(2,1)S(1)}) custom-call(s32[4]{0:T(128)S(1)} %pad_add_fusion.place, bf16[384,2048]{1,0:T(8,128)(2,1)} %get-tuple-element.51.normed, ...), custom_call_target="tpu_custom_call" | custom-call | flops 2000000 | tf_op jit(solution)/shard_map/pallas_call | solution.py:49
  84.8 1.4 %shard_map.164.rec = bf16[384,128]{1,0:T(8,128)(2,1)S(1)} custom-call(s32[4]{0:T(128)S(1)} %pad_add_fusion.place, f32[384,128]{1,0:T(8,128)S(1)} %get-tuple-element.78.local, bf16[2,384,128]{2,1,0:T(8,128)(2,1)S(1)} %get-tuple-element.79.lifted, bf16[8,144,128]{2,1,0:T(8,128)(2,1)S(1)} %all-to-all-done.1.every, f32[2,136,128]{2,1,0:T(8,128)} %get-tuple-element.80.before, ...), custom_call_target="tpu_custom_call" | custom-call | flops 4000000 | tf_op jit(solution)/shard_map/pallas_call | solution.py:49
  86.1 0.5 shard_map.166
  86.7 9.0 %collective-permute-start.20 = (bf16[4,48,2048]{2,1,0:T(8,128)(2,1)S(1)}, bf16[4,48,2048]{2,1,0:T(8,128)(2,1)S(1)}, u32[]{:S(2)}, u32[]{:S(2)}) collective-permute-start(bf16[4,48,2048]{2,1,0:T(8,128)(2,1)S(1)} %shard_map.166), channel_id=1, source_target_pairs={{0,1},{1,0},{2,3},{3,2},{4,5},{5,4},{6,7},{7,6},{8,9},{9,8},{10,11... | collective-permute-start | bytes 2359304 | tf_op jit(solution)/shard_map/ppermute | solution.py:27
  95.7 0.5 shard_map.165.mine
  96.2 1.4 %collective-permute-done.20.got = bf16[4,48,2048]{2,1,0:T(8,128)(2,1)S(1)} collective-permute-done((bf16[4,48,2048]{2,1,0:T(8,128)(2,1)S(1)}, bf16[4,48,2048]{2,1,0:T(8,128)(2,1)S(1)}, u32[]{:S(2)}, u32[]{:S(2)}) %collective-permute-start.20) | collective-permute-done | bytes 786464 | tf_op jit(solution)/shard_map/ppermute | solution.py:27
  97.6 0.7 shard_map.167
  98.3 1.4 %collective-permute-start.21 = (bf16[48,1024]{1,0:T(8,128)(2,1)S(1)}, bf16[48,1024]{1,0:T(8,128)(2,1)S(1)}, u32[]{:S(2)}, u32[]{:S(2)}) collective-permute-start(bf16[48,1024]{1,0:T(8,128)(2,1)S(1)} %get-tuple-element.87), channel_id=1, source_target_pairs={{0,2},{2,4},{4,6},{6,0},{1,3},{3,5},{5,7},{7,1},{8,10},{10,12},{12... | collective-permute-start | bytes 294920 | tf_op jit(solution)/shard_map/ppermute | solution.py:27
  99.7 1.5 %collective-permute-start.22 = (bf16[48,1024]{1,0:T(8,128)(2,1)S(1)}, bf16[48,1024]{1,0:T(8,128)(2,1)S(1)}, u32[]{:S(2)}, u32[]{:S(2)}) collective-permute-start(bf16[48,1024]{1,0:T(8,128)(2,1)S(1)} %get-tuple-element.88), channel_id=1, source_target_pairs={{0,6},{2,0},{4,2},{6,4},{1,7},{3,1},{5,3},{7,5},{8,14},{10,8},{12,... | collective-permute-start | bytes 294920 | tf_op jit(solution)/shard_map/ppermute | solution.py:27
  101.2 2.5 %collective-permute-done.21.low = bf16[48,1024]{1,0:T(8,128)(2,1)S(1)} collective-permute-done((bf16[48,1024]{1,0:T(8,128)(2,1)S(1)}, bf16[48,1024]{1,0:T(8,128)(2,1)S(1)}, u32[]{:S(2)}, u32[]{:S(2)}) %collective-permute-start.21) | collective-permute-done | bytes 98336 | tf_op jit(solution)/shard_map/ppermute | solution.py:27
  103.7 0.0 collective-permute-done.22.high
  103.7 0.1 shard_map.168
  103.7 0.9 collective-permute-start.23
  104.6 1.9 %collective-permute-start.24 = (bf16[48,2048]{1,0:T(8,128)(2,1)S(1)}, bf16[48,2048]{1,0:T(8,128)(2,1)S(1)}, u32[]{:S(2)}, u32[]{:S(2)}) collective-permute-start(bf16[48,2048]{1,0:T(8,128)(2,1)S(1)} %get-tuple-element.90), channel_id=1, source_target_pairs={{0,6},{2,0},{4,2},{6,4},{1,7},{3,1},{5,3},{7,5},{8,14},{10,8},{12,... | collective-permute-start | bytes 589832 | tf_op jit(solution)/shard_map/ppermute | solution.py:27
  106.5 3.7 %collective-permute-done.23 = bf16[48,2048]{1,0:T(8,128)(2,1)S(1)} collective-permute-done((bf16[48,2048]{1,0:T(8,128)(2,1)S(1)}, bf16[48,2048]{1,0:T(8,128)(2,1)S(1)}, u32[]{:S(2)}, u32[]{:S(2)}) %collective-permute-start.23) | collective-permute-done | bytes 196640 | tf_op jit(solution)/shard_map/ppermute | solution.py:27
  110.2 0.7 add_convert_fusion
  (30 shorter events, 0.1 us)
Async XLA Ops:
  0.0 15.2 %copy-start.6 = (bf16[2048]{0:T(1024)(128)(2,1)S(1)}, bf16[2048]{0:T(1024)(128)(2,1)}, u32[]{:S(2)}) copy-start(bf16[2048]{0:T(1024)(128)(2,1)} %param.17) | copy-start | bytes 12292
  1.6 23.3 %all-to-all-start = ((bf16[8,64,384]{2,1,0:T(8,128)(2,1)}), bf16[8,64,384]{2,1,0:T(8,128)(2,1)S(1)}, u32[]{:S(2)}, u32[]{:S(2)}) async-start(bf16[8,64,384]{2,1,0:T(8,128)(2,1)} %shard_map.157), calls=%async_computation | async-start | bytes 786432 | tf_op jit(solution)/shard_map/all_to_all | solution.py:435
  11.5 16.0 %collective-permute-start = (bf16[64,768]{1,0:T(8,128)(2,1)S(1)}, bf16[64,768]{1,0:T(8,128)(2,1)S(1)}, u32[]{:S(2)}, u32[]{:S(2)}) collective-permute-start(bf16[64,768]{1,0:T(8,128)(2,1)S(1)} %get-tuple-element.54.own), channel_id=1, source_target_pairs={{0,24},{8,0},{16,8},{24,16},{1,25},{9,1},{17,9},{25,17},{2,26},{10... | collective-permute-start | bytes 294920 | tf_op jit(solution)/shard_map/ppermute | solution.py:27
  14.1 13.4 %collective-permute-start.1 = (bf16[64,768]{1,0:T(8,128)(2,1)S(1)}, bf16[64,768]{1,0:T(8,128)(2,1)S(1)}, u32[]{:S(2)}, u32[]{:S(2)}) collective-permute-start(bf16[64,768]{1,0:T(8,128)(2,1)S(1)} %get-tuple-element.54.own), channel_id=1, source_target_pairs={{0,16},{8,24},{16,0},{24,8},{1,17},{9,25},{17,1},{25,9},{2,18},{10... | collective-permute-start | bytes 294920 | tf_op jit(solution)/shard_map/ppermute | solution.py:27
  14.6 12.9 %collective-permute-start.2 = (bf16[64,768]{1,0:T(8,128)(2,1)S(1)}, bf16[64,768]{1,0:T(8,128)(2,1)S(1)}, u32[]{:S(2)}, u32[]{:S(2)}) collective-permute-start(bf16[64,768]{1,0:T(8,128)(2,1)S(1)} %get-tuple-element.54.own), channel_id=1, source_target_pairs={{0,8},{8,16},{16,24},{24,0},{1,9},{9,17},{17,25},{25,1},{2,10},{10... | collective-permute-start | bytes 294920 | tf_op jit(solution)/shard_map/ppermute | solution.py:27
  24.8 16.1 %collective-permute-start.6 = (bf16[512,384]{1,0:T(8,128)(2,1)S(1)}, bf16[512,384]{1,0:T(8,128)(2,1)S(1)}, u32[]{:S(2)}, u32[]{:S(2)}) collective-permute-start(bf16[512,384]{1,0:T(8,128)(2,1)S(1)} %bitcast.11), channel_id=1, source_target_pairs={{0,8},{8,16},{16,24},{24,0},{1,9},{9,17},{17,25},{25,1},{2,10},{10... | collective-permute-start | bytes 1179656 | tf_op jit(solution)/shard_map/ppermute | solution.py:27
  26.0 14.9 %collective-permute-start.5 = (bf16[512,384]{1,0:T(8,128)(2,1)S(1)}, bf16[512,384]{1,0:T(8,128)(2,1)S(1)}, u32[]{:S(2)}, u32[]{:S(2)}) collective-permute-start(bf16[512,384]{1,0:T(8,128)(2,1)S(1)} %bitcast.12), channel_id=1, source_target_pairs={{0,24},{8,0},{16,8},{24,16},{1,25},{9,1},{17,9},{25,17},{2,26},{10... | collective-permute-start | bytes 1179656 | tf_op jit(solution)/shard_map/ppermute | solution.py:27
  28.3 13.5 %collective-permute-start.7 = (bf16[256,768]{1,0:T(8,128)(2,1)}, bf16[256,768]{1,0:T(8,128)(2,1)}, u32[]{:S(2)}, u32[]{:S(2)}) collective-permute-start(bf16[256,768]{1,0:T(8,128)(2,1)} %shard_map.158.refs_0_), channel_id=1, source_target_pairs={{0,32},{32,64},{64,96},{96,128},{128,160},{160,192},{192,224},{224... | collective-permute-start | bytes 1179656 | tf_op jit(solution)/shard_map/ppermute | solution.py:27
  28.3 13.5 %collective-permute-start.8 = (bf16[256,768]{1,0:T(8,128)(2,1)}, bf16[256,768]{1,0:T(8,128)(2,1)}, u32[]{:S(2)}, u32[]{:S(2)}) collective-permute-start(bf16[256,768]{1,0:T(8,128)(2,1)} %shard_map.158.refs_0_), channel_id=1, source_target_pairs={{0,224},{32,0},{64,32},{96,64},{128,96},{160,128},{192,160},{224,1... | collective-permute-start | bytes 1179656 | tf_op jit(solution)/shard_map/ppermute | solution.py:27
  31.0 3.8 %collective-permute-start.3 = (bf16[16,2048]{1,0:T(8,128)(2,1)S(1)}, bf16[16,2048]{1,0:T(8,128)(2,1)S(1)}, u32[]{:S(2)}, u32[]{:S(2)}) collective-permute-start(bf16[16,2048]{1,0:T(8,128)(2,1)S(1)} %get-tuple-element.52), channel_id=1, source_target_pairs={{0,8},{8,16},{16,24},{24,32},{32,40},{40,48},{48,56},{56,64},{64,7... | collective-permute-start | bytes 196616 | tf_op jit(solution)/shard_map/ppermute | solution.py:33
  34.8 15.2 %copy-start.7 = (f32[2,384,1]{1,2,0:T(1,128)S(1)}, f32[2,384,1]{1,2,0:T(1,128)}, u32[]{:S(2)}) copy-start(f32[2,384,1]{1,2,0:T(1,128)} %param.26) | copy-start | bytes 9220
  34.8 21.1 %copy-start.1 = (f32[2,128]{1,0:T(2,128)S(1)}, f32[2,128]{1,0:T(2,128)}, u32[]{:S(2)}) copy-start(f32[2,128]{1,0:T(2,128)} %slack.1) | copy-start | bytes 3076
  34.8 6.2 %collective-permute-start.4 = (bf16[16,2048]{1,0:T(8,128)(2,1)S(1)}, bf16[16,2048]{1,0:T(8,128)(2,1)S(1)}, u32[]{:S(2)}, u32[]{:S(2)}) collective-permute-start(bf16[16,2048]{1,0:T(8,128)(2,1)S(1)} %get-tuple-element.53), channel_id=1, source_target_pairs={{8,0},{16,8},{24,16},{32,24},{40,32},{48,40},{56,48},{64,56},{72,6... | collective-permute-start | bytes 196616 | tf_op jit(solution)/shard_map/ppermute | solution.py:33
  41.8 15.8 %collective-permute-start.11 = (bf16[256,768]{1,0:T(8,128)(2,1)}, bf16[256,768]{1,0:T(8,128)(2,1)}, u32[]{:S(2)}, u32[]{:S(2)}) collective-permute-start(bf16[256,768]{1,0:T(8,128)(2,1)} %collective-permute-done.7.refs_4_), channel_id=1, source_target_pairs={{0,32},{32,64},{64,96},{96,128},{128,160},{160,192},{192,224},{224... | collective-permute-start | bytes 1179656 | tf_op jit(solution)/shard_map/ppermute | solution.py:27
  45.1 12.5 %collective-permute-start.12 = (bf16[256,768]{1,0:T(8,128)(2,1)}, bf16[256,768]{1,0:T(8,128)(2,1)}, u32[]{:S(2)}, u32[]{:S(2)}) collective-permute-start(bf16[256,768]{1,0:T(8,128)(2,1)} %collective-permute-done.8.refs_1_), channel_id=1, source_target_pairs={{0,224},{32,0},{64,32},{96,64},{128,96},{160,128},{192,160},{224,1... | collective-permute-start | bytes 1179656 | tf_op jit(solution)/shard_map/ppermute | solution.py:27
  45.1 6.8 %collective-permute-start.10 = (bf16[256,384]{1,0:T(8,128)(2,1)S(1)}, bf16[256,384]{1,0:T(8,128)(2,1)S(1)}, u32[]{:S(2)}, u32[]{:S(2)}) collective-permute-start(bf16[256,384]{1,0:T(8,128)(2,1)S(1)} %slice.17), channel_id=1, source_target_pairs={{0,24},{8,0},{16,8},{24,16},{1,25},{9,1},{17,9},{25,17},{2,26},{10... | collective-permute-start | bytes 589832 | tf_op jit(solution)/shard_map/ppermute | solution.py:27
  49.9 5.9 %collective-permute-start.9 = (bf16[256,384]{1,0:T(8,128)(2,1)}, bf16[256,384]{1,0:T(8,128)(2,1)S(1)}, u32[]{:S(2)}, u32[]{:S(2)}) collective-permute-start(bf16[256,384]{1,0:T(8,128)(2,1)} %slice.16), channel_id=1, source_target_pairs={{0,8},{8,16},{16,24},{24,0},{1,9},{9,17},{17,25},{25,1},{2,10},{10... | collective-permute-start | bytes 589832 | tf_op jit(solution)/shard_map/ppermute | solution.py:27
  57.6 13.4 %collective-permute-start.16 = (bf16[256,768]{1,0:T(8,128)(2,1)}, bf16[256,768]{1,0:T(8,128)(2,1)S(1)}, u32[]{:S(2)}, u32[]{:S(2)}) collective-permute-start(bf16[256,768]{1,0:T(8,128)(2,1)} %collective-permute-done.11.refs_3_), channel_id=1, source_target_pairs={{0,32},{32,64},{64,96},{96,128},{128,160},{160,192},{192,224},{224... | collective-permute-start | bytes 1179656 | tf_op jit(solution)/shard_map/ppermute | solution.py:27
  57.8 13.1 %collective-permute-start.17 = (bf16[256,768]{1,0:T(8,128)(2,1)}, bf16[256,768]{1,0:T(8,128)(2,1)S(1)}, u32[]{:S(2)}, u32[]{:S(2)}) collective-permute-start(bf16[256,768]{1,0:T(8,128)(2,1)} %collective-permute-done.12.refs_2_), channel_id=1, source_target_pairs={{0,224},{32,0},{64,32},{96,64},{128,96},{160,128},{192,160},{224,1... | collective-permute-start | bytes 1179656 | tf_op jit(solution)/shard_map/ppermute | solution.py:27
  60.5 3.2 %collective-permute-start.13 = (bf16[2,144,128]{2,1,0:T(8,128)(2,1)S(1)}, bf16[2,144,128]{2,1,0:T(8,128)(2,1)S(1)}, u32[]{:S(2)}, u32[]{:S(2)}) collective-permute-start(bf16[2,144,128]{2,1,0:T(8,128)(2,1)S(1)} %get-tuple-element.62.own), channel_id=1, source_target_pairs={{0,24},{8,0},{16,8},{24,16},{1,25},{9,1},{17,9},{25,17},{2,26},{10... | collective-permute-start | bytes 221192 | tf_op jit(solution)/shard_map/ppermute | solution.py:27
  60.5 4.7 %collective-permute-start.14 = (bf16[2,144,128]{2,1,0:T(8,128)(2,1)S(1)}, bf16[2,144,128]{2,1,0:T(8,128)(2,1)S(1)}, u32[]{:S(2)}, u32[]{:S(2)}) collective-permute-start(bf16[2,144,128]{2,1,0:T(8,128)(2,1)S(1)} %get-tuple-element.62.own), channel_id=1, source_target_pairs={{0,16},{8,24},{16,0},{24,8},{1,17},{9,25},{17,1},{25,9},{2,18},{10... | collective-permute-start | bytes 221192 | tf_op jit(solution)/shard_map/ppermute | solution.py:27
  61.5 4.6 %collective-permute-start.15 = (bf16[2,144,128]{2,1,0:T(8,128)(2,1)S(1)}, bf16[2,144,128]{2,1,0:T(8,128)(2,1)S(1)}, u32[]{:S(2)}, u32[]{:S(2)}) collective-permute-start(bf16[2,144,128]{2,1,0:T(8,128)(2,1)S(1)} %get-tuple-element.62.own), channel_id=1, source_target_pairs={{0,8},{8,16},{16,24},{24,0},{1,9},{9,17},{17,25},{25,1},{2,10},{10... | collective-permute-start | bytes 221192 | tf_op jit(solution)/shard_map/ppermute | solution.py:27
  67.5 17.3 %all-to-all-start.1 = ((bf16[8,144,128]{2,1,0:T(8,128)(2,1)}), bf16[8,144,128]{2,1,0:T(8,128)(2,1)S(1)}, u32[]{:S(2)}, u32[]{:S(2)}) async-start(bf16[8,144,128]{2,1,0:T(8,128)(2,1)} %get-tuple-element.70), calls=%async_computation.1 | async-start | bytes 589824 | tf_op jit(solution)/shard_map/all_to_all | solution.py:502
  70.9 7.4 %copy-start.4 = (bf16[256,768]{1,0:T(8,128)(2,1)}, bf16[256,768]{1,0:T(8,128)(2,1)S(1)}, u32[]{:S(2)}) copy-start(bf16[256,768]{1,0:T(8,128)(2,1)S(1)} %collective-permute-done.16.refs_8_) | copy-start | bytes 1179652
  71.0 7.4 %copy-start.5 = (bf16[256,768]{1,0:T(8,128)(2,1)}, bf16[256,768]{1,0:T(8,128)(2,1)S(1)}, u32[]{:S(2)}) copy-start(bf16[256,768]{1,0:T(8,128)(2,1)S(1)} %collective-permute-done.17.refs_5_) | copy-start | bytes 1179652
  71.0 8.6 %collective-permute-start.18 = (bf16[128,768]{1,0:T(8,128)(2,1)S(1)}, bf16[128,768]{1,0:T(8,128)(2,1)S(1)}, u32[]{:S(2)}, u32[]{:S(2)}) collective-permute-start(bf16[128,768]{1,0:T(8,128)(2,1)S(1)} %slice.14), channel_id=1, source_target_pairs={{0,32},{32,64},{64,96},{96,128},{128,160},{160,192},{192,224},{224... | collective-permute-start | bytes 589832 | tf_op jit(solution)/shard_map/ppermute | solution.py:27
  72.4 7.1 %collective-permute-start.19 = (bf16[128,768]{1,0:T(8,128)(2,1)S(1)}, bf16[128,768]{1,0:T(8,128)(2,1)S(1)}, u32[]{:S(2)}, u32[]{:S(2)}) collective-permute-start(bf16[128,768]{1,0:T(8,128)(2,1)S(1)} %slice.15), channel_id=1, source_target_pairs={{0,224},{32,0},{64,32},{96,64},{128,96},{160,128},{192,160},{224,1... | collective-permute-start | bytes 589832 | tf_op jit(solution)/shard_map/ppermute | solution.py:27
  74.6 4.9 %copy-start = (bf16[31,128]{1,0:T(8,128)(2,1)S(1)}, bf16[31,128]{1,0:T(8,128)(2,1)}, u32[]{:S(2)}) copy-start(bf16[31,128]{1,0:T(8,128)(2,1)} %refs_14_.1) | copy-start | bytes 23812
  74.6 4.9 %copy-start.3 = (bf16[128]{0:T(256)(128)(2,1)S(1)}, bf16[128]{0:T(256)(128)(2,1)}, u32[]{:S(2)}) copy-start(bf16[128]{0:T(256)(128)(2,1)} %param.29) | copy-start | bytes 772
  79.6 5.2 %copy-start.2 = (bf16[128]{0:T(256)(128)(2,1)S(1)}, bf16[128]{0:T(256)(128)(2,1)}, u32[]{:S(2)}) copy-start(bf16[128]{0:T(256)(128)(2,1)} %param.27) | copy-start | bytes 772
  86.7 11.0 %collective-permute-start.20 = (bf16[4,48,2048]{2,1,0:T(8,128)(2,1)S(1)}, bf16[4,48,2048]{2,1,0:T(8,128)(2,1)S(1)}, u32[]{:S(2)}, u32[]{:S(2)}) collective-permute-start(bf16[4,48,2048]{2,1,0:T(8,128)(2,1)S(1)} %shard_map.166), channel_id=1, source_target_pairs={{0,1},{1,0},{2,3},{3,2},{4,5},{5,4},{6,7},{7,6},{8,9},{9,8},{10,11... | collective-permute-start | bytes 2359304 | tf_op jit(solution)/shard_map/ppermute | solution.py:27
  98.3 5.4 %collective-permute-start.21 = (bf16[48,1024]{1,0:T(8,128)(2,1)S(1)}, bf16[48,1024]{1,0:T(8,128)(2,1)S(1)}, u32[]{:S(2)}, u32[]{:S(2)}) collective-permute-start(bf16[48,1024]{1,0:T(8,128)(2,1)S(1)} %get-tuple-element.87), channel_id=1, source_target_pairs={{0,2},{2,4},{4,6},{6,0},{1,3},{3,5},{5,7},{7,1},{8,10},{10,12},{12... | collective-permute-start | bytes 294920 | tf_op jit(solution)/shard_map/ppermute | solution.py:27
  99.7 4.0 %collective-permute-start.22 = (bf16[48,1024]{1,0:T(8,128)(2,1)S(1)}, bf16[48,1024]{1,0:T(8,128)(2,1)S(1)}, u32[]{:S(2)}, u32[]{:S(2)}) collective-permute-start(bf16[48,1024]{1,0:T(8,128)(2,1)S(1)} %get-tuple-element.88), channel_id=1, source_target_pairs={{0,6},{2,0},{4,2},{6,4},{1,7},{3,1},{5,3},{7,5},{8,14},{10,8},{12,... | collective-permute-start | bytes 294920 | tf_op jit(solution)/shard_map/ppermute | solution.py:27
  103.7 6.5 %collective-permute-start.23 = (bf16[48,2048]{1,0:T(8,128)(2,1)S(1)}, bf16[48,2048]{1,0:T(8,128)(2,1)S(1)}, u32[]{:S(2)}, u32[]{:S(2)}) collective-permute-start(bf16[48,2048]{1,0:T(8,128)(2,1)S(1)} %get-tuple-element.89), channel_id=1, source_target_pairs={{0,2},{2,4},{4,6},{6,0},{1,3},{3,5},{5,7},{7,1},{8,10},{10,12},{12... | collective-permute-start | bytes 589832 | tf_op jit(solution)/shard_map/ppermute | solution.py:27
  104.6 5.6 %collective-permute-start.24 = (bf16[48,2048]{1,0:T(8,128)(2,1)S(1)}, bf16[48,2048]{1,0:T(8,128)(2,1)S(1)}, u32[]{:S(2)}, u32[]{:S(2)}) collective-permute-start(bf16[48,2048]{1,0:T(8,128)(2,1)S(1)} %get-tuple-element.90), channel_id=1, source_target_pairs={{0,6},{2,0},{4,2},{6,4},{1,7},{3,1},{5,3},{7,5},{8,14},{10,8},{12,... | collective-permute-start | bytes 589832 | tf_op jit(solution)/shard_map/ppermute | solution.py:27
